TPU v7x, 32 devices: a whole 2x2x4 slice. The times are simulated.
32 devices in a mesh: dp: 4 (over y, x), kv: 4 (over z), tp: 2 (over core).
Axes of the slice: x: 2, y: 2, z: 4, core: 2. Of those that a mesh axis runs over, the one named last changes fastest.
Arguments:
- stream: bfloat16 [32, 2048], P('dp', ('kv', 'tp')), parts along dimension 0, may hold values from -40 to 40
- old_state: float32 [32, 8, 64, 128], P(('dp', 'kv'), 'tp'), parts along dimension 0, may hold values from -6 to 6
- decay_amounts: float32 [32, 512], P(('dp', 'kv'), 'tp'), parts along dimension 0, may hold values from 0.003 to 1
- first_gain: float32 [2048], replicated, may hold values from 0.1 to 1.9
- first_gate: bfloat16 [2048, 5632], P(None, ('kv', 'tp')), may hold values from -0.125 to 0.125
- first_up: bfloat16 [2048, 5632], P(None, ('kv', 'tp')), may hold values from -0.125 to 0.125
- first_down: bfloat16 [5632, 2048], P(('kv', 'tp')), may hold values from -0.078125 to 0.078125
- mixer_gain: float32 [2048], P('kv'), may hold values from 0.1 to 1.9
- query_weight: bfloat16 [2048, 512], P('kv', 'tp'), may hold values from -0.125 to 0.125
- key_weight: bfloat16 [2048, 512], P('kv', 'tp'), may hold values from -0.125 to 0.125
- decay_weight: bfloat16 [2048, 512], P('kv', 'tp'), may hold values from -0.5 to 0.5
- value_weight: bfloat16 [2048, 1024], P('kv', 'tp'), may hold values from -0.125 to 0.125
- output_gate_weight: bfloat16 [2048, 1024], P('kv', 'tp'), may hold values from -0.125 to 0.125
- head_gain: float32 [1024], P('tp'), may hold values from 0.1 to 1.9
- output_weight: bfloat16 [1024, 2048], P('tp', 'kv'), may hold values from -0.1875 to 0.1875
- second_gain: float32 [2048], replicated, may hold values from 0.1 to 1.9
- second_gate: bfloat16 [2048, 5632], P(None, ('kv', 'tp')), may hold values from -0.125 to 0.125
- second_up: bfloat16 [2048, 5632], P(None, ('kv', 'tp')), may hold values from -0.125 to 0.125
- second_down: bfloat16 [5632, 2048], P(('kv', 'tp')), may hold values from -0.078125 to 0.078125
Outputs:
- mixed_stream: bfloat16 [32, 2048], P('dp', ('kv', 'tp')), parts along dimension 0
- new_state: float32 [32, 8, 64, 128], P(('dp', 'kv'), 'tp'), parts along dimension 0
There are 4 independent parts, one for each index of `dp`. A program takes and returns all parts, laid end to end along the dimension named above; an argument that names none is the same for every part. Nothing has to cross between parts.
All inputs are finite; a program needn't handle non-finite values.
Results may differ from a plain program's by a relative error of at most 0.007.
Values may be sent and summed in bfloat16 or wider, within the bound.
No kernel may reach another device: no remote copies, remote signals or barrier semaphores. Data moves between devices by JAX's collectives and lax.ppermute only.
A program may use at most 64 MiB of HBM per device.

v0:
```python
import functools

import jax
import jax.numpy as jnp
from jax import lax
from jax.experimental import pallas as pl
from jax.experimental.pallas import tpu as pltpu
from jax.sharding import PartitionSpec as P


EPSILON = 1e-06
GATE_SOFTNESS = 16.0
f32 = jnp.float32
bf16 = jnp.bfloat16
LANES = 128
WAIT = 6_000_000_000


def shape(dims, dtype=f32):
    return jax.ShapeDtypeStruct(tuple(dims), dtype)


def call(kernel, outs, *args, scratch=(), flops=0, limit=4, moved=None):
    vmem = pl.BlockSpec(memory_space=pltpu.VMEM)
    moved = moved or 1 << 16
    return pl.pallas_call(
        kernel,
        out_shape=outs,
        in_specs=[vmem] * len(args),
        out_specs=jax.tree.map(lambda _: vmem, outs),
        scratch_shapes=list(scratch),
        cost_estimate=pl.CostEstimate(flops=flops, bytes_accessed=moved, transcendentals=0),
        compiler_params=pltpu.CompilerParams(vmem_limit_bytes=limit << 20),
    )(*args)


def swap(x, axis, size, shift):
    return lax.ppermute(x, axis, [(j, j ^ shift) for j in range(size)])


def send_kv(blocks, n_kv):
    got = []
    for s in range(1, n_kv):
        got.append(swap(blocks[s - 1], ("kv", "tp"), 2 * n_kv, 2 * s + 1))
    return got


def lend(arrays):
    got = []
    for array in arrays:
        got.append(swap(array, "tp", 2, 1))
    return got


silu = jax.nn.silu


def dot_t(a, b):
    return lax.dot_general(a, b, (((1,), (1,)), ((), ())), preferred_element_type=f32)


def dot(a, b):
    return jnp.dot(a, b, preferred_element_type=f32)


def add_pieces(pieces, order, gain, w_gate, w_up, gate, up, square):
    kv = lax.axis_index("kv")
    for piece, s in zip(pieces, order):
        width = piece.shape[1]
        cols = pl.ds(pl.multiple_of((kv ^ s) * width, width), width)
        wide = piece.astype(f32)
        scaled = (wide * gain[:, cols]).astype(bf16)
        one = dot_t(scaled, w_gate[:, cols])
        two = dot_t(scaled, w_up[:, cols])
        gate = one if gate is None else gate + one
        up = two if up is None else up + two
        squares = jnp.sum(wide * wide, axis=1, keepdims=True)
        square = squares if square is None else square + squares
    return gate, up, square


def hidden_of(gate, up, square, depth):
    scale = lax.rsqrt(square / depth + EPSILON)
    return (silu(gate * scale) * (up * scale)).astype(bf16)


def copy_kernel(x, out):
    out[...] = x[...]


def pair_kernel(mine, other, both):
    lower = lax.axis_index("tp") == 0
    own = mine.shape[1]
    one, two = mine[...].astype(f32), other[...].astype(f32)
    both[:, :own] = jnp.where(lower, one, two).astype(bf16)
    both[:, own:] = jnp.where(lower, two, one).astype(bf16)


def up_first_kernel(x, gain, w_gate, w_up, w_later, acc, sq):
    gate, up, square = add_pieces([x[...]], [0], gain, w_gate, w_up, None, None, None)
    acc[0], acc[1] = gate, up
    sq[...] = jnp.broadcast_to(square, sq.shape)


def up_more_kernel(s, x, gain, w_gate, w_up, acc, sq, acc_out, sq_out):
    gate, up, square = add_pieces([x[...]], [s], gain, w_gate, w_up, acc[0], acc[1], sq[:, :1])
    acc_out[0], acc_out[1] = gate, up
    sq_out[...] = jnp.broadcast_to(square, sq_out.shape)


def first_kernel(x, gain, w_gate, w_up, acc, sq, w_down, *outs):
    gate, up, square = add_pieces([x[...]], [1], gain, w_gate, w_up, acc[0], acc[1], sq[:, :1])
    hidden = hidden_of(gate, up, square, w_gate.shape[1])
    kv = lax.axis_index("kv")
    for s, out in enumerate(outs):
        width = out.shape[1]
        cols = pl.ds(pl.multiple_of((kv ^ s) * width, width), width)
        out[...] = dot(hidden, w_down[:, cols]).astype(out.dtype)


def sum_kernel(*refs):
    *ins, out = refs
    total = ins[0][...]
    for ref in ins[1:]:
        total = total + ref[...].astype(f32)
    out[...] = total


def project_kernel(mine, other, x, gain, *refs):
    weights, middle, outs, scr = refs[:10], refs[10], refs[11:-1], refs[-1]
    kv = lax.axis_index("kv")
    mid = (x[...].astype(f32) + 0.5 * (mine[...] + other[...])).astype(bf16)
    middle[...] = mid
    wide = mid.astype(f32)
    scaled = (wide * gain[...]).astype(bf16)
    n, height, width = scr.shape
    squares = jnp.sum(wide * wide, axis=1, keepdims=True)
    rows = wide.shape[0] // n
    high = squares.astype(bf16).astype(f32)
    squares = jnp.concatenate(
        [jnp.broadcast_to(part, (wide.shape[0], LANES)) for part in (high, squares - high)], axis=1
    )
    half = len(weights) // 2
    for side in range(2):
        q, k, z, v, o = (dot(scaled, w[...]) for w in weights[side * half:(side + 1) * half])
        chunk = 0
        for part in (q, k, z, squares, v, o):
            for at in range(0, part.shape[1], LANES):
                down, across = chunk_place(chunk, rows, height, side * width // 2)
                for j in range(n):
                    scr[j, down, across] = part[j * rows:(j + 1) * rows, at:at + LANES]
                chunk += 1
    for s, out in enumerate(outs):
        out[...] = scr[kv ^ s].astype(out.dtype)


def chunk_place(chunk, rows, height, start):
    per = height // rows
    down = chunk % per * rows
    across = start + chunk // per * LANES
    return slice(down, down + rows), slice(across, across + LANES)


def extras_kernel(amounts, head_gain, out):
    pieces = [amounts[:, at:at + LANES] for at in range(0, amounts.shape[1], LANES)]
    pieces += [head_gain[:, at:at + LANES] for at in range(0, head_gain.shape[1], LANES)]
    at = 0
    for piece in pieces:
        out[at:at + piece.shape[0]] = piece
        at += piece.shape[0]


def gates_of(depth, block, extras):
    half = block.shape[0] // 2
    qk, zs, value, gate = (block[:, at:at + LANES] for at in range(0, 4 * LANES, LANES))
    rows = half // 2
    squares = zs[half:half + rows, :1] + zs[half + rows:, :1]
    scale = lax.rsqrt(squares / depth + EPSILON)
    scale = jnp.concatenate([scale, scale], axis=0)
    query, key = qk[:half] * scale, qk[half:] * scale
    z = zs[:half] * scale
    scale = jnp.concatenate([scale, scale], axis=0)
    log_sigmoid = jnp.minimum(z, 0.0) - jnp.log1p(jnp.exp(-jnp.abs(z)))
    decay = jnp.exp(log_sigmoid / GATE_SOFTNESS - extras[:half])
    query = query * (LANES // 2) ** (-0.5)
    return query, key, decay, value * scale, gate * scale


def turn(*arrays):
    stacked = jnp.concatenate(arrays, axis=0)
    short = -stacked.shape[0] % 8
    if short:
        stacked = jnp.concatenate([stacked, jnp.zeros((short, LANES), f32)], axis=0)
    return stacked.T


def mix_heads(depth, block, old, extras):
    rows, heads, keys, values = old.shape
    query, key, decay, value, gate = gates_of(depth, block, extras)
    columns = turn(query * decay)
    agree = query * key
    first_half = lax.broadcasted_iota(jnp.int32, agree.shape, 1) < keys
    low = jnp.sum(jnp.where(first_half, agree, 0.0), axis=1, keepdims=True)
    high = jnp.sum(jnp.where(first_half, 0.0, agree), axis=1, keepdims=True)
    both, gains, reads = [], [], []
    for h in range(heads):
        pair = h // 2
        both.append((high if h % 2 else low)[pair * rows:(pair + 1) * rows])
        row = query.shape[0] + h
        gains.append(jnp.broadcast_to(extras[row:row + 1], (rows, values)))
        at = slice(h % 2 * keys, (h % 2 + 1) * keys)
        for b in range(rows):
            column = columns[at, pair * rows + b:pair * rows + b + 1]
            reads.append(jnp.sum(column * old[b, h], axis=0, keepdims=True))
    readout = jnp.concatenate(reads, axis=0) + jnp.concatenate(both, axis=0) * value
    normed = readout * lax.rsqrt(jnp.mean(readout * readout, axis=1, keepdims=True) + EPSILON)
    return normed * jnp.concatenate(gains, axis=0) * silu(gate)


def mix_kernel(depth, *refs):
    *ins, old, old_other, extras, extras_other, mixed, total = refs
    rows, heads, _, values = old.shape
    half = ins[0].shape[1] // 2
    mine, theirs = ins[0][:, :half], ins[0][:, half:]
    for ref in ins[1:]:
        mine, theirs = mine + ref[:, half:].astype(f32), theirs + ref[:, :half].astype(f32)
    total[...] = mine
    for side, result in enumerate((
        mix_heads(depth, mine, old, extras[...]),
        mix_heads(depth, theirs, old_other, extras_other[...]),
    )):
        for h in range(heads):
            at = (side * heads + h) * values
            mixed[:, at:at + values] = result[h * rows:(h + 1) * rows].astype(bf16)


def state_kernel(depth, total, old, extras, new):
    rows, heads, keys, _ = old.shape
    _, key, decay, value, _ = gates_of(depth, total[...], extras[...])
    half = key.shape[0]
    columns = turn(key, decay)
    for h in range(heads):
        at = slice(h % 2 * keys, (h % 2 + 1) * keys)
        for b in range(rows):
            i = h // 2 * rows + b
            row = value[h * rows + b:h * rows + b + 1]
            new[b, h] = columns[at, half + i:half + i + 1] * old[b, h] + columns[at, i:i + 1] * row


def after_kernel(*refs):
    *ins, middle, w_mine, w_theirs, after, scr = refs
    kv = lax.axis_index("kv")
    half = w_mine.shape[0]
    for s, ref in enumerate(ins):
        one, two = ref[:, :half].astype(f32), ref[:, half:].astype(f32)
        scr[kv ^ s, :, :half] = one if s == 0 else two
        scr[kv ^ s, :, half:] = two if s == 0 else one
    heads = jnp.concatenate([scr[j] for j in range(len(ins))], axis=0).astype(bf16)
    mine = dot(heads[:, :half], w_mine[...]).astype(bf16).astype(f32)
    theirs = dot(heads[:, half:], w_theirs[...]).astype(bf16).astype(f32)
    after[...] = (middle[...].astype(f32) + (mine + theirs)).astype(bf16)


def down_halves(hidden, w_down, sides, out):
    kv = lax.axis_index("kv")
    width = out.shape[2]
    for s, side in enumerate(sides):
        cols = pl.ds(pl.multiple_of(((kv ^ s) * 2 + side) * width, width), width)
        out[s] = dot(hidden, w_down[:, cols])


def second_kernel(x, gain, w_gate, w_up, acc, sq, w_down, hidden, theirs):
    gate, up, square = add_pieces([x[...]], [1], gain, w_gate, w_up, acc[0], acc[1], sq[:, :1])
    hid = hidden_of(gate, up, square, w_gate.shape[1])
    hidden[...] = hid
    tp = lax.axis_index("tp")
    down_halves(hid, w_down, [1 - tp] + [tp] * (theirs.shape[0] - 1), theirs)


def second_mine_kernel(hidden, w_down, mine):
    tp = lax.axis_index("tp")
    down_halves(hidden[...], w_down, [tp] + [1 - tp] * (mine.shape[0] - 1), mine)


def split_sum_kernel(mine, other, *outs):
    for s, out in enumerate(outs):
        out[...] = (mine[s] + other[s]).astype(out.dtype)


def last_kernel(after, *refs):
    *ins, out = refs
    total = ins[0][...]
    for ref in ins[1:]:
        total = total + ref[...].astype(f32)
    own = out.shape[1]
    lower = lax.axis_index("tp") == 0
    base = jnp.where(lower, after[:, :own].astype(f32), after[:, own:].astype(f32))
    out[...] = (base + 0.5 * total).astype(bf16)


def body(n_kv, n_tp,
    stream, old_state, decay_amounts, first_gain, first_gate, first_up, first_down, mixer_gain,
    query_weight, key_weight, decay_weight, value_weight, output_gate_weight, head_gain, output_weight,
    second_gain, second_gate, second_up, second_down,
):
    rows, own = stream.shape
    pair = own * n_tp
    depth = pair * n_kv
    hid = first_gate.shape[1]
    local_rows, heads, keys, values = old_state.shape
    nk, nv = heads * keys, heads * values
    sums = lambda dims: [shape(dims)] + [shape(dims, bf16)] * (n_kv - 1)
    acc_shape = [shape((2, rows, hid)), shape((rows, LANES))]
    g1, g2, gm, gh = (g.reshape(1, -1) for g in (first_gain, second_gain, mixer_gain, head_gain))

    near = call(copy_kernel, shape(stream.shape, bf16), stream, flops=WAIT)
    wide = call(pair_kernel, shape((rows, pair), bf16), near, swap(stream, "tp", n_tp, 1), flops=2 * WAIT)
    wide = call(copy_kernel, shape((rows, pair), bf16), wide, flops=WAIT)
    others = send_kv([wide] * (n_kv - 1), n_kv)
    up_flops = 4 * rows * pair * hid
    wg, wu = first_gate.T, first_up.T

    def up(x, others, gain, wg, wu, down):
        acc = call(up_first_kernel, acc_shape, x, gain, wg, wu, down, flops=up_flops, limit=12)
        for s in range(n_kv - 1, 1, -1):
            acc = call(
                functools.partial(up_more_kernel, s), acc_shape, others[s - 1], gain, wg, wu, *acc,
                flops=up_flops, limit=12,
            )
        return acc

    acc = up(wide, others, g1, wg, wu, first_down)
    blocks = call(
        first_kernel, sums((rows, pair)), others[0], g1, wg, wu, *acc, first_down,
        flops=2 * up_flops, limit=16,
    )
    weights = (query_weight, key_weight, decay_weight, value_weight, output_gate_weight)
    lent = lend(weights)
    extras = call(extras_kernel, shape((heads // 2 * local_rows + heads, LANES)), decay_amounts, gh)
    mine = call(
        sum_kernel, shape((rows, pair)), blocks[0], *send_kv(blocks[1:], n_kv),
        flops=WAIT,
    )
    old_other, w_other, extras_other = lend((old_state, output_weight, extras))
    other = swap(mine, "tp", n_tp, 1)
    total = 2 * (3 * nk + 2 * nv + 2 * LANES)
    dense = (8, total * local_rows // 8)
    middle, *parts = call(
        project_kernel, [shape((rows, pair), bf16)] + sums(dense),
        mine, other, wide, gm, *weights, *lent, scratch=[pltpu.VMEM((n_kv,) + dense, f32)],
        flops=2 * rows * pair * total, limit=8,
    )
    mixed, summed = call(
        functools.partial(mix_kernel, depth),
        [shape((local_rows, 2 * nv), bf16), shape((8, dense[1] // 2))],
        parts[0], *send_kv(parts[1:], n_kv), old_state, old_other, extras, extras_other,
        flops=8 * old_state.size,
    )
    new_state = call(
        functools.partial(state_kernel, depth), shape(old_state.shape), summed, old_state, extras,
        flops=1_000_000_000,
    )
    after = call(
        after_kernel, shape((rows, pair), bf16), mixed, *send_kv([mixed] * (n_kv - 1), n_kv),
        middle, output_weight, w_other, scratch=[pltpu.VMEM((n_kv, local_rows, 2 * nv), f32)],
        flops=WAIT,
    )
    others = send_kv([after] * (n_kv - 1), n_kv)
    wg, wu = second_gate.T, second_up.T
    acc = up(after, others, g2, wg, wu, second_down)
    hidden, theirs = call(
        second_kernel, [shape((rows, hid), bf16), shape((n_kv, rows, own))],
        others[0], g2, wg, wu, *acc, second_down, flops=2 * up_flops, limit=16,
    )
    arrived = swap(theirs, "tp", n_tp, 1)
    mine = call(
        second_mine_kernel, shape((n_kv, rows, own)), hidden, second_down,
        flops=up_flops, limit=12,
    )
    blocks = call(split_sum_kernel, sums((rows, own)), mine, arrived)
    mixed_stream = call(last_kernel, shape((rows, own), bf16), after, blocks[0], *send_kv(blocks[1:], n_kv))
    return (mixed_stream, new_state)


def half_block(stream, norm_gain, w_gate, w_up, w_down):
    wide = lax.all_gather(stream, ("kv", "tp"), axis=1, tiled=True).astype(jnp.float32)
    scaled = (wide * norm_gain).astype(jnp.bfloat16)
    gate_acc = jnp.dot(scaled, w_gate, preferred_element_type=jnp.float32)
    up_acc = jnp.dot(scaled, w_up, preferred_element_type=jnp.float32)
    square_acc = jnp.sum(wide * wide, axis=1)
    row_scale = lax.rsqrt(square_acc / norm_gain.shape[0] + EPSILON)[:, None]
    hidden = (jax.nn.silu(gate_acc * row_scale) * (up_acc * row_scale)).astype(jnp.bfloat16)
    partial_out = jnp.dot(hidden, w_down, preferred_element_type=jnp.float32)
    summed = lax.psum_scatter(partial_out, ("kv", "tp"), scatter_dimension=1, tiled=True)
    return (stream.astype(jnp.float32) + 0.5 * summed).astype(jnp.bfloat16)


def wide_body(
    stream,
    old_state,
    decay_amounts,
    first_gain,
    first_gate,
    first_up,
    first_down,
    mixer_gain,
    query_weight,
    key_weight,
    decay_weight,
    value_weight,
    output_gate_weight,
    head_gain,
    output_weight,
    second_gain,
    second_gate,
    second_up,
    second_down,
):
    middle = half_block(stream, first_gain, first_gate, first_up, first_down)
    paired_cols = lax.all_gather(middle, "tp", axis=1, tiled=True)
    wide_cols = paired_cols.astype(jnp.float32)
    scaled = (wide_cols * mixer_gain).astype(jnp.bfloat16)
    query_part = jnp.dot(scaled, query_weight, preferred_element_type=jnp.float32)
    key_part = jnp.dot(scaled, key_weight, preferred_element_type=jnp.float32)
    decay_part = jnp.dot(scaled, decay_weight, preferred_element_type=jnp.float32)
    value_part = jnp.dot(scaled, value_weight, preferred_element_type=jnp.float32)
    outgate_part = jnp.dot(scaled, output_gate_weight, preferred_element_type=jnp.float32)
    local_rows = old_state.shape[0]
    local_heads = old_state.shape[1]
    key_dim = old_state.shape[2]
    value_dim = old_state.shape[3]
    query_sum, key_sum, decay_sum, value_sum, outgate_sum, own_squares = (
        lax.psum_scatter(query_part, "kv", scatter_dimension=0, tiled=True),
        lax.psum_scatter(key_part, "kv", scatter_dimension=0, tiled=True),
        lax.psum_scatter(decay_part, "kv", scatter_dimension=0, tiled=True),
        lax.psum_scatter(value_part, "kv", scatter_dimension=0, tiled=True),
        lax.psum_scatter(outgate_part, "kv", scatter_dimension=0, tiled=True),
        lax.psum_scatter(
            jnp.sum(wide_cols * wide_cols, axis=1), "kv", scatter_dimension=0, tiled=True
        ),
    )
    row_scale = lax.rsqrt(own_squares / (wide_cols.shape[1] * lax.axis_size("kv")) + EPSILON)[:, None]
    query = (query_sum * row_scale * key_dim ** (-0.5)).reshape(local_rows, local_heads, key_dim)
    keys = (key_sum * row_scale).reshape(local_rows, local_heads, key_dim)
    gate_logits = (decay_sum * row_scale).reshape(local_rows, local_heads, key_dim)
    values = (value_sum * row_scale).reshape(local_rows, local_heads, value_dim)
    decay_logarithm = jax.nn.log_sigmoid(gate_logits) / GATE_SOFTNESS - decay_amounts.reshape(
        local_rows, local_heads, key_dim
    )
    new_state = (
        jnp.exp(decay_logarithm)[..., None] * old_state + keys[..., None] * values[:, :, None, :]
    )
    readout = jnp.einsum("bhk,bhkv->bhv", query, new_state, precision=lax.Precision.HIGHEST)
    normed = readout * lax.rsqrt(jnp.mean(readout * readout, axis=-1, keepdims=True) + EPSILON)
    mixed_heads = (
        normed.reshape(local_rows, local_heads * value_dim)
        * head_gain
        * jax.nn.silu(outgate_sum * row_scale)
    ).astype(jnp.bfloat16)
    projected = jnp.dot(
        lax.all_gather(mixed_heads, "kv", axis=0, tiled=True),
        output_weight,
        preferred_element_type=jnp.float32,
    ).astype(jnp.bfloat16)
    attention_out = lax.psum_scatter(
        lax.optimization_barrier(projected).astype(jnp.float32).astype(jnp.bfloat16),
        "tp",
        scatter_dimension=1,
        tiled=True,
    ).astype(jnp.float32)
    after = (middle.astype(jnp.float32) + attention_out).astype(jnp.bfloat16)
    mixed_stream = half_block(after, second_gain, second_gate, second_up, second_down)
    return (mixed_stream, new_state)


def solution(mesh):
    n_kv, n_tp = mesh.shape["kv"], mesh.shape["tp"]
    few = n_kv <= 8 and n_kv & (n_kv - 1) == 0 and n_tp == 2
    program = functools.partial(body, n_kv, n_tp) if few else wide_body
    in_specs = (
        P("dp", ("kv", "tp")),
        P(("dp", "kv"), "tp", None, None),
        P(("dp", "kv"), "tp"),
        P(),
        P(None, ("kv", "tp")),
        P(None, ("kv", "tp")),
        P(("kv", "tp"), None),
        P("kv"),
        P("kv", "tp"),
        P("kv", "tp"),
        P("kv", "tp"),
        P("kv", "tp"),
        P("kv", "tp"),
        P("tp"),
        P("tp", "kv"),
        P(),
        P(None, ("kv", "tp")),
        P(None, ("kv", "tp")),
        P(("kv", "tp"), None),
    )
    out_specs = (P("dp", ("kv", "tp")), P(("dp", "kv"), "tp", None, None))
    return jax.shard_map(program, mesh=mesh, in_specs=in_specs, out_specs=out_specs, check_vma=False)
```

profile of v0, /device:TPU:0, one launch (start us, length us, event | category | flops | bytes accessed | tf_op | source)
XLA Modules:
  0.0 54.7 jit_solution(8832430644310163425)
XLA Ops:
  0.6 0.6 %collective-permute-start = (bf16[8,256]{1,0:T(8,128)(2,1)}, bf16[8,256]{1,0:T(8,128)(2,1)S(1)}, u32[]{:S(2)}, u32[]{:S(2)}) collective-permute-start(bf16[8,256]{1,0:T(8,128)(2,1)} %x.1), channel_id=1, source_target_pairs={{0,1},{1,0},{2,3},{3,2},{4,5},{5,4},{6,7},{7,6},{8,9},{9,8},{10,11... | collective-permute-start | bytes 12296 | tf_op jit(solution)/shard_map/ppermute | solution.py:38
  1.2 0.7 %copy-done.18 = bf16[8,256]{1,0:T(8,128)(2,1)S(1)} copy-done((bf16[8,256]{1,0:T(8,128)(2,1)S(1)}, bf16[8,256]{1,0:T(8,128)(2,1)}, u32[]{:S(2)}) %copy-start.18) | copy-done | bytes 4120
  2.3 4.8 %collective-permute-start.3 = (bf16[8,512]{1,0:T(8,128)(2,1)S(1)}, bf16[8,512]{1,0:T(8,128)(2,1)S(1)}, u32[]{:S(2)}, u32[]{:S(2)}) collective-permute-start(bf16[8,512]{1,0:T(8,128)(2,1)S(1)} %shard_map.196.x), channel_id=1, source_target_pairs={{0,7},{1,6},{2,5},{3,4},{4,3},{5,2},{6,1},{7,0},{8,15},{9,14},{10,... | collective-permute-start | bytes 24584 | tf_op jit(solution)/shard_map/ppermute | solution.py:38
  7.0 0.6 %collective-permute-start.1 = (bf16[8,512]{1,0:T(8,128)(2,1)S(1)}, bf16[8,512]{1,0:T(8,128)(2,1)S(1)}, u32[]{:S(2)}, u32[]{:S(2)}) collective-permute-start(bf16[8,512]{1,0:T(8,128)(2,1)S(1)} %shard_map.196.x), channel_id=1, source_target_pairs={{0,3},{1,2},{2,1},{3,0},{4,7},{5,6},{6,5},{7,4},{8,11},{9,10},{10,... | collective-permute-start | bytes 24584 | tf_op jit(solution)/shard_map/ppermute | solution.py:38
  7.6 0.5 shard_map.197
  8.9 2.1 %collective-permute-done.2.x = bf16[8,512]{1,0:T(8,128)(2,1)S(1)} collective-permute-done((bf16[8,512]{1,0:T(8,128)(2,1)S(1)}, bf16[8,512]{1,0:T(8,128)(2,1)S(1)}, u32[]{:S(2)}, u32[]{:S(2)}) %collective-permute-start.2) | collective-permute-done | bytes 8224 | tf_op jit(solution)/shard_map/ppermute | solution.py:38
  11.5 0.9 %shard_map.200 = (f32[8,512]{1,0:T(8,128)S(1)}, bf16[8,512]{1,0:T(8,128)(2,1)S(1)}, bf16[8,512]{1,0:T(8,128)(2,1)S(1)}, bf16[8,512]{1,0:T(8,128)(2,1)S(1)}) custom-call(bf16[8,512]{1,0:T(8,128)(2,1)S(1)} %collective-permute-done.1.x, f32[1,2048]{1,0:T(1,128)S(1)} %bitcast.27, bf16[704,2048]{1,0:T(8,128)(2,1)S(1)} %bitcast.11, ...), custom_call_target="tpu_custom_call" | custom-call | flops 23068672 | bytes 65536 | tf_op jit(solution)/shard_map/pallas_call | solution.py:26
  12.4 1.9 %collective-permute-start.5 = (bf16[8,512]{1,0:T(8,128)(2,1)S(1)}, bf16[8,512]{1,0:T(8,128)(2,1)S(1)}, u32[]{:S(2)}, u32[]{:S(2)}) collective-permute-start(bf16[8,512]{1,0:T(8,128)(2,1)S(1)} %get-tuple-element.39), channel_id=1, source_target_pairs={{0,5},{1,4},{2,7},{3,6},{4,1},{5,0},{6,3},{7,2},{8,13},{9,12},{10,... | collective-permute-start | bytes 24584 | tf_op jit(solution)/shard_map/ppermute | solution.py:38
  14.3 2.1 %collective-permute-start.6 = (bf16[8,512]{1,0:T(8,128)(2,1)S(1)}, bf16[8,512]{1,0:T(8,128)(2,1)S(1)}, u32[]{:S(2)}, u32[]{:S(2)}) collective-permute-start(bf16[8,512]{1,0:T(8,128)(2,1)S(1)} %get-tuple-element.40), channel_id=1, source_target_pairs={{0,7},{1,6},{2,5},{3,4},{4,3},{5,2},{6,1},{7,0},{8,15},{9,14},{10,... | collective-permute-start | bytes 24584 | tf_op jit(solution)/shard_map/ppermute | solution.py:38
  17.2 2.0 %collective-permute-done.6.refs_3_ = bf16[8,512]{1,0:T(8,128)(2,1)S(1)} collective-permute-done((bf16[8,512]{1,0:T(8,128)(2,1)S(1)}, bf16[8,512]{1,0:T(8,128)(2,1)S(1)}, u32[]{:S(2)}, u32[]{:S(2)}) %collective-permute-start.6) | collective-permute-done | bytes 8224 | tf_op jit(solution)/shard_map/ppermute | solution.py:38
  19.6 0.6 %copy-done.8 = bf16[512,256]{1,0:T(8,128)(2,1)S(1)} copy-done((bf16[512,256]{1,0:T(8,128)(2,1)S(1)}, bf16[512,256]{1,0:T(8,128)(2,1)}, u32[]{:S(2)}) %copy-start.8) | copy-done | bytes 262168
  21.1 0.7 %collective-permute-done.8.refs_5_ = bf16[512,256]{1,0:T(8,128)(2,1)S(1)} collective-permute-done((bf16[512,256]{1,0:T(8,128)(2,1)S(1)}, bf16[512,256]{1,0:T(8,128)(2,1)S(1)}, u32[]{:S(2)}, u32[]{:S(2)}) %collective-permute-start.8) | collective-permute-done | bytes 262176 | tf_op jit(solution)/shard_map/ppermute | solution.py:38
  22.0 0.9 %collective-permute-done.9.refs_6_ = bf16[512,256]{1,0:T(8,128)(2,1)S(1)} collective-permute-done((bf16[512,256]{1,0:T(8,128)(2,1)S(1)}, bf16[512,256]{1,0:T(8,128)(2,1)S(1)}, u32[]{:S(2)}, u32[]{:S(2)}) %collective-permute-start.9) | collective-permute-done | bytes 262176 | tf_op jit(solution)/shard_map/ppermute | solution.py:38
  23.1 0.6 %shard_map.202 = (bf16[8,512]{1,0:T(8,128)(2,1)S(1)}, f32[8,1024]{1,0:T(8,128)S(1)}, bf16[8,1024]{1,0:T(8,128)(2,1)S(1)}, bf16[8,1024]{1,0:T(8,128)(2,1)S(1)}, bf16[8,1024]{1,0:T(8,128)(2,1)S(1)}) custom-call(f32[8,512]{1,0:T(8,128)S(1)} %shard_map.201.mine, f32[8,512]{1,0:T(8,128)S(1)} %collective-permute-done.7.other, bf16[8,512]{1,0:T(8,128)(2,1)S(1)} %shard_map.196.x, ...), custom_call_target="tpu_custom_call" | custom-call | flops 33554432 | bytes 65536 | tf_op jit(solution)/shard_map/pallas_call | solution.py:26
  23.8 2.6 %collective-permute-start.14 = (bf16[8,1024]{1,0:T(8,128)(2,1)S(1)}, bf16[8,1024]{1,0:T(8,128)(2,1)S(1)}, u32[]{:S(2)}, u32[]{:S(2)}) collective-permute-start(bf16[8,1024]{1,0:T(8,128)(2,1)S(1)} %get-tuple-element.43), channel_id=1, source_target_pairs={{0,5},{1,4},{2,7},{3,6},{4,1},{5,0},{6,3},{7,2},{8,13},{9,12},{10,... | collective-permute-start | bytes 49160 | tf_op jit(solution)/shard_map/ppermute | solution.py:38
  26.4 1.4 %collective-permute-start.15 = (bf16[8,1024]{1,0:T(8,128)(2,1)S(1)}, bf16[8,1024]{1,0:T(8,128)(2,1)S(1)}, u32[]{:S(2)}, u32[]{:S(2)}) collective-permute-start(bf16[8,1024]{1,0:T(8,128)(2,1)S(1)} %get-tuple-element.44), channel_id=1, source_target_pairs={{0,7},{1,6},{2,5},{3,4},{4,3},{5,2},{6,1},{7,0},{8,15},{9,14},{10,... | collective-permute-start | bytes 49160 | tf_op jit(solution)/shard_map/ppermute | solution.py:38
  27.9 3.4 %collective-permute-done.15.refs_3_ = bf16[8,1024]{1,0:T(8,128)(2,1)S(1)} collective-permute-done((bf16[8,1024]{1,0:T(8,128)(2,1)S(1)}, bf16[8,1024]{1,0:T(8,128)(2,1)S(1)}, u32[]{:S(2)}, u32[]{:S(2)}) %collective-permute-start.15) | collective-permute-done | bytes 16416 | tf_op jit(solution)/shard_map/ppermute | solution.py:38
  31.3 0.6 %shard_map.204 = (bf16[2,1024]{1,0:T(2,128)(2,1)S(1)}, f32[8,512]{1,0:T(8,128)S(1)}) custom-call(f32[8,1024]{1,0:T(8,128)S(1)} %get-tuple-element.41.refs_0_, bf16[8,1024]{1,0:T(8,128)(2,1)S(1)} %collective-permute-done.13.refs_1_, bf16[8,1024]{1,0:T(8,128)(2,1)S(1)} %collective-permute-done.14.refs_2_, bf16[8,1024]{1,0:T(8,128)(2,1)S(1)} %collective-permute-done.15.refs_3_, ...), custom_call_target="tpu_custom_call" | custom-call | flops 524288 | bytes 65536 | tf_op jit(solution)/shard_map/pallas_call | solution.py:26
  31.9 1.8 %collective-permute-start.19 = (bf16[2,1024]{1,0:T(2,128)(2,1)S(1)}, bf16[2,1024]{1,0:T(2,128)(2,1)S(1)}, u32[]{:S(2)}, u32[]{:S(2)}) collective-permute-start(bf16[2,1024]{1,0:T(2,128)(2,1)S(1)} %get-tuple-element.45.refs_0_), channel_id=1, source_target_pairs={{0,5},{1,4},{2,7},{3,6},{4,1},{5,0},{6,3},{7,2},{8,13},{9,12},{10,... | collective-permute-start | bytes 12296 | tf_op jit(solution)/shard_map/ppermute | solution.py:38
  33.7 2.1 %collective-permute-start.20 = (bf16[2,1024]{1,0:T(2,128)(2,1)S(1)}, bf16[2,1024]{1,0:T(2,128)(2,1)S(1)}, u32[]{:S(2)}, u32[]{:S(2)}) collective-permute-start(bf16[2,1024]{1,0:T(2,128)(2,1)S(1)} %get-tuple-element.45.refs_0_), channel_id=1, source_target_pairs={{0,7},{1,6},{2,5},{3,4},{4,3},{5,2},{6,1},{7,0},{8,15},{9,14},{10,... | collective-permute-start | bytes 12296 | tf_op jit(solution)/shard_map/ppermute | solution.py:38
  35.9 2.6 %collective-permute-done.20.refs_3_ = bf16[2,1024]{1,0:T(2,128)(2,1)S(1)} collective-permute-done((bf16[2,1024]{1,0:T(2,128)(2,1)S(1)}, bf16[2,1024]{1,0:T(2,128)(2,1)S(1)}, u32[]{:S(2)}, u32[]{:S(2)}) %collective-permute-start.20) | collective-permute-done | bytes 4128 | tf_op jit(solution)/shard_map/ppermute | solution.py:38
  38.8 2.1 %collective-permute-start.24 = (bf16[8,512]{1,0:T(8,128)(2,1)S(1)}, bf16[8,512]{1,0:T(8,128)(2,1)S(1)}, u32[]{:S(2)}, u32[]{:S(2)}) collective-permute-start(bf16[8,512]{1,0:T(8,128)(2,1)S(1)} %shard_map.205.x.after), channel_id=1, source_target_pairs={{0,7},{1,6},{2,5},{3,4},{4,3},{5,2},{6,1},{7,0},{8,15},{9,14},{10,... | collective-permute-start | bytes 24584 | tf_op jit(solution)/shard_map/ppermute | solution.py:38
  40.9 1.9 %collective-permute-start.22 = (bf16[8,512]{1,0:T(8,128)(2,1)S(1)}, bf16[8,512]{1,0:T(8,128)(2,1)S(1)}, u32[]{:S(2)}, u32[]{:S(2)}) collective-permute-start(bf16[8,512]{1,0:T(8,128)(2,1)S(1)} %shard_map.205.x.after), channel_id=1, source_target_pairs={{0,3},{1,2},{2,1},{3,0},{4,7},{5,6},{6,5},{7,4},{8,11},{9,10},{10,... | collective-permute-start | bytes 24584 | tf_op jit(solution)/shard_map/ppermute | solution.py:38
  44.2 0.7 %collective-permute-done.23.x = bf16[8,512]{1,0:T(8,128)(2,1)S(1)} collective-permute-done((bf16[8,512]{1,0:T(8,128)(2,1)S(1)}, bf16[8,512]{1,0:T(8,128)(2,1)S(1)}, u32[]{:S(2)}, u32[]{:S(2)}) %collective-permute-start.23) | collective-permute-done | bytes 8224 | tf_op jit(solution)/shard_map/ppermute | solution.py:38
  45.3 0.7 %shard_map.209 = (bf16[8,704]{1,0:T(8,128)(2,1)S(1)}, f32[4,8,256]{2,1,0:T(8,128)S(1)}) custom-call(bf16[8,512]{1,0:T(8,128)(2,1)S(1)} %collective-permute-done.22.x, f32[1,2048]{1,0:T(1,128)S(1)} %bitcast.31, bf16[704,2048]{1,0:T(8,128)(2,1)S(1)} %bitcast.19, bf16[704,2048]{1,0:T(8,128)(2,1)S(1)} %bitcast.23, f32[2,8,704]{2,1,0:T(8,128)S(1)} %get-tuple-element.51.acc, ...), custom_call_target="tpu_custom_call" | custom-call | flops 23068672 | bytes 65536 | tf_op jit(solution)/shard_map/pallas_call | solution.py:26
  46.7 0.6 %collective-permute-done.25.other = f32[4,8,256]{2,1,0:T(8,128)S(1)} collective-permute-done((f32[4,8,256]{2,1,0:T(8,128)S(1)}, f32[4,8,256]{2,1,0:T(8,128)S(1)}, u32[]{:S(2)}, u32[]{:S(2)}) %collective-permute-start.25) | collective-permute-done | bytes 32800 | tf_op jit(solution)/shard_map/ppermute | solution.py:38
  47.3 0.5 collective-permute-start.26
  47.8 1.4 %collective-permute-start.27 = (bf16[8,256]{1,0:T(8,128)(2,1)S(1)}, bf16[8,256]{1,0:T(8,128)(2,1)S(1)}, u32[]{:S(2)}, u32[]{:S(2)}) collective-permute-start(bf16[8,256]{1,0:T(8,128)(2,1)S(1)} %get-tuple-element.57), channel_id=1, source_target_pairs={{0,5},{1,4},{2,7},{3,6},{4,1},{5,0},{6,3},{7,2},{8,13},{9,12},{10,... | collective-permute-start | bytes 12296 | tf_op jit(solution)/shard_map/ppermute | solution.py:38
  49.2 2.1 %collective-permute-start.28 = (bf16[8,256]{1,0:T(8,128)(2,1)S(1)}, bf16[8,256]{1,0:T(8,128)(2,1)S(1)}, u32[]{:S(2)}, u32[]{:S(2)}) collective-permute-start(bf16[8,256]{1,0:T(8,128)(2,1)S(1)} %get-tuple-element.58), channel_id=1, source_target_pairs={{0,7},{1,6},{2,5},{3,4},{4,3},{5,2},{6,1},{7,0},{8,15},{9,14},{10,... | collective-permute-start | bytes 12296 | tf_op jit(solution)/shard_map/ppermute | solution.py:38
  51.4 1.1 %shard_map.213 = f32[2,4,64,128]{3,2,1,0:T(8,128)} custom-call(f32[8,512]{1,0:T(8,128)S(1)} %get-tuple-element.59.total, f32[2,4,64,128]{3,2,1,0:T(8,128)S(1)} %copy-done.11, f32[8,128]{1,0:T(8,128)S(1)} %shard_map.203.refs_6_.extras), custom_call_target="tpu_custom_call" | custom-call | flops 1000000000 | bytes 65536 | tf_op jit(solution)/shard_map/pallas_call | solution.py:26
  52.5 1.6 %collective-permute-done.28.refs_3_ = bf16[8,256]{1,0:T(8,128)(2,1)S(1)} collective-permute-done((bf16[8,256]{1,0:T(8,128)(2,1)S(1)}, bf16[8,256]{1,0:T(8,128)(2,1)S(1)}, u32[]{:S(2)}, u32[]{:S(2)}) %collective-permute-start.28) | collective-permute-done | bytes 4128 | tf_op jit(solution)/shard_map/ppermute | solution.py:38
  54.1 0.6 %shard_map.212 = bf16[8,256]{1,0:T(8,128)(2,1)} custom-call(bf16[8,512]{1,0:T(8,128)(2,1)S(1)} %shard_map.205.x.after, f32[8,256]{1,0:T(8,128)S(1)} %get-tuple-element.55.refs_0_, bf16[8,256]{1,0:T(8,128)(2,1)S(1)} %collective-permute-done.26.refs_1_, bf16[8,256]{1,0:T(8,128)(2,1)S(1)} %collective-permute-done.27.refs_2_, ...), custom_call_target="tpu_custom_call" | custom-call | bytes 65536 | tf_op jit(solution)/shard_map/pallas_call | solution.py:26
  (84 shorter events, 7.2 us)
Async XLA Ops:
  0.6 1.6 %collective-permute-start = (bf16[8,256]{1,0:T(8,128)(2,1)}, bf16[8,256]{1,0:T(8,128)(2,1)S(1)}, u32[]{:S(2)}, u32[]{:S(2)}) collective-permute-start(bf16[8,256]{1,0:T(8,128)(2,1)} %x.1), channel_id=1, source_target_pairs={{0,1},{1,0},{2,3},{3,2},{4,5},{5,4},{6,7},{7,6},{8,9},{9,8},{10,11... | collective-permute-start | bytes 12296 | tf_op jit(solution)/shard_map/ppermute | solution.py:38
  2.2 5.4 %copy-start = (bf16[2048,704]{0,1:T(8,128)(2,1)S(1)}, bf16[2048,704]{0,1:T(8,128)(2,1)}, u32[]{:S(2)}) copy-start(bf16[2048,704]{0,1:T(8,128)(2,1)} %param.23) | copy-start | bytes 8650756
  2.2 5.4 %copy-start.1 = (bf16[2048,704]{0,1:T(8,128)(2,1)S(1)}, bf16[2048,704]{0,1:T(8,128)(2,1)}, u32[]{:S(2)}) copy-start(bf16[2048,704]{0,1:T(8,128)(2,1)} %param.24) | copy-start | bytes 8650756
  2.3 6.1 %collective-permute-start.3 = (bf16[8,512]{1,0:T(8,128)(2,1)S(1)}, bf16[8,512]{1,0:T(8,128)(2,1)S(1)}, u32[]{:S(2)}, u32[]{:S(2)}) collective-permute-start(bf16[8,512]{1,0:T(8,128)(2,1)S(1)} %shard_map.196.x), channel_id=1, source_target_pairs={{0,7},{1,6},{2,5},{3,4},{4,3},{5,2},{6,1},{7,0},{8,15},{9,14},{10,... | collective-permute-start | bytes 24584 | tf_op jit(solution)/shard_map/ppermute | solution.py:38
  7.0 4.0 %collective-permute-start.2 = (bf16[8,512]{1,0:T(8,128)(2,1)S(1)}, bf16[8,512]{1,0:T(8,128)(2,1)S(1)}, u32[]{:S(2)}, u32[]{:S(2)}) collective-permute-start(bf16[8,512]{1,0:T(8,128)(2,1)S(1)} %shard_map.196.x), channel_id=1, source_target_pairs={{0,5},{1,4},{2,7},{3,6},{4,1},{5,0},{6,3},{7,2},{8,13},{9,12},{10,... | collective-permute-start | bytes 24584 | tf_op jit(solution)/shard_map/ppermute | solution.py:38
  7.0 4.4 %collective-permute-start.1 = (bf16[8,512]{1,0:T(8,128)(2,1)S(1)}, bf16[8,512]{1,0:T(8,128)(2,1)S(1)}, u32[]{:S(2)}, u32[]{:S(2)}) collective-permute-start(bf16[8,512]{1,0:T(8,128)(2,1)S(1)} %shard_map.196.x), channel_id=1, source_target_pairs={{0,3},{1,2},{2,1},{3,0},{4,7},{5,6},{6,5},{7,4},{8,11},{9,10},{10,... | collective-permute-start | bytes 24584 | tf_op jit(solution)/shard_map/ppermute | solution.py:38
  11.5 5.5 %copy-start.10 = (bf16[512,256]{1,0:T(8,128)(2,1)S(1)}, bf16[512,256]{1,0:T(8,128)(2,1)}, u32[]{:S(2)}) copy-start(bf16[512,256]{1,0:T(8,128)(2,1)} %refs_2_.1) | copy-start | bytes 786436
  12.4 4.6 %collective-permute-start.4 = (bf16[8,512]{1,0:T(8,128)(2,1)S(1)}, bf16[8,512]{1,0:T(8,128)(2,1)S(1)}, u32[]{:S(2)}, u32[]{:S(2)}) collective-permute-start(bf16[8,512]{1,0:T(8,128)(2,1)S(1)} %get-tuple-element.38), channel_id=1, source_target_pairs={{0,3},{1,2},{2,1},{3,0},{4,7},{5,6},{6,5},{7,4},{8,11},{9,10},{10,... | collective-permute-start | bytes 24584 | tf_op jit(solution)/shard_map/ppermute | solution.py:38
  12.4 4.8 %collective-permute-start.5 = (bf16[8,512]{1,0:T(8,128)(2,1)S(1)}, bf16[8,512]{1,0:T(8,128)(2,1)S(1)}, u32[]{:S(2)}, u32[]{:S(2)}) collective-permute-start(bf16[8,512]{1,0:T(8,128)(2,1)S(1)} %get-tuple-element.39), channel_id=1, source_target_pairs={{0,5},{1,4},{2,7},{3,6},{4,1},{5,0},{6,3},{7,2},{8,13},{9,12},{10,... | collective-permute-start | bytes 24584 | tf_op jit(solution)/shard_map/ppermute | solution.py:38
  14.3 4.9 %collective-permute-start.6 = (bf16[8,512]{1,0:T(8,128)(2,1)S(1)}, bf16[8,512]{1,0:T(8,128)(2,1)S(1)}, u32[]{:S(2)}, u32[]{:S(2)}) collective-permute-start(bf16[8,512]{1,0:T(8,128)(2,1)S(1)} %get-tuple-element.40), channel_id=1, source_target_pairs={{0,7},{1,6},{2,5},{3,4},{4,3},{5,2},{6,1},{7,0},{8,15},{9,14},{10,... | collective-permute-start | bytes 24584 | tf_op jit(solution)/shard_map/ppermute | solution.py:38
  16.5 6.6 %collective-permute-start.11 = (bf16[512,512]{1,0:T(8,128)(2,1)S(1)}, bf16[512,512]{1,0:T(8,128)(2,1)S(1)}, u32[]{:S(2)}, u32[]{:S(2)}) collective-permute-start(bf16[512,512]{1,0:T(8,128)(2,1)S(1)} %copy-done.6), channel_id=1, source_target_pairs={{0,1},{1,0},{2,3},{3,2},{4,5},{5,4},{6,7},{7,6},{8,9},{9,8},{10,11... | collective-permute-start | bytes 1572872 | tf_op jit(solution)/shard_map/ppermute | solution.py:38
  16.7 6.4 %collective-permute-start.12 = (bf16[512,512]{1,0:T(8,128)(2,1)S(1)}, bf16[512,512]{1,0:T(8,128)(2,1)S(1)}, u32[]{:S(2)}, u32[]{:S(2)}) collective-permute-start(bf16[512,512]{1,0:T(8,128)(2,1)S(1)} %copy-done.7), channel_id=1, source_target_pairs={{0,1},{1,0},{2,3},{3,2},{4,5},{5,4},{6,7},{7,6},{8,9},{9,8},{10,11... | collective-permute-start | bytes 1572872 | tf_op jit(solution)/shard_map/ppermute | solution.py:38
  17.0 3.8 %collective-permute-start.10 = (bf16[512,256]{1,0:T(8,128)(2,1)S(1)}, bf16[512,256]{1,0:T(8,128)(2,1)S(1)}, u32[]{:S(2)}, u32[]{:S(2)}) collective-permute-start(bf16[512,256]{1,0:T(8,128)(2,1)S(1)} %copy-done.10), channel_id=1, source_target_pairs={{0,1},{1,0},{2,3},{3,2},{4,5},{5,4},{6,7},{7,6},{8,9},{9,8},{10,11... | collective-permute-start | bytes 786440 | tf_op jit(solution)/shard_map/ppermute | solution.py:38
  19.3 1.2 %collective-permute-start.7 = (f32[8,512]{1,0:T(8,128)S(1)}, f32[8,512]{1,0:T(8,128)S(1)}, u32[]{:S(2)}, u32[]{:S(2)}) collective-permute-start(f32[8,512]{1,0:T(8,128)S(1)} %shard_map.201.mine), channel_id=1, source_target_pairs={{0,1},{1,0},{2,3},{3,2},{4,5},{5,4},{6,7},{7,6},{8,9},{9,8},{10,11... | collective-permute-start | bytes 49160 | tf_op jit(solution)/shard_map/ppermute | solution.py:38
  20.2 1.5 %collective-permute-start.8 = (bf16[512,256]{1,0:T(8,128)(2,1)S(1)}, bf16[512,256]{1,0:T(8,128)(2,1)S(1)}, u32[]{:S(2)}, u32[]{:S(2)}) collective-permute-start(bf16[512,256]{1,0:T(8,128)(2,1)S(1)} %copy-done.8), channel_id=1, source_target_pairs={{0,1},{1,0},{2,3},{3,2},{4,5},{5,4},{6,7},{7,6},{8,9},{9,8},{10,11... | collective-permute-start | bytes 786440 | tf_op jit(solution)/shard_map/ppermute | solution.py:38
  20.5 15.3 %collective-permute-start.21 = (bf16[512,512]{1,0:T(8,128)(2,1)S(1)}, bf16[512,512]{1,0:T(8,128)(2,1)S(1)}, u32[]{:S(2)}, u32[]{:S(2)}) collective-permute-start(bf16[512,512]{1,0:T(8,128)(2,1)S(1)} %copy-done.17), channel_id=1, source_target_pairs={{0,1},{1,0},{2,3},{3,2},{4,5},{5,4},{6,7},{7,6},{8,9},{9,8},{10,11... | collective-permute-start | bytes 1572872 | tf_op jit(solution)/shard_map/ppermute | solution.py:38
  20.8 2.0 %collective-permute-start.9 = (bf16[512,256]{1,0:T(8,128)(2,1)S(1)}, bf16[512,256]{1,0:T(8,128)(2,1)S(1)}, u32[]{:S(2)}, u32[]{:S(2)}) collective-permute-start(bf16[512,256]{1,0:T(8,128)(2,1)S(1)} %copy-done.9), channel_id=1, source_target_pairs={{0,1},{1,0},{2,3},{3,2},{4,5},{5,4},{6,7},{7,6},{8,9},{9,8},{10,11... | collective-permute-start | bytes 786440 | tf_op jit(solution)/shard_map/ppermute | solution.py:38
  21.7 6.0 %collective-permute-start.16 = (f32[2,4,64,128]{3,2,1,0:T(8,128)S(1)}, f32[2,4,64,128]{3,2,1,0:T(8,128)S(1)}, u32[]{:S(2)}, u32[]{:S(2)}) collective-permute-start(f32[2,4,64,128]{3,2,1,0:T(8,128)S(1)} %copy-done.11), channel_id=1, source_target_pairs={{0,1},{1,0},{2,3},{3,2},{4,5},{5,4},{6,7},{7,6},{8,9},{9,8},{10,11... | collective-permute-start | bytes 786440 | tf_op jit(solution)/shard_map/ppermute | solution.py:38
  22.8 3.5 %collective-permute-start.17 = (f32[8,128]{1,0:T(8,128)S(1)}, f32[8,128]{1,0:T(8,128)S(1)}, u32[]{:S(2)}, u32[]{:S(2)}) collective-permute-start(f32[8,128]{1,0:T(8,128)S(1)} %shard_map.203.refs_6_.extras), channel_id=1, source_target_pairs={{0,1},{1,0},{2,3},{3,2},{4,5},{5,4},{6,7},{7,6},{8,9},{9,8},{10,11... | collective-permute-start | bytes 12296 | tf_op jit(solution)/shard_map/ppermute | solution.py:38
  23.7 4.1 %collective-permute-start.13 = (bf16[8,1024]{1,0:T(8,128)(2,1)S(1)}, bf16[8,1024]{1,0:T(8,128)(2,1)S(1)}, u32[]{:S(2)}, u32[]{:S(2)}) collective-permute-start(bf16[8,1024]{1,0:T(8,128)(2,1)S(1)} %get-tuple-element.42), channel_id=1, source_target_pairs={{0,3},{1,2},{2,1},{3,0},{4,7},{5,6},{6,5},{7,4},{8,11},{9,10},{10,... | collective-permute-start | bytes 49160 | tf_op jit(solution)/shard_map/ppermute | solution.py:38
  23.8 4.1 %collective-permute-start.14 = (bf16[8,1024]{1,0:T(8,128)(2,1)S(1)}, bf16[8,1024]{1,0:T(8,128)(2,1)S(1)}, u32[]{:S(2)}, u32[]{:S(2)}) collective-permute-start(bf16[8,1024]{1,0:T(8,128)(2,1)S(1)} %get-tuple-element.43), channel_id=1, source_target_pairs={{0,5},{1,4},{2,7},{3,6},{4,1},{5,0},{6,3},{7,2},{8,13},{9,12},{10,... | collective-permute-start | bytes 49160 | tf_op jit(solution)/shard_map/ppermute | solution.py:38
  26.4 5.0 %collective-permute-start.15 = (bf16[8,1024]{1,0:T(8,128)(2,1)S(1)}, bf16[8,1024]{1,0:T(8,128)(2,1)S(1)}, u32[]{:S(2)}, u32[]{:S(2)}) collective-permute-start(bf16[8,1024]{1,0:T(8,128)(2,1)S(1)} %get-tuple-element.44), channel_id=1, source_target_pairs={{0,7},{1,6},{2,5},{3,4},{4,3},{5,2},{6,1},{7,0},{8,15},{9,14},{10,... | collective-permute-start | bytes 49160 | tf_op jit(solution)/shard_map/ppermute | solution.py:38
  31.9 3.9 %collective-permute-start.18 = (bf16[2,1024]{1,0:T(2,128)(2,1)S(1)}, bf16[2,1024]{1,0:T(2,128)(2,1)S(1)}, u32[]{:S(2)}, u32[]{:S(2)}) collective-permute-start(bf16[2,1024]{1,0:T(2,128)(2,1)S(1)} %get-tuple-element.45.refs_0_), channel_id=1, source_target_pairs={{0,3},{1,2},{2,1},{3,0},{4,7},{5,6},{6,5},{7,4},{8,11},{9,10},{10,... | collective-permute-start | bytes 12296 | tf_op jit(solution)/shard_map/ppermute | solution.py:38
  31.9 4.0 %collective-permute-start.19 = (bf16[2,1024]{1,0:T(2,128)(2,1)S(1)}, bf16[2,1024]{1,0:T(2,128)(2,1)S(1)}, u32[]{:S(2)}, u32[]{:S(2)}) collective-permute-start(bf16[2,1024]{1,0:T(2,128)(2,1)S(1)} %get-tuple-element.45.refs_0_), channel_id=1, source_target_pairs={{0,5},{1,4},{2,7},{3,6},{4,1},{5,0},{6,3},{7,2},{8,13},{9,12},{10,... | collective-permute-start | bytes 12296 | tf_op jit(solution)/shard_map/ppermute | solution.py:38
  33.7 4.8 %collective-permute-start.20 = (bf16[2,1024]{1,0:T(2,128)(2,1)S(1)}, bf16[2,1024]{1,0:T(2,128)(2,1)S(1)}, u32[]{:S(2)}, u32[]{:S(2)}) collective-permute-start(bf16[2,1024]{1,0:T(2,128)(2,1)S(1)} %get-tuple-element.45.refs_0_), channel_id=1, source_target_pairs={{0,7},{1,6},{2,5},{3,4},{4,3},{5,2},{6,1},{7,0},{8,15},{9,14},{10,... | collective-permute-start | bytes 12296 | tf_op jit(solution)/shard_map/ppermute | solution.py:38
  38.8 4.9 %collective-permute-start.24 = (bf16[8,512]{1,0:T(8,128)(2,1)S(1)}, bf16[8,512]{1,0:T(8,128)(2,1)S(1)}, u32[]{:S(2)}, u32[]{:S(2)}) collective-permute-start(bf16[8,512]{1,0:T(8,128)(2,1)S(1)} %shard_map.205.x.after), channel_id=1, source_target_pairs={{0,7},{1,6},{2,5},{3,4},{4,3},{5,2},{6,1},{7,0},{8,15},{9,14},{10,... | collective-permute-start | bytes 24584 | tf_op jit(solution)/shard_map/ppermute | solution.py:38
  40.9 4.0 %collective-permute-start.23 = (bf16[8,512]{1,0:T(8,128)(2,1)S(1)}, bf16[8,512]{1,0:T(8,128)(2,1)S(1)}, u32[]{:S(2)}, u32[]{:S(2)}) collective-permute-start(bf16[8,512]{1,0:T(8,128)(2,1)S(1)} %shard_map.205.x.after), channel_id=1, source_target_pairs={{0,5},{1,4},{2,7},{3,6},{4,1},{5,0},{6,3},{7,2},{8,13},{9,12},{10,... | collective-permute-start | bytes 24584 | tf_op jit(solution)/shard_map/ppermute | solution.py:38
  40.9 4.4 %collective-permute-start.22 = (bf16[8,512]{1,0:T(8,128)(2,1)S(1)}, bf16[8,512]{1,0:T(8,128)(2,1)S(1)}, u32[]{:S(2)}, u32[]{:S(2)}) collective-permute-start(bf16[8,512]{1,0:T(8,128)(2,1)S(1)} %shard_map.205.x.after), channel_id=1, source_target_pairs={{0,3},{1,2},{2,1},{3,0},{4,7},{5,6},{6,5},{7,4},{8,11},{9,10},{10,... | collective-permute-start | bytes 24584 | tf_op jit(solution)/shard_map/ppermute | solution.py:38
  46.1 1.2 %collective-permute-start.25 = (f32[4,8,256]{2,1,0:T(8,128)S(1)}, f32[4,8,256]{2,1,0:T(8,128)S(1)}, u32[]{:S(2)}, u32[]{:S(2)}) collective-permute-start(f32[4,8,256]{2,1,0:T(8,128)S(1)} %get-tuple-element.54), channel_id=1, source_target_pairs={{0,1},{1,0},{2,3},{3,2},{4,5},{5,4},{6,7},{7,6},{8,9},{9,8},{10,11... | collective-permute-start | bytes 98312 | tf_op jit(solution)/shard_map/ppermute | solution.py:38
  47.3 5.2 %collective-permute-start.26 = (bf16[8,256]{1,0:T(8,128)(2,1)S(1)}, bf16[8,256]{1,0:T(8,128)(2,1)S(1)}, u32[]{:S(2)}, u32[]{:S(2)}) collective-permute-start(bf16[8,256]{1,0:T(8,128)(2,1)S(1)} %get-tuple-element.56), channel_id=1, source_target_pairs={{0,3},{1,2},{2,1},{3,0},{4,7},{5,6},{6,5},{7,4},{8,11},{9,10},{10,... | collective-permute-start | bytes 12296 | tf_op jit(solution)/shard_map/ppermute | solution.py:38
  47.8 4.7 %collective-permute-start.27 = (bf16[8,256]{1,0:T(8,128)(2,1)S(1)}, bf16[8,256]{1,0:T(8,128)(2,1)S(1)}, u32[]{:S(2)}, u32[]{:S(2)}) collective-permute-start(bf16[8,256]{1,0:T(8,128)(2,1)S(1)} %get-tuple-element.57), channel_id=1, source_target_pairs={{0,5},{1,4},{2,7},{3,6},{4,1},{5,0},{6,3},{7,2},{8,13},{9,12},{10,... | collective-permute-start | bytes 12296 | tf_op jit(solution)/shard_map/ppermute | solution.py:38
  49.2 4.8 %collective-permute-start.28 = (bf16[8,256]{1,0:T(8,128)(2,1)S(1)}, bf16[8,256]{1,0:T(8,128)(2,1)S(1)}, u32[]{:S(2)}, u32[]{:S(2)}) collective-permute-start(bf16[8,256]{1,0:T(8,128)(2,1)S(1)} %get-tuple-element.58), channel_id=1, source_target_pairs={{0,7},{1,6},{2,5},{3,4},{4,3},{5,2},{6,1},{7,0},{8,15},{9,14},{10,... | collective-permute-start | bytes 12296 | tf_op jit(solution)/shard_map/ppermute | solution.py:38
  (16 other events, 54.3 us)
where the time goes:
time: 54.8 us; the launch traced here: 54.7 us
  starting transfers between devices  28.5 us (52%)
  waiting for transfers between devices  16 us (29%)
  Pallas kernels  7.98 us (15%)
  local copies, waits for them, and re-layouts  1.36 us (2%)
  between operations  0.79 us (1%)
    ppermute x29, starting transfers between devices, swap(): return lax.ppermute(x, axis, [(j, j ^ shift) for j in range(size)])  28.5 us
    ppermute x29, waiting for transfers between devices, swap(): return lax.ppermute(x, axis, [(j, j ^ shift) for j in range(size)])  16 us
    pallas_call x20, Pallas kernels, call(): pl.pallas_call(kernel, out_shape=outs, in_specs=[vmem] * len(args), out_s...  7.98 us
    unnamed x38, local copies, waits for them, and re-layouts  1.36 us
  transfers between devices with their start and end apart: 29, of which 15 were waited for; matrix products, arithmetic and copies ran while one was open for 0% of the time, Pallas kernels for 10%

commit v1 on v0

--- a/solution.py
+++ b/solution.py
@@ -38,6 +38,25 @@
     return lax.ppermute(x, axis, [(j, j ^ shift) for j in range(size)])
 
 
+def source(slot, kv, n):
+    if n != 4 or slot in (0, 3):
+        return kv ^ slot
+    end = (kv == 0) | (kv == 3)
+    return kv ^ jnp.where(end, 3 - slot, slot)
+
+
+def gather_kv(block, n_kv):
+    got = []
+    for slot in range(1, n_kv):
+        pairs = []
+        for kv in range(n_kv):
+            ends = n_kv == 4 and slot < 3 and kv in (0, 3)
+            start = kv ^ (3 - slot if ends else slot)
+            pairs += [(2 * start + t, 2 * kv + 1 - t) for t in range(2)]
+        got.append(lax.ppermute(block, ("kv", "tp"), pairs))
+    return got
+
+
 def send_kv(blocks, n_kv):
     got = []
     for s in range(1, n_kv):
@@ -67,7 +86,7 @@
     kv = lax.axis_index("kv")
     for piece, s in zip(pieces, order):
         width = piece.shape[1]
-        cols = pl.ds(pl.multiple_of((kv ^ s) * width, width), width)
+        cols = pl.ds(pl.multiple_of(source(s, kv, w_gate.shape[1] // width) * width, width), width)
         wide = piece.astype(f32)
         scaled = (wide * gain[:, cols]).astype(bf16)
         one = dot_t(scaled, w_gate[:, cols])
@@ -108,11 +127,18 @@
     sq_out[...] = jnp.broadcast_to(square, sq_out.shape)
 
 
-def first_kernel(x, gain, w_gate, w_up, acc, sq, w_down, *outs):
+def first_own_kernel(hidden, w_down, out):
+    width = out.shape[1]
+    cols = pl.ds(pl.multiple_of(lax.axis_index("kv") * width, width), width)
+    out[...] = dot(hidden[...], w_down[:, cols])
+
+
+def first_kernel(x, gain, w_gate, w_up, acc, sq, w_down, keep, *outs):
     gate, up, square = add_pieces([x[...]], [1], gain, w_gate, w_up, acc[0], acc[1], sq[:, :1])
     hidden = hidden_of(gate, up, square, w_gate.shape[1])
+    keep[...] = hidden
     kv = lax.axis_index("kv")
-    for s, out in enumerate(outs):
+    for s, out in enumerate(outs, 1):
         width = out.shape[1]
         cols = pl.ds(pl.multiple_of((kv ^ s) * width, width), width)
         out[...] = dot(hidden, w_down[:, cols]).astype(out.dtype)
@@ -126,8 +152,8 @@
     out[...] = total
 
 
-def project_kernel(mine, other, x, gain, *refs):
-    weights, middle, outs, scr = refs[:10], refs[10], refs[11:-1], refs[-1]
+def project_kernel(sizes, mine, other, x, gain, *refs):
+    (one, two, middle, *outs, scr) = refs
     kv = lax.axis_index("kv")
     mid = (x[...].astype(f32) + 0.5 * (mine[...] + other[...])).astype(bf16)
     middle[...] = mid
@@ -140,11 +166,11 @@
     squares = jnp.concatenate(
         [jnp.broadcast_to(part, (wide.shape[0], LANES)) for part in (high, squares - high)], axis=1
     )
-    half = len(weights) // 2
-    for side in range(2):
-        q, k, z, v, o = (dot(scaled, w[...]) for w in weights[side * half:(side + 1) * half])
+    keys, _ = sizes
+    for side, w in enumerate((one, two)):
+        product = dot(scaled, w[...])
         chunk = 0
-        for part in (q, k, z, squares, v, o):
+        for part in (product[:, :3 * keys], squares, product[:, 3 * keys:]):
             for at in range(0, part.shape[1], LANES):
                 down, across = chunk_place(chunk, rows, height, side * width // 2)
                 for j in range(n):
@@ -161,10 +187,23 @@
     return slice(down, down + rows), slice(across, across + LANES)
 
 
-def extras_kernel(amounts, head_gain, out):
+def beside_kernel(*refs):
+    *ins, out = refs
+    at = 0
+    for ref in ins:
+        out[:, at:at + ref.shape[1]] = ref[...]
+        at += ref.shape[1]
+
+
+def states_kernel(old, amounts, head_gain, out):
+    rows, heads, keys, _ = old.shape
+    at = 0
+    for b in range(rows):
+        for h in range(heads):
+            out[at:at + keys] = old[b, h]
+            at += keys
     pieces = [amounts[:, at:at + LANES] for at in range(0, amounts.shape[1], LANES)]
     pieces += [head_gain[:, at:at + LANES] for at in range(0, head_gain.shape[1], LANES)]
-    at = 0
     for piece in pieces:
         out[at:at + piece.shape[0]] = piece
         at += piece.shape[0]
@@ -194,8 +233,9 @@
     return stacked.T
 
 
-def mix_heads(depth, block, old, extras):
-    rows, heads, keys, values = old.shape
+def mix_heads(depth, sizes, block, packed):
+    rows, heads, keys, values = sizes
+    extras = packed[rows * heads * keys:]
     query, key, decay, value, gate = gates_of(depth, block, extras)
     columns = turn(query * decay)
     agree = query * key
@@ -211,32 +251,34 @@
         at = slice(h % 2 * keys, (h % 2 + 1) * keys)
         for b in range(rows):
             column = columns[at, pair * rows + b:pair * rows + b + 1]
-            reads.append(jnp.sum(column * old[b, h], axis=0, keepdims=True))
+            state = packed[(b * heads + h) * keys:(b * heads + h + 1) * keys]
+            reads.append(jnp.sum(column * state, axis=0, keepdims=True))
     readout = jnp.concatenate(reads, axis=0) + jnp.concatenate(both, axis=0) * value
     normed = readout * lax.rsqrt(jnp.mean(readout * readout, axis=1, keepdims=True) + EPSILON)
     return normed * jnp.concatenate(gains, axis=0) * silu(gate)
 
 
-def mix_kernel(depth, *refs):
-    *ins, old, old_other, extras, extras_other, mixed, total = refs
-    rows, heads, _, values = old.shape
+def mix_kernel(depth, sizes, *refs):
+    *ins, packed, packed_other, mixed, total = refs
+    rows, heads, _, values = sizes
     half = ins[0].shape[1] // 2
     mine, theirs = ins[0][:, :half], ins[0][:, half:]
     for ref in ins[1:]:
         mine, theirs = mine + ref[:, half:].astype(f32), theirs + ref[:, :half].astype(f32)
     total[...] = mine
     for side, result in enumerate((
-        mix_heads(depth, mine, old, extras[...]),
-        mix_heads(depth, theirs, old_other, extras_other[...]),
+        mix_heads(depth, sizes, mine, packed),
+        mix_heads(depth, sizes, theirs, packed_other),
     )):
         for h in range(heads):
             at = (side * heads + h) * values
             mixed[:, at:at + values] = result[h * rows:(h + 1) * rows].astype(bf16)
 
 
-def state_kernel(depth, total, old, extras, new):
-    rows, heads, keys, _ = old.shape
-    _, key, decay, value, _ = gates_of(depth, total[...], extras[...])
+def state_kernel(depth, total, packed, new):
+    rows, heads, keys, _ = new.shape
+    states = rows * heads * keys
+    _, key, decay, value, _ = gates_of(depth, total[...], packed[states:])
     half = key.shape[0]
     columns = turn(key, decay)
     for h in range(heads):
@@ -244,7 +286,8 @@
         for b in range(rows):
             i = h // 2 * rows + b
             row = value[h * rows + b:h * rows + b + 1]
-            new[b, h] = columns[at, half + i:half + i + 1] * old[b, h] + columns[at, i:i + 1] * row
+            old = packed[(b * heads + h) * keys:(b * heads + h + 1) * keys]
+            new[b, h] = columns[at, half + i:half + i + 1] * old + columns[at, i:i + 1] * row
 
 
 def after_kernel(*refs):
@@ -316,7 +359,7 @@
     near = call(copy_kernel, shape(stream.shape, bf16), stream, flops=WAIT)
     wide = call(pair_kernel, shape((rows, pair), bf16), near, swap(stream, "tp", n_tp, 1), flops=2 * WAIT)
     wide = call(copy_kernel, shape((rows, pair), bf16), wide, flops=WAIT)
-    others = send_kv([wide] * (n_kv - 1), n_kv)
+    others = gather_kv(wide, n_kv)
     up_flops = 4 * rows * pair * hid
     wg, wu = first_gate.T, first_up.T
 
@@ -330,34 +373,42 @@
         return acc
 
     acc = up(wide, others, g1, wg, wu, first_down)
-    blocks = call(
-        first_kernel, sums((rows, pair)), others[0], g1, wg, wu, *acc, first_down,
+    hidden, *blocks = call(
+        first_kernel, [shape((rows, hid), bf16)] + sums((rows, pair))[1:], others[0], g1, wg, wu, *acc, first_down,
         flops=2 * up_flops, limit=16,
     )
-    weights = (query_weight, key_weight, decay_weight, value_weight, output_gate_weight)
-    lent = lend(weights)
-    extras = call(extras_kernel, shape((heads // 2 * local_rows + heads, LANES)), decay_amounts, gh)
+    wide_weights = call(
+        beside_kernel, shape((pair, 3 * nk + 2 * nv), bf16), query_weight, key_weight, decay_weight,
+        value_weight, output_gate_weight, limit=8,
+    )
+    (lent_weights,) = lend((wide_weights,))
+    packed = call(
+        states_kernel, shape((local_rows * heads * keys + heads // 2 * local_rows + heads, LANES)),
+        old_state, decay_amounts, gh,
+    )
+    arrived = send_kv(blocks, n_kv)
+    own_block = call(first_own_kernel, shape((rows, pair)), hidden, first_down, flops=up_flops, limit=8)
     mine = call(
-        sum_kernel, shape((rows, pair)), blocks[0], *send_kv(blocks[1:], n_kv),
+        sum_kernel, shape((rows, pair)), own_block, *arrived,
         flops=WAIT,
     )
-    old_other, w_other, extras_other = lend((old_state, output_weight, extras))
+    packed_other, w_other = lend((packed, output_weight))
     other = swap(mine, "tp", n_tp, 1)
     total = 2 * (3 * nk + 2 * nv + 2 * LANES)
     dense = (8, total * local_rows // 8)
     middle, *parts = call(
-        project_kernel, [shape((rows, pair), bf16)] + sums(dense),
-        mine, other, wide, gm, *weights, *lent, scratch=[pltpu.VMEM((n_kv,) + dense, f32)],
+        functools.partial(project_kernel, (nk, nv)), [shape((rows, pair), bf16)] + sums(dense),
+        mine, other, wide, gm, wide_weights, lent_weights, scratch=[pltpu.VMEM((n_kv,) + dense, f32)],
         flops=2 * rows * pair * total, limit=8,
     )
     mixed, summed = call(
-        functools.partial(mix_kernel, depth),
+        functools.partial(mix_kernel, depth, old_state.shape),
         [shape((local_rows, 2 * nv), bf16), shape((8, dense[1] // 2))],
-        parts[0], *send_kv(parts[1:], n_kv), old_state, old_other, extras, extras_other,
+        parts[0], *send_kv(parts[1:], n_kv), packed, packed_other,
         flops=8 * old_state.size,
     )
     new_state = call(
-        functools.partial(state_kernel, depth), shape(old_state.shape), summed, old_state, extras,
+        functools.partial(state_kernel, depth), shape(old_state.shape), summed, packed,
         flops=1_000_000_000,
     )
     after = call(
@@ -365,7 +416,7 @@
         middle, output_weight, w_other, scratch=[pltpu.VMEM((n_kv, local_rows, 2 * nv), f32)],
         flops=WAIT,
     )
-    others = send_kv([after] * (n_kv - 1), n_kv)
+    others = gather_kv(after, n_kv)
     wg, wu = second_gate.T, second_up.T
     acc = up(after, others, g2, wg, wu, second_down)
     hidden, theirs = call(

time: 54.8 us -> 54.3 us (level)
  local copies, waits for them, and re-layouts: 1.36 us -> 5.48 us
  waiting for transfers between devices: 16 us -> 12.7 us
  starting transfers between devices: 28.5 us -> 26.8 us
    ppermute x29 -> x18, starting transfers between devices: 28.5 us -> 16.9 us  [swap(): return lax.ppermute(x, axis, [(j, j ^ shift) for j in range(size)])]
    ppermute x0 -> x6, starting transfers between devices: none -> 9.83 us  [gather_kv(): got.append(lax.ppermute(block, ('kv', 'tp'), pairs))]
    ppermute x29 -> x18, waiting for transfers between devices: 16 us -> 10.9 us  [swap(): return lax.ppermute(x, axis, [(j, j ^ shift) for j in range(size)])]
    unnamed x38, local copies, waits for them, and re-layouts: 1.36 us -> 5.48 us
    ppermute x0 -> x6, waiting for transfers between devices: none -> 1.85 us  [gather_kv(): got.append(lax.ppermute(block, ('kv', 'tp'), pairs))]
    pallas_call x20 -> x22, Pallas kernels: 7.98 us -> 8.26 us  [call(): pl.pallas_call(kernel, out_shape=outs, in_specs=[vmem] * len(args), out_s...]
  transfers between devices with their start and end apart: 29 -> 24, of which waited for: 15 -> 12; matrix products, arithmetic and copies ran while one was open for 0% -> 0% of each run, Pallas kernels for 10% -> 12%
where the time goes in v1:
time: 54.3 us; the launch traced here: 54 us
  starting transfers between devices  26.8 us (49%)
  waiting for transfers between devices  12.7 us (23%)
  Pallas kernels  8.26 us (15%)
  local copies, waits for them, and re-layouts  5.48 us (10%)
  between operations  0.76 us (1%)
    ppermute x18, starting transfers between devices, swap(): return lax.ppermute(x, axis, [(j, j ^ shift) for j in range(size)])  16.9 us
    ppermute x18, waiting for transfers between devices, swap(): return lax.ppermute(x, axis, [(j, j ^ shift) for j in range(size)])  10.9 us
    ppermute x6, starting transfers between devices, gather_kv(): got.append(lax.ppermute(block, ('kv', 'tp'), pairs))  9.83 us
    pallas_call x22, Pallas kernels, call(): pl.pallas_call(kernel, out_shape=outs, in_specs=[vmem] * len(args), out_s...  8.26 us
    unnamed x38, local copies, waits for them, and re-layouts  5.48 us
    ppermute x6, waiting for transfers between devices, gather_kv(): got.append(lax.ppermute(block, ('kv', 'tp'), pairs))  1.85 us
  transfers between devices with their start and end apart: 24, of which 12 were waited for; matrix products, arithmetic and copies ran while one was open for 0% of the time, Pallas kernels for 12%

profile of v1, /device:TPU:0, one launch (start us, length us, event | category | flops | bytes accessed | tf_op | source)
XLA Modules:
  0.0 54.0 jit_solution(6649213610748124514)
XLA Ops:
  1.2 1.0 %copy-done.6 = bf16[512,512]{1,0:T(8,128)(2,1)S(1)} copy-done((bf16[512,512]{1,0:T(8,128)(2,1)S(1)}, bf16[512,512]{1,0:T(8,128)(2,1)}, u32[]{:S(2)}) %copy-start.6) | copy-done | bytes 524312
  2.2 1.0 %copy-done.7 = bf16[512,512]{1,0:T(8,128)(2,1)S(1)} copy-done((bf16[512,512]{1,0:T(8,128)(2,1)S(1)}, bf16[512,512]{1,0:T(8,128)(2,1)}, u32[]{:S(2)}) %copy-start.7) | copy-done | bytes 524312
  3.3 0.9 %copy-done.8 = bf16[512,256]{1,0:T(8,128)(2,1)S(1)} copy-done((bf16[512,256]{1,0:T(8,128)(2,1)S(1)}, bf16[512,256]{1,0:T(8,128)(2,1)}, u32[]{:S(2)}) %copy-start.8) | copy-done | bytes 262168
  4.2 0.9 %copy-done.9 = bf16[512,256]{1,0:T(8,128)(2,1)S(1)} copy-done((bf16[512,256]{1,0:T(8,128)(2,1)S(1)}, bf16[512,256]{1,0:T(8,128)(2,1)}, u32[]{:S(2)}) %copy-start.9) | copy-done | bytes 262168
  5.2 0.9 %copy-done.10 = bf16[512,256]{1,0:T(8,128)(2,1)S(1)} copy-done((bf16[512,256]{1,0:T(8,128)(2,1)S(1)}, bf16[512,256]{1,0:T(8,128)(2,1)}, u32[]{:S(2)}) %copy-start.10) | copy-done | bytes 262168
  6.9 4.8 %collective-permute-start.3 = (bf16[8,512]{1,0:T(8,128)(2,1)S(1)}, bf16[8,512]{1,0:T(8,128)(2,1)S(1)}, u32[]{:S(2)}, u32[]{:S(2)}) collective-permute-start(bf16[8,512]{1,0:T(8,128)(2,1)S(1)} %shard_map.196.x), channel_id=1, source_target_pairs={{6,1},{7,0},{4,3},{5,2},{2,5},{3,4},{0,7},{1,6},{14,9},{15,8},{12,... | collective-permute-start | bytes 24584 | tf_op jit(solution)/shard_map/ppermute | solution.py:56
  11.7 1.7 %collective-permute-start.1 = (bf16[8,512]{1,0:T(8,128)(2,1)S(1)}, bf16[8,512]{1,0:T(8,128)(2,1)S(1)}, u32[]{:S(2)}, u32[]{:S(2)}) collective-permute-start(bf16[8,512]{1,0:T(8,128)(2,1)S(1)} %shard_map.196.x), channel_id=1, source_target_pairs={{4,1},{5,0},{0,3},{1,2},{6,5},{7,4},{2,7},{3,6},{12,9},{13,8},{8,1... | collective-permute-start | bytes 24584 | tf_op jit(solution)/shard_map/ppermute | solution.py:56
  15.6 0.8 %shard_map.200 = (bf16[8,704]{1,0:T(8,128)(2,1)S(1)}, bf16[8,512]{1,0:T(8,128)(2,1)S(1)}, bf16[8,512]{1,0:T(8,128)(2,1)S(1)}, bf16[8,512]{1,0:T(8,128)(2,1)S(1)}) custom-call(bf16[8,512]{1,0:T(8,128)(2,1)S(1)} %collective-permute-done.1.x, f32[1,2048]{1,0:T(1,128)S(1)} %bitcast.27, bf16[704,2048]{1,0:T(8,128)(2,1)S(1)} %bitcast.11, ...), custom_call_target="tpu_custom_call" | custom-call | flops 23068672 | bytes 65536 | tf_op jit(solution)/shard_map/pallas_call | solution.py:26
  16.4 0.9 %collective-permute-start.4 = (bf16[8,512]{1,0:T(8,128)(2,1)S(1)}, bf16[8,512]{1,0:T(8,128)(2,1)S(1)}, u32[]{:S(2)}, u32[]{:S(2)}) collective-permute-start(bf16[8,512]{1,0:T(8,128)(2,1)S(1)} %get-tuple-element.38), channel_id=1, source_target_pairs={{0,3},{1,2},{2,1},{3,0},{4,7},{5,6},{6,5},{7,4},{8,11},{9,10},{10,... | collective-permute-start | bytes 24584 | tf_op jit(solution)/shard_map/ppermute | solution.py:38
  17.3 1.3 %collective-permute-start.5 = (bf16[8,512]{1,0:T(8,128)(2,1)S(1)}, bf16[8,512]{1,0:T(8,128)(2,1)S(1)}, u32[]{:S(2)}, u32[]{:S(2)}) collective-permute-start(bf16[8,512]{1,0:T(8,128)(2,1)S(1)} %get-tuple-element.39), channel_id=1, source_target_pairs={{0,5},{1,4},{2,7},{3,6},{4,1},{5,0},{6,3},{7,2},{8,13},{9,12},{10,... | collective-permute-start | bytes 24584 | tf_op jit(solution)/shard_map/ppermute | solution.py:38
  18.6 1.7 %collective-permute-start.6 = (bf16[8,512]{1,0:T(8,128)(2,1)S(1)}, bf16[8,512]{1,0:T(8,128)(2,1)S(1)}, u32[]{:S(2)}, u32[]{:S(2)}) collective-permute-start(bf16[8,512]{1,0:T(8,128)(2,1)S(1)} %get-tuple-element.40), channel_id=1, source_target_pairs={{0,7},{1,6},{2,5},{3,4},{4,3},{5,2},{6,1},{7,0},{8,15},{9,14},{10,... | collective-permute-start | bytes 24584 | tf_op jit(solution)/shard_map/ppermute | solution.py:38
  21.3 2.2 %collective-permute-done.6.refs_3_ = bf16[8,512]{1,0:T(8,128)(2,1)S(1)} collective-permute-done((bf16[8,512]{1,0:T(8,128)(2,1)S(1)}, bf16[8,512]{1,0:T(8,128)(2,1)S(1)}, u32[]{:S(2)}, u32[]{:S(2)}) %collective-permute-start.6) | collective-permute-done | bytes 8224 | tf_op jit(solution)/shard_map/ppermute | solution.py:38
  24.0 0.8 %collective-permute-done.7.other = f32[8,512]{1,0:T(8,128)S(1)} collective-permute-done((f32[8,512]{1,0:T(8,128)S(1)}, f32[8,512]{1,0:T(8,128)S(1)}, u32[]{:S(2)}, u32[]{:S(2)}) %collective-permute-start.7) | collective-permute-done | bytes 16416 | tf_op jit(solution)/shard_map/ppermute | solution.py:38
  24.8 0.6 %shard_map.204 = (bf16[8,512]{1,0:T(8,128)(2,1)S(1)}, f32[8,1024]{1,0:T(8,128)S(1)}, bf16[8,1024]{1,0:T(8,128)(2,1)S(1)}, bf16[8,1024]{1,0:T(8,128)(2,1)S(1)}, bf16[8,1024]{1,0:T(8,128)(2,1)S(1)}) custom-call(f32[8,512]{1,0:T(8,128)S(1)} %shard_map.202.mine, f32[8,512]{1,0:T(8,128)S(1)} %collective-permute-done.7.other, bf16[8,512]{1,0:T(8,128)(2,1)S(1)} %shard_map.196.x, ...), custom_call_target="tpu_custom_call" | custom-call | flops 33554432 | bytes 65536 | tf_op jit(solution)/shard_map/pallas_call | solution.py:26
  25.5 1.7 %collective-permute-start.11 = (bf16[8,1024]{1,0:T(8,128)(2,1)S(1)}, bf16[8,1024]{1,0:T(8,128)(2,1)S(1)}, u32[]{:S(2)}, u32[]{:S(2)}) collective-permute-start(bf16[8,1024]{1,0:T(8,128)(2,1)S(1)} %get-tuple-element.44), channel_id=1, source_target_pairs={{0,7},{1,6},{2,5},{3,4},{4,3},{5,2},{6,1},{7,0},{8,15},{9,14},{10,... | collective-permute-start | bytes 49160 | tf_op jit(solution)/shard_map/ppermute | solution.py:38
  27.2 1.4 %collective-permute-start.9 = (bf16[8,1024]{1,0:T(8,128)(2,1)S(1)}, bf16[8,1024]{1,0:T(8,128)(2,1)S(1)}, u32[]{:S(2)}, u32[]{:S(2)}) collective-permute-start(bf16[8,1024]{1,0:T(8,128)(2,1)S(1)} %get-tuple-element.42), channel_id=1, source_target_pairs={{0,3},{1,2},{2,1},{3,0},{4,7},{5,6},{6,5},{7,4},{8,11},{9,10},{10,... | collective-permute-start | bytes 49160 | tf_op jit(solution)/shard_map/ppermute | solution.py:38
  28.7 0.9 %collective-permute-done.10.refs_2_ = bf16[8,1024]{1,0:T(8,128)(2,1)S(1)} collective-permute-done((bf16[8,1024]{1,0:T(8,128)(2,1)S(1)}, bf16[8,1024]{1,0:T(8,128)(2,1)S(1)}, u32[]{:S(2)}, u32[]{:S(2)}) %collective-permute-start.10) | collective-permute-done | bytes 16416 | tf_op jit(solution)/shard_map/ppermute | solution.py:38
  29.6 1.0 %collective-permute-done.11.refs_3_ = bf16[8,1024]{1,0:T(8,128)(2,1)S(1)} collective-permute-done((bf16[8,1024]{1,0:T(8,128)(2,1)S(1)}, bf16[8,1024]{1,0:T(8,128)(2,1)S(1)}, u32[]{:S(2)}, u32[]{:S(2)}) %collective-permute-start.11) | collective-permute-done | bytes 16416 | tf_op jit(solution)/shard_map/ppermute | solution.py:38
  31.1 1.3 %collective-permute-start.13 = (bf16[2,1024]{1,0:T(2,128)(2,1)S(1)}, bf16[2,1024]{1,0:T(2,128)(2,1)S(1)}, u32[]{:S(2)}, u32[]{:S(2)}) collective-permute-start(bf16[2,1024]{1,0:T(2,128)(2,1)S(1)} %get-tuple-element.45.refs_0_), channel_id=1, source_target_pairs={{0,3},{1,2},{2,1},{3,0},{4,7},{5,6},{6,5},{7,4},{8,11},{9,10},{10,... | collective-permute-start | bytes 12296 | tf_op jit(solution)/shard_map/ppermute | solution.py:38
  32.4 1.2 %collective-permute-start.14 = (bf16[2,1024]{1,0:T(2,128)(2,1)S(1)}, bf16[2,1024]{1,0:T(2,128)(2,1)S(1)}, u32[]{:S(2)}, u32[]{:S(2)}) collective-permute-start(bf16[2,1024]{1,0:T(2,128)(2,1)S(1)} %get-tuple-element.45.refs_0_), channel_id=1, source_target_pairs={{0,5},{1,4},{2,7},{3,6},{4,1},{5,0},{6,3},{7,2},{8,13},{9,12},{10,... | collective-permute-start | bytes 12296 | tf_op jit(solution)/shard_map/ppermute | solution.py:38
  33.7 1.6 %collective-permute-start.15 = (bf16[2,1024]{1,0:T(2,128)(2,1)S(1)}, bf16[2,1024]{1,0:T(2,128)(2,1)S(1)}, u32[]{:S(2)}, u32[]{:S(2)}) collective-permute-start(bf16[2,1024]{1,0:T(2,128)(2,1)S(1)} %get-tuple-element.45.refs_0_), channel_id=1, source_target_pairs={{0,7},{1,6},{2,5},{3,4},{4,3},{5,2},{6,1},{7,0},{8,15},{9,14},{10,... | collective-permute-start | bytes 12296 | tf_op jit(solution)/shard_map/ppermute | solution.py:38
  35.2 1.1 %collective-permute-done.14.refs_2_ = bf16[2,1024]{1,0:T(2,128)(2,1)S(1)} collective-permute-done((bf16[2,1024]{1,0:T(2,128)(2,1)S(1)}, bf16[2,1024]{1,0:T(2,128)(2,1)S(1)}, u32[]{:S(2)}, u32[]{:S(2)}) %collective-permute-start.14) | collective-permute-done | bytes 4128 | tf_op jit(solution)/shard_map/ppermute | solution.py:38
  36.4 2.1 %collective-permute-done.15.refs_3_ = bf16[2,1024]{1,0:T(2,128)(2,1)S(1)} collective-permute-done((bf16[2,1024]{1,0:T(2,128)(2,1)S(1)}, bf16[2,1024]{1,0:T(2,128)(2,1)S(1)}, u32[]{:S(2)}, u32[]{:S(2)}) %collective-permute-start.15) | collective-permute-done | bytes 4128 | tf_op jit(solution)/shard_map/ppermute | solution.py:38
  38.7 1.6 %collective-permute-start.19 = (bf16[8,512]{1,0:T(8,128)(2,1)S(1)}, bf16[8,512]{1,0:T(8,128)(2,1)S(1)}, u32[]{:S(2)}, u32[]{:S(2)}) collective-permute-start(bf16[8,512]{1,0:T(8,128)(2,1)S(1)} %shard_map.207.x.after), channel_id=1, source_target_pairs={{6,1},{7,0},{4,3},{5,2},{2,5},{3,4},{0,7},{1,6},{14,9},{15,8},{12,... | collective-permute-start | bytes 24584 | tf_op jit(solution)/shard_map/ppermute | solution.py:56
  40.3 1.7 %collective-permute-start.17 = (bf16[8,512]{1,0:T(8,128)(2,1)S(1)}, bf16[8,512]{1,0:T(8,128)(2,1)S(1)}, u32[]{:S(2)}, u32[]{:S(2)}) collective-permute-start(bf16[8,512]{1,0:T(8,128)(2,1)S(1)} %shard_map.207.x.after), channel_id=1, source_target_pairs={{4,1},{5,0},{0,3},{1,2},{6,5},{7,4},{2,7},{3,6},{12,9},{13,8},{8,1... | collective-permute-start | bytes 24584 | tf_op jit(solution)/shard_map/ppermute | solution.py:56
  42.6 1.1 %collective-permute-done.19.x = bf16[8,512]{1,0:T(8,128)(2,1)S(1)} collective-permute-done((bf16[8,512]{1,0:T(8,128)(2,1)S(1)}, bf16[8,512]{1,0:T(8,128)(2,1)S(1)}, u32[]{:S(2)}, u32[]{:S(2)}) %collective-permute-start.19) | collective-permute-done | bytes 8224 | tf_op jit(solution)/shard_map/ppermute | solution.py:56
  44.6 0.7 %shard_map.211 = (bf16[8,704]{1,0:T(8,128)(2,1)S(1)}, f32[4,8,256]{2,1,0:T(8,128)S(1)}) custom-call(bf16[8,512]{1,0:T(8,128)(2,1)S(1)} %collective-permute-done.17.x, f32[1,2048]{1,0:T(1,128)S(1)} %bitcast.31, bf16[704,2048]{1,0:T(8,128)(2,1)S(1)} %bitcast.19, bf16[704,2048]{1,0:T(8,128)(2,1)S(1)} %bitcast.23, f32[2,8,704]{2,1,0:T(8,128)S(1)} %get-tuple-element.51.acc, ...), custom_call_target="tpu_custom_call" | custom-call | flops 23068672 | bytes 65536 | tf_op jit(solution)/shard_map/pallas_call | solution.py:26
  45.8 0.8 %collective-permute-done.20.other = f32[4,8,256]{2,1,0:T(8,128)S(1)} collective-permute-done((f32[4,8,256]{2,1,0:T(8,128)S(1)}, f32[4,8,256]{2,1,0:T(8,128)S(1)}, u32[]{:S(2)}, u32[]{:S(2)}) %collective-permute-start.20) | collective-permute-done | bytes 32800 | tf_op jit(solution)/shard_map/ppermute | solution.py:38
  47.1 1.5 %collective-permute-start.22 = (bf16[8,256]{1,0:T(8,128)(2,1)S(1)}, bf16[8,256]{1,0:T(8,128)(2,1)S(1)}, u32[]{:S(2)}, u32[]{:S(2)}) collective-permute-start(bf16[8,256]{1,0:T(8,128)(2,1)S(1)} %get-tuple-element.57), channel_id=1, source_target_pairs={{0,5},{1,4},{2,7},{3,6},{4,1},{5,0},{6,3},{7,2},{8,13},{9,12},{10,... | collective-permute-start | bytes 12296 | tf_op jit(solution)/shard_map/ppermute | solution.py:38
  48.5 1.9 %collective-permute-start.23 = (bf16[8,256]{1,0:T(8,128)(2,1)S(1)}, bf16[8,256]{1,0:T(8,128)(2,1)S(1)}, u32[]{:S(2)}, u32[]{:S(2)}) collective-permute-start(bf16[8,256]{1,0:T(8,128)(2,1)S(1)} %get-tuple-element.58), channel_id=1, source_target_pairs={{0,7},{1,6},{2,5},{3,4},{4,3},{5,2},{6,1},{7,0},{8,15},{9,14},{10,... | collective-permute-start | bytes 12296 | tf_op jit(solution)/shard_map/ppermute | solution.py:38
  50.4 1.1 %shard_map.215 = f32[2,4,64,128]{3,2,1,0:T(8,128)} custom-call(f32[8,512]{1,0:T(8,128)S(1)} %get-tuple-element.59.total, f32[520,128]{1,0:T(8,128)S(1)} %shard_map.205.refs_4_.packed), custom_call_target="tpu_custom_call" | custom-call | flops 1000000000 | bytes 65536 | tf_op jit(solution)/shard_map/pallas_call | solution.py:26
  51.6 1.8 %collective-permute-done.23.refs_3_ = bf16[8,256]{1,0:T(8,128)(2,1)S(1)} collective-permute-done((bf16[8,256]{1,0:T(8,128)(2,1)S(1)}, bf16[8,256]{1,0:T(8,128)(2,1)S(1)}, u32[]{:S(2)}, u32[]{:S(2)}) %collective-permute-start.23) | collective-permute-done | bytes 4128 | tf_op jit(solution)/shard_map/ppermute | solution.py:38
  (76 shorter events, 9.0 us)
Async XLA Ops:
  0.6 6.2 %collective-permute-start = (bf16[8,256]{1,0:T(8,128)(2,1)}, bf16[8,256]{1,0:T(8,128)(2,1)S(1)}, u32[]{:S(2)}, u32[]{:S(2)}) collective-permute-start(bf16[8,256]{1,0:T(8,128)(2,1)} %x.1), channel_id=1, source_target_pairs={{0,1},{1,0},{2,3},{3,2},{4,5},{5,4},{6,7},{7,6},{8,9},{9,8},{10,11... | collective-permute-start | bytes 12296 | tf_op jit(solution)/shard_map/ppermute | solution.py:38
  6.2 18.6 %collective-permute-start.8 = (bf16[512,1792]{1,0:T(8,128)(2,1)S(1)}, bf16[512,1792]{1,0:T(8,128)(2,1)S(1)}, u32[]{:S(2)}, u32[]{:S(2)}) collective-permute-start(bf16[512,1792]{1,0:T(8,128)(2,1)S(1)} %shard_map.203.refs_0_), channel_id=1, source_target_pairs={{0,1},{1,0},{2,3},{3,2},{4,5},{5,4},{6,7},{7,6},{8,9},{9,8},{10,11... | collective-permute-start | bytes 5505032 | tf_op jit(solution)/shard_map/ppermute | solution.py:38
  6.8 6.6 %copy-start = (bf16[2048,704]{0,1:T(8,128)(2,1)S(1)}, bf16[2048,704]{0,1:T(8,128)(2,1)}, u32[]{:S(2)}) copy-start(bf16[2048,704]{0,1:T(8,128)(2,1)} %param.23) | copy-start | bytes 8650756
  6.8 6.6 %copy-start.1 = (bf16[2048,704]{0,1:T(8,128)(2,1)S(1)}, bf16[2048,704]{0,1:T(8,128)(2,1)}, u32[]{:S(2)}) copy-start(bf16[2048,704]{0,1:T(8,128)(2,1)} %param.24) | copy-start | bytes 8650756
  6.8 6.6 %copy-start.4 = (bf16[704,2048]{1,0:T(8,128)(2,1)S(1)}, bf16[704,2048]{1,0:T(8,128)(2,1)}, u32[]{:S(2)}) copy-start(bf16[704,2048]{1,0:T(8,128)(2,1)} %w_down.5) | copy-start | bytes 8650756
  6.9 6.5 %copy-start.12 = (f32[2048]{0:T(1024)S(1)}, f32[2048]{0:T(1024)}, u32[]{:S(2)}) copy-start(f32[2048]{0:T(1024)} %param.22) | copy-start | bytes 24580
  6.9 7.0 %collective-permute-start.3 = (bf16[8,512]{1,0:T(8,128)(2,1)S(1)}, bf16[8,512]{1,0:T(8,128)(2,1)S(1)}, u32[]{:S(2)}, u32[]{:S(2)}) collective-permute-start(bf16[8,512]{1,0:T(8,128)(2,1)S(1)} %shard_map.196.x), channel_id=1, source_target_pairs={{6,1},{7,0},{4,3},{5,2},{2,5},{3,4},{0,7},{1,6},{14,9},{15,8},{12,... | collective-permute-start | bytes 24584 | tf_op jit(solution)/shard_map/ppermute | solution.py:56
  11.7 3.1 %collective-permute-start.2 = (bf16[8,512]{1,0:T(8,128)(2,1)S(1)}, bf16[8,512]{1,0:T(8,128)(2,1)S(1)}, u32[]{:S(2)}, u32[]{:S(2)}) collective-permute-start(bf16[8,512]{1,0:T(8,128)(2,1)S(1)} %shard_map.196.x), channel_id=1, source_target_pairs={{2,1},{3,0},{6,3},{7,2},{0,5},{1,4},{4,7},{5,6},{10,9},{11,8},{14,... | collective-permute-start | bytes 24584 | tf_op jit(solution)/shard_map/ppermute | solution.py:56
  11.7 4.0 %collective-permute-start.1 = (bf16[8,512]{1,0:T(8,128)(2,1)S(1)}, bf16[8,512]{1,0:T(8,128)(2,1)S(1)}, u32[]{:S(2)}, u32[]{:S(2)}) collective-permute-start(bf16[8,512]{1,0:T(8,128)(2,1)S(1)} %shard_map.196.x), channel_id=1, source_target_pairs={{4,1},{5,0},{0,3},{1,2},{6,5},{7,4},{2,7},{3,6},{12,9},{13,8},{8,1... | collective-permute-start | bytes 24584 | tf_op jit(solution)/shard_map/ppermute | solution.py:56
  15.6 4.7 %copy-start.11 = (f32[2,4,64,128]{3,2,1,0:T(8,128)S(1)}, f32[2,4,64,128]{3,2,1,0:T(8,128)}, u32[]{:S(2)}) copy-start(f32[2,4,64,128]{3,2,1,0:T(8,128)} %old.1) | copy-start | bytes 786436
  15.6 4.7 %copy-start.14 = (f32[2,256]{1,0:T(2,128)S(1)}, f32[2,256]{1,0:T(2,128)}, u32[]{:S(2)}) copy-start(f32[2,256]{1,0:T(2,128)} %amounts.1) | copy-start | bytes 6148
  15.6 4.7 %copy-start.15 = (f32[512]{0:T(512)S(1)}, f32[512]{0:T(512)}, u32[]{:S(2)}) copy-start(f32[512]{0:T(512)} %param.32) | copy-start | bytes 6148
  16.4 4.5 %copy-start.17 = (bf16[512,512]{1,0:T(8,128)(2,1)S(1)}, bf16[512,512]{1,0:T(8,128)(2,1)}, u32[]{:S(2)}) copy-start(bf16[512,512]{1,0:T(8,128)(2,1)} %refs_5_.1) | copy-start | bytes 1572868
  16.4 4.5 %collective-permute-start.4 = (bf16[8,512]{1,0:T(8,128)(2,1)S(1)}, bf16[8,512]{1,0:T(8,128)(2,1)S(1)}, u32[]{:S(2)}, u32[]{:S(2)}) collective-permute-start(bf16[8,512]{1,0:T(8,128)(2,1)S(1)} %get-tuple-element.38), channel_id=1, source_target_pairs={{0,3},{1,2},{2,1},{3,0},{4,7},{5,6},{6,5},{7,4},{8,11},{9,10},{10,... | collective-permute-start | bytes 24584 | tf_op jit(solution)/shard_map/ppermute | solution.py:38
  17.3 4.0 %collective-permute-start.5 = (bf16[8,512]{1,0:T(8,128)(2,1)S(1)}, bf16[8,512]{1,0:T(8,128)(2,1)S(1)}, u32[]{:S(2)}, u32[]{:S(2)}) collective-permute-start(bf16[8,512]{1,0:T(8,128)(2,1)S(1)} %get-tuple-element.39), channel_id=1, source_target_pairs={{0,5},{1,4},{2,7},{3,6},{4,1},{5,0},{6,3},{7,2},{8,13},{9,12},{10,... | collective-permute-start | bytes 24584 | tf_op jit(solution)/shard_map/ppermute | solution.py:38
  18.6 4.9 %collective-permute-start.6 = (bf16[8,512]{1,0:T(8,128)(2,1)S(1)}, bf16[8,512]{1,0:T(8,128)(2,1)S(1)}, u32[]{:S(2)}, u32[]{:S(2)}) collective-permute-start(bf16[8,512]{1,0:T(8,128)(2,1)S(1)} %get-tuple-element.40), channel_id=1, source_target_pairs={{0,7},{1,6},{2,5},{3,4},{4,3},{5,2},{6,1},{7,0},{8,15},{9,14},{10,... | collective-permute-start | bytes 24584 | tf_op jit(solution)/shard_map/ppermute | solution.py:38
  20.3 8.4 %collective-permute-start.12 = (f32[520,128]{1,0:T(8,128)S(1)}, f32[520,128]{1,0:T(8,128)S(1)}, u32[]{:S(2)}, u32[]{:S(2)}) collective-permute-start(f32[520,128]{1,0:T(8,128)S(1)} %shard_map.205.refs_4_.packed), channel_id=1, source_target_pairs={{0,1},{1,0},{2,3},{3,2},{4,5},{5,4},{6,7},{7,6},{8,9},{9,8},{10,11... | collective-permute-start | bytes 798728 | tf_op jit(solution)/shard_map/ppermute | solution.py:38
  21.0 14.2 %collective-permute-start.16 = (bf16[512,512]{1,0:T(8,128)(2,1)S(1)}, bf16[512,512]{1,0:T(8,128)(2,1)S(1)}, u32[]{:S(2)}, u32[]{:S(2)}) collective-permute-start(bf16[512,512]{1,0:T(8,128)(2,1)S(1)} %copy-done.17), channel_id=1, source_target_pairs={{0,1},{1,0},{2,3},{3,2},{4,5},{5,4},{6,7},{7,6},{8,9},{9,8},{10,11... | collective-permute-start | bytes 1572872 | tf_op jit(solution)/shard_map/ppermute | solution.py:38
  23.4 1.4 %collective-permute-start.7 = (f32[8,512]{1,0:T(8,128)S(1)}, f32[8,512]{1,0:T(8,128)S(1)}, u32[]{:S(2)}, u32[]{:S(2)}) collective-permute-start(f32[8,512]{1,0:T(8,128)S(1)} %shard_map.202.mine), channel_id=1, source_target_pairs={{0,1},{1,0},{2,3},{3,2},{4,5},{5,4},{6,7},{7,6},{8,9},{9,8},{10,11... | collective-permute-start | bytes 49160 | tf_op jit(solution)/shard_map/ppermute | solution.py:38
  25.4 4.1 %collective-permute-start.10 = (bf16[8,1024]{1,0:T(8,128)(2,1)S(1)}, bf16[8,1024]{1,0:T(8,128)(2,1)S(1)}, u32[]{:S(2)}, u32[]{:S(2)}) collective-permute-start(bf16[8,1024]{1,0:T(8,128)(2,1)S(1)} %get-tuple-element.43), channel_id=1, source_target_pairs={{0,5},{1,4},{2,7},{3,6},{4,1},{5,0},{6,3},{7,2},{8,13},{9,12},{10,... | collective-permute-start | bytes 49160 | tf_op jit(solution)/shard_map/ppermute | solution.py:38
  25.5 5.0 %collective-permute-start.11 = (bf16[8,1024]{1,0:T(8,128)(2,1)S(1)}, bf16[8,1024]{1,0:T(8,128)(2,1)S(1)}, u32[]{:S(2)}, u32[]{:S(2)}) collective-permute-start(bf16[8,1024]{1,0:T(8,128)(2,1)S(1)} %get-tuple-element.44), channel_id=1, source_target_pairs={{0,7},{1,6},{2,5},{3,4},{4,3},{5,2},{6,1},{7,0},{8,15},{9,14},{10,... | collective-permute-start | bytes 49160 | tf_op jit(solution)/shard_map/ppermute | solution.py:38
  27.2 3.3 %collective-permute-start.9 = (bf16[8,1024]{1,0:T(8,128)(2,1)S(1)}, bf16[8,1024]{1,0:T(8,128)(2,1)S(1)}, u32[]{:S(2)}, u32[]{:S(2)}) collective-permute-start(bf16[8,1024]{1,0:T(8,128)(2,1)S(1)} %get-tuple-element.42), channel_id=1, source_target_pairs={{0,3},{1,2},{2,1},{3,0},{4,7},{5,6},{6,5},{7,4},{8,11},{9,10},{10,... | collective-permute-start | bytes 49160 | tf_op jit(solution)/shard_map/ppermute | solution.py:38
  31.1 4.1 %collective-permute-start.13 = (bf16[2,1024]{1,0:T(2,128)(2,1)S(1)}, bf16[2,1024]{1,0:T(2,128)(2,1)S(1)}, u32[]{:S(2)}, u32[]{:S(2)}) collective-permute-start(bf16[2,1024]{1,0:T(2,128)(2,1)S(1)} %get-tuple-element.45.refs_0_), channel_id=1, source_target_pairs={{0,3},{1,2},{2,1},{3,0},{4,7},{5,6},{6,5},{7,4},{8,11},{9,10},{10,... | collective-permute-start | bytes 12296 | tf_op jit(solution)/shard_map/ppermute | solution.py:38
  32.4 3.9 %collective-permute-start.14 = (bf16[2,1024]{1,0:T(2,128)(2,1)S(1)}, bf16[2,1024]{1,0:T(2,128)(2,1)S(1)}, u32[]{:S(2)}, u32[]{:S(2)}) collective-permute-start(bf16[2,1024]{1,0:T(2,128)(2,1)S(1)} %get-tuple-element.45.refs_0_), channel_id=1, source_target_pairs={{0,5},{1,4},{2,7},{3,6},{4,1},{5,0},{6,3},{7,2},{8,13},{9,12},{10,... | collective-permute-start | bytes 12296 | tf_op jit(solution)/shard_map/ppermute | solution.py:38
  33.7 4.8 %collective-permute-start.15 = (bf16[2,1024]{1,0:T(2,128)(2,1)S(1)}, bf16[2,1024]{1,0:T(2,128)(2,1)S(1)}, u32[]{:S(2)}, u32[]{:S(2)}) collective-permute-start(bf16[2,1024]{1,0:T(2,128)(2,1)S(1)} %get-tuple-element.45.refs_0_), channel_id=1, source_target_pairs={{0,7},{1,6},{2,5},{3,4},{4,3},{5,2},{6,1},{7,0},{8,15},{9,14},{10,... | collective-permute-start | bytes 12296 | tf_op jit(solution)/shard_map/ppermute | solution.py:38
  38.7 4.9 %collective-permute-start.19 = (bf16[8,512]{1,0:T(8,128)(2,1)S(1)}, bf16[8,512]{1,0:T(8,128)(2,1)S(1)}, u32[]{:S(2)}, u32[]{:S(2)}) collective-permute-start(bf16[8,512]{1,0:T(8,128)(2,1)S(1)} %shard_map.207.x.after), channel_id=1, source_target_pairs={{6,1},{7,0},{4,3},{5,2},{2,5},{3,4},{0,7},{1,6},{14,9},{15,8},{12,... | collective-permute-start | bytes 24584 | tf_op jit(solution)/shard_map/ppermute | solution.py:56
  40.3 3.8 %collective-permute-start.18 = (bf16[8,512]{1,0:T(8,128)(2,1)S(1)}, bf16[8,512]{1,0:T(8,128)(2,1)S(1)}, u32[]{:S(2)}, u32[]{:S(2)}) collective-permute-start(bf16[8,512]{1,0:T(8,128)(2,1)S(1)} %shard_map.207.x.after), channel_id=1, source_target_pairs={{2,1},{3,0},{6,3},{7,2},{0,5},{1,4},{4,7},{5,6},{10,9},{11,8},{14,... | collective-permute-start | bytes 24584 | tf_op jit(solution)/shard_map/ppermute | solution.py:56
  40.3 4.3 %collective-permute-start.17 = (bf16[8,512]{1,0:T(8,128)(2,1)S(1)}, bf16[8,512]{1,0:T(8,128)(2,1)S(1)}, u32[]{:S(2)}, u32[]{:S(2)}) collective-permute-start(bf16[8,512]{1,0:T(8,128)(2,1)S(1)} %shard_map.207.x.after), channel_id=1, source_target_pairs={{4,1},{5,0},{0,3},{1,2},{6,5},{7,4},{2,7},{3,6},{12,9},{13,8},{8,1... | collective-permute-start | bytes 24584 | tf_op jit(solution)/shard_map/ppermute | solution.py:56
  45.3 1.2 %collective-permute-start.20 = (f32[4,8,256]{2,1,0:T(8,128)S(1)}, f32[4,8,256]{2,1,0:T(8,128)S(1)}, u32[]{:S(2)}, u32[]{:S(2)}) collective-permute-start(f32[4,8,256]{2,1,0:T(8,128)S(1)} %get-tuple-element.54), channel_id=1, source_target_pairs={{0,1},{1,0},{2,3},{3,2},{4,5},{5,4},{6,7},{7,6},{8,9},{9,8},{10,11... | collective-permute-start | bytes 98312 | tf_op jit(solution)/shard_map/ppermute | solution.py:38
  46.6 5.0 %collective-permute-start.21 = (bf16[8,256]{1,0:T(8,128)(2,1)S(1)}, bf16[8,256]{1,0:T(8,128)(2,1)S(1)}, u32[]{:S(2)}, u32[]{:S(2)}) collective-permute-start(bf16[8,256]{1,0:T(8,128)(2,1)S(1)} %get-tuple-element.56), channel_id=1, source_target_pairs={{0,3},{1,2},{2,1},{3,0},{4,7},{5,6},{6,5},{7,4},{8,11},{9,10},{10,... | collective-permute-start | bytes 12296 | tf_op jit(solution)/shard_map/ppermute | solution.py:38
  47.1 4.5 %collective-permute-start.22 = (bf16[8,256]{1,0:T(8,128)(2,1)S(1)}, bf16[8,256]{1,0:T(8,128)(2,1)S(1)}, u32[]{:S(2)}, u32[]{:S(2)}) collective-permute-start(bf16[8,256]{1,0:T(8,128)(2,1)S(1)} %get-tuple-element.57), channel_id=1, source_target_pairs={{0,5},{1,4},{2,7},{3,6},{4,1},{5,0},{6,3},{7,2},{8,13},{9,12},{10,... | collective-permute-start | bytes 12296 | tf_op jit(solution)/shard_map/ppermute | solution.py:38
  48.5 4.8 %collective-permute-start.23 = (bf16[8,256]{1,0:T(8,128)(2,1)S(1)}, bf16[8,256]{1,0:T(8,128)(2,1)S(1)}, u32[]{:S(2)}, u32[]{:S(2)}) collective-permute-start(bf16[8,256]{1,0:T(8,128)(2,1)S(1)} %get-tuple-element.58), channel_id=1, source_target_pairs={{0,7},{1,6},{2,5},{3,4},{4,3},{5,2},{6,1},{7,0},{8,15},{9,14},{10,... | collective-permute-start | bytes 12296 | tf_op jit(solution)/shard_map/ppermute | solution.py:38
  (11 other events, 23.8 us)

commit v2 on v1

--- a/solution.py
+++ b/solution.py
@@ -127,35 +127,40 @@
     sq_out[...] = jnp.broadcast_to(square, sq_out.shape)
 
 
-def first_own_kernel(hidden, w_down, out):
-    width = out.shape[1]
-    cols = pl.ds(pl.multiple_of(lax.axis_index("kv") * width, width), width)
-    out[...] = dot(hidden[...], w_down[:, cols])
-
-
-def first_kernel(x, gain, w_gate, w_up, acc, sq, w_down, keep, *outs):
+def down_block(hidden, w_down, s, width):
+    cols = pl.ds(pl.multiple_of((lax.axis_index("kv") ^ s) * width, width), width)
+    return dot(hidden, w_down[:, cols])
+
+
+def first_kernel(x, gain, w_gate, w_up, acc, sq, w_down, keep, far):
     gate, up, square = add_pieces([x[...]], [1], gain, w_gate, w_up, acc[0], acc[1], sq[:, :1])
     hidden = hidden_of(gate, up, square, w_gate.shape[1])
     keep[...] = hidden
+    far[...] = down_block(hidden, w_down, w_down.shape[1] // far.shape[1] - 1, far.shape[1])
+
+
+def first_rest_kernel(hidden, w_down, out):
+    for s in range(out.shape[0]):
+        out[s] = down_block(hidden[...], w_down, s, out.shape[2])
+
+
+def add_kernel(mine, other, out):
+    out[...] = (mine[...] + other[...]).astype(out.dtype)
+
+
+def add_rest_kernel(mine, other, *outs):
+    for s, out in enumerate(outs):
+        out[...] = (mine[s] + other[s]).astype(out.dtype)
+
+
+def project_kernel(sizes, *refs):
+    n = refs[-1].shape[0]
+    sums, (x, gain, one, two, middle), outs, scr = refs[:n], refs[n:n + 5], refs[n + 5:-1], refs[-1]
+    total = sums[0][...]
+    for ref in sums[1:]:
+        total = total + ref[...].astype(f32)
     kv = lax.axis_index("kv")
-    for s, out in enumerate(outs, 1):
-        width = out.shape[1]
-        cols = pl.ds(pl.multiple_of((kv ^ s) * width, width), width)
-        out[...] = dot(hidden, w_down[:, cols]).astype(out.dtype)
-
-
-def sum_kernel(*refs):
-    *ins, out = refs
-    total = ins[0][...]
-    for ref in ins[1:]:
-        total = total + ref[...].astype(f32)
-    out[...] = total
-
-
-def project_kernel(sizes, mine, other, x, gain, *refs):
-    (one, two, middle, *outs, scr) = refs
-    kv = lax.axis_index("kv")
-    mid = (x[...].astype(f32) + 0.5 * (mine[...] + other[...])).astype(bf16)
+    mid = (x[...].astype(f32) + 0.5 * total).astype(bf16)
     middle[...] = mid
     wide = mid.astype(f32)
     scaled = (wide * gain[...]).astype(bf16)
@@ -213,7 +218,7 @@
     half = block.shape[0] // 2
     qk, zs, value, gate = (block[:, at:at + LANES] for at in range(0, 4 * LANES, LANES))
     rows = half // 2
-    squares = zs[half:half + rows, :1] + zs[half + rows:, :1]
+    squares = zs[half:half + rows] + zs[half + rows:]
     scale = lax.rsqrt(squares / depth + EPSILON)
     scale = jnp.concatenate([scale, scale], axis=0)
     query, key = qk[:half] * scale, qk[half:] * scale
@@ -304,30 +309,33 @@
     after[...] = (middle[...].astype(f32) + (mine + theirs)).astype(bf16)
 
 
-def down_halves(hidden, w_down, sides, out):
-    kv = lax.axis_index("kv")
-    width = out.shape[2]
-    for s, side in enumerate(sides):
-        cols = pl.ds(pl.multiple_of(((kv ^ s) * 2 + side) * width, width), width)
-        out[s] = dot(hidden, w_down[:, cols])
+def half_product(hidden, w_down, s, side, width):
+    tp = lax.axis_index("tp")
+    half = tp if side == 0 else 1 - tp
+    cols = pl.ds(pl.multiple_of(((lax.axis_index("kv") ^ s) * 2 + half) * width, width), width)
+    return dot(hidden, w_down[:, cols])
 
 
 def second_kernel(x, gain, w_gate, w_up, acc, sq, w_down, hidden, theirs):
     gate, up, square = add_pieces([x[...]], [1], gain, w_gate, w_up, acc[0], acc[1], sq[:, :1])
     hid = hidden_of(gate, up, square, w_gate.shape[1])
     hidden[...] = hid
-    tp = lax.axis_index("tp")
-    down_halves(hid, w_down, [1 - tp] + [tp] * (theirs.shape[0] - 1), theirs)
+    width = theirs.shape[1]
+    theirs[...] = half_product(hid, w_down, w_down.shape[1] // (2 * width) - 1, 0, width)
+
+
+def second_rest_kernel(hidden, w_down, theirs):
+    for s in range(theirs.shape[0]):
+        theirs[s] = half_product(hidden[...], w_down, s, 0 if s else 1, theirs.shape[2])
 
 
 def second_mine_kernel(hidden, w_down, mine):
-    tp = lax.axis_index("tp")
-    down_halves(hidden[...], w_down, [tp] + [1 - tp] * (mine.shape[0] - 1), mine)
-
-
-def split_sum_kernel(mine, other, *outs):
-    for s, out in enumerate(outs):
-        out[...] = (mine[s] + other[s]).astype(out.dtype)
+    for s in range(mine.shape[0]):
+        mine[s] = half_product(hidden[...], w_down, s, 1 if s else 0, mine.shape[2])
+
+
+def add_far_kernel(mine, other, out):
+    out[...] = (mine[mine.shape[0] - 1] + other[...]).astype(out.dtype)
 
 
 def last_kernel(after, *refs):
@@ -373,10 +381,18 @@
         return acc
 
     acc = up(wide, others, g1, wg, wu, first_down)
-    hidden, *blocks = call(
-        first_kernel, [shape((rows, hid), bf16)] + sums((rows, pair))[1:], others[0], g1, wg, wu, *acc, first_down,
-        flops=2 * up_flops, limit=16,
-    )
+    hidden, far = call(
+        first_kernel, [shape((rows, hid), bf16), shape((rows, pair))], others[0], g1, wg, wu, *acc,
+        first_down, flops=2 * up_flops, limit=16,
+    )
+    far_other = swap(far, "tp", n_tp, 1)
+    rest = call(
+        first_rest_kernel, shape((n_kv - 1, rows, pair)), hidden, first_down, flops=up_flops,
+        limit=8,
+    )
+    rest_other = swap(rest, "tp", n_tp, 1)
+    far = call(add_kernel, shape((rows, pair), bf16), far, far_other)
+    own_block, *blocks = call(add_rest_kernel, sums((rows, pair))[:-1], rest, rest_other, flops=WAIT)
     wide_weights = call(
         beside_kernel, shape((pair, 3 * nk + 2 * nv), bf16), query_weight, key_weight, decay_weight,
         value_weight, output_gate_weight, limit=8,
@@ -386,19 +402,13 @@
         states_kernel, shape((local_rows * heads * keys + heads // 2 * local_rows + heads, LANES)),
         old_state, decay_amounts, gh,
     )
-    arrived = send_kv(blocks, n_kv)
-    own_block = call(first_own_kernel, shape((rows, pair)), hidden, first_down, flops=up_flops, limit=8)
-    mine = call(
-        sum_kernel, shape((rows, pair)), own_block, *arrived,
-        flops=WAIT,
-    )
+    arrived = send_kv(blocks + [far], n_kv)
     packed_other, w_other = lend((packed, output_weight))
-    other = swap(mine, "tp", n_tp, 1)
     total = 2 * (3 * nk + 2 * nv + 2 * LANES)
     dense = (8, total * local_rows // 8)
     middle, *parts = call(
         functools.partial(project_kernel, (nk, nv)), [shape((rows, pair), bf16)] + sums(dense),
-        mine, other, wide, gm, wide_weights, lent_weights, scratch=[pltpu.VMEM((n_kv,) + dense, f32)],
+        own_block, *arrived, wide, gm, wide_weights, lent_weights, scratch=[pltpu.VMEM((n_kv,) + dense, f32)],
         flops=2 * rows * pair * total, limit=8,
     )
     mixed, summed = call(
@@ -420,15 +430,22 @@
     wg, wu = second_gate.T, second_up.T
     acc = up(after, others, g2, wg, wu, second_down)
     hidden, theirs = call(
-        second_kernel, [shape((rows, hid), bf16), shape((n_kv, rows, own))],
+        second_kernel, [shape((rows, hid), bf16), shape((rows, own))],
         others[0], g2, wg, wu, *acc, second_down, flops=2 * up_flops, limit=16,
     )
-    arrived = swap(theirs, "tp", n_tp, 1)
+    far = swap(theirs, "tp", n_tp, 1)
+    theirs = call(
+        second_rest_kernel, shape((n_kv - 1, rows, own)), hidden, second_down, flops=up_flops,
+        limit=8,
+    )
+    rest = swap(theirs, "tp", n_tp, 1)
     mine = call(
-        second_mine_kernel, shape((n_kv, rows, own)), hidden, second_down,
-        flops=up_flops, limit=12,
-    )
-    blocks = call(split_sum_kernel, sums((rows, own)), mine, arrived)
+        second_mine_kernel, shape((n_kv, rows, own)), hidden, second_down, flops=up_flops,
+        limit=8,
+    )
+    far = call(add_far_kernel, shape((rows, own), bf16), mine, far)
+    own_block, *blocks = call(add_rest_kernel, sums((rows, own))[:-1], mine, rest)
+    blocks = [own_block, *blocks, far]
     mixed_stream = call(last_kernel, shape((rows, own), bf16), after, blocks[0], *send_kv(blocks[1:], n_kv))
     return (mixed_stream, new_state)
 

time: 54.3 us -> 58 us (1.068)
  waiting for transfers between devices: 12.7 us -> 16.6 us
    ppermute x18 -> x20, waiting for transfers between devices: 10.9 us -> 15.1 us  [swap(): return lax.ppermute(x, axis, [(j, j ^ shift) for j in range(size)])]
    ppermute x18 -> x20, starting transfers between devices: 16.9 us -> 16.2 us  [swap(): return lax.ppermute(x, axis, [(j, j ^ shift) for j in range(size)])]
    pallas_call x22 -> x25, Pallas kernels: 8.26 us -> 8.44 us  [call(): pl.pallas_call(kernel, out_shape=outs, in_specs=[vmem] * len(args), out_s...]
  transfers between devices with their start and end apart: 24 -> 26, of which waited for: 12 -> 13; matrix products, arithmetic and copies ran while one was open for 0% -> 0% of each run, Pallas kernels for 12% -> 12%
where the time goes in v2:
time: 58 us; the launch traced here: 57.6 us
  starting transfers between devices  26.3 us (45%)
  waiting for transfers between devices  16.6 us (29%)
  Pallas kernels  8.44 us (15%)
  local copies, waits for them, and re-layouts  5.49 us (9%)
  between operations  0.79 us (1%)
    ppermute x20, starting transfers between devices, swap(): return lax.ppermute(x, axis, [(j, j ^ shift) for j in range(size)])  16.2 us
    ppermute x20, waiting for transfers between devices, swap(): return lax.ppermute(x, axis, [(j, j ^ shift) for j in range(size)])  15.1 us
    ppermute x6, starting transfers between devices, gather_kv(): got.append(lax.ppermute(block, ('kv', 'tp'), pairs))  10.2 us
    pallas_call x25, Pallas kernels, call(): pl.pallas_call(kernel, out_shape=outs, in_specs=[vmem] * len(args), out_s...  8.44 us
    unnamed x38, local copies, waits for them, and re-layouts  5.49 us
    ppermute x6, waiting for transfers between devices, gather_kv(): got.append(lax.ppermute(block, ('kv', 'tp'), pairs))  1.51 us
  transfers between devices with their start and end apart: 26, of which 13 were waited for; matrix products, arithmetic and copies ran while one was open for 0% of the time, Pallas kernels for 12%

profile of v2, /device:TPU:0, one launch (start us, length us, event | category | flops | bytes accessed | tf_op | source)
XLA Modules:
  0.0 57.6 jit_solution(13516388506244025288)
XLA Ops:
  0.6 0.6 collective-permute-start
  1.2 1.0 %copy-done.6 = bf16[512,512]{1,0:T(8,128)(2,1)S(1)} copy-done((bf16[512,512]{1,0:T(8,128)(2,1)S(1)}, bf16[512,512]{1,0:T(8,128)(2,1)}, u32[]{:S(2)}) %copy-start.6) | copy-done | bytes 524312
  2.2 1.0 %copy-done.7 = bf16[512,512]{1,0:T(8,128)(2,1)S(1)} copy-done((bf16[512,512]{1,0:T(8,128)(2,1)S(1)}, bf16[512,512]{1,0:T(8,128)(2,1)}, u32[]{:S(2)}) %copy-start.7) | copy-done | bytes 524312
  3.3 0.9 %copy-done.8 = bf16[512,256]{1,0:T(8,128)(2,1)S(1)} copy-done((bf16[512,256]{1,0:T(8,128)(2,1)S(1)}, bf16[512,256]{1,0:T(8,128)(2,1)}, u32[]{:S(2)}) %copy-start.8) | copy-done | bytes 262168
  4.2 0.9 %copy-done.9 = bf16[512,256]{1,0:T(8,128)(2,1)S(1)} copy-done((bf16[512,256]{1,0:T(8,128)(2,1)S(1)}, bf16[512,256]{1,0:T(8,128)(2,1)}, u32[]{:S(2)}) %copy-start.9) | copy-done | bytes 262168
  5.2 0.9 %copy-done.10 = bf16[512,256]{1,0:T(8,128)(2,1)S(1)} copy-done((bf16[512,256]{1,0:T(8,128)(2,1)S(1)}, bf16[512,256]{1,0:T(8,128)(2,1)}, u32[]{:S(2)}) %copy-start.10) | copy-done | bytes 262168
  6.9 4.8 %collective-permute-start.3 = (bf16[8,512]{1,0:T(8,128)(2,1)S(1)}, bf16[8,512]{1,0:T(8,128)(2,1)S(1)}, u32[]{:S(2)}, u32[]{:S(2)}) collective-permute-start(bf16[8,512]{1,0:T(8,128)(2,1)S(1)} %shard_map.196.x.refs_4_), channel_id=1, source_target_pairs={{6,1},{7,0},{4,3},{5,2},{2,5},{3,4},{0,7},{1,6},{14,9},{15,8},{12,... | collective-permute-start | bytes 24584 | tf_op jit(solution)/shard_map/ppermute | solution.py:56
  11.7 1.7 %collective-permute-start.1 = (bf16[8,512]{1,0:T(8,128)(2,1)S(1)}, bf16[8,512]{1,0:T(8,128)(2,1)S(1)}, u32[]{:S(2)}, u32[]{:S(2)}) collective-permute-start(bf16[8,512]{1,0:T(8,128)(2,1)S(1)} %shard_map.196.x.refs_4_), channel_id=1, source_target_pairs={{4,1},{5,0},{0,3},{1,2},{6,5},{7,4},{2,7},{3,6},{12,9},{13,8},{8,1... | collective-permute-start | bytes 24584 | tf_op jit(solution)/shard_map/ppermute | solution.py:56
  13.4 0.5 shard_map.197
  15.6 0.6 %shard_map.200 = (bf16[8,704]{1,0:T(8,128)(2,1)S(1)}, f32[8,512]{1,0:T(8,128)S(1)}) custom-call(bf16[8,512]{1,0:T(8,128)(2,1)S(1)} %collective-permute-done.1.x, f32[1,2048]{1,0:T(1,128)S(1)} %bitcast.27, bf16[704,2048]{1,0:T(8,128)(2,1)S(1)} %bitcast.11, bf16[704,2048]{1,0:T(8,128)(2,1)S(1)} %bitcast.15, f32[2,8,704]{2,1,0:T(8,128)S(1)} %get-tuple-element.35.acc, ...), custom_call_target="tpu_custom_call" | custom-call | flops 23068672 | bytes 65536 | tf_op jit(solution)/shard_map/pallas_call | solution.py:26
  18.0 1.9 %collective-permute-start.8 = (bf16[8,512]{1,0:T(8,128)(2,1)S(1)}, bf16[8,512]{1,0:T(8,128)(2,1)S(1)}, u32[]{:S(2)}, u32[]{:S(2)}) collective-permute-start(bf16[8,512]{1,0:T(8,128)(2,1)S(1)} %shard_map.203), channel_id=1, source_target_pairs={{0,7},{1,6},{2,5},{3,4},{4,3},{5,2},{6,1},{7,0},{8,15},{9,14},{10,... | collective-permute-start | bytes 24584 | tf_op jit(solution)/shard_map/ppermute | solution.py:38
  20.0 2.9 %collective-permute-done.8.refs_3_ = bf16[8,512]{1,0:T(8,128)(2,1)S(1)} collective-permute-done((bf16[8,512]{1,0:T(8,128)(2,1)S(1)}, bf16[8,512]{1,0:T(8,128)(2,1)S(1)}, u32[]{:S(2)}, u32[]{:S(2)}) %collective-permute-start.8) | collective-permute-done | bytes 8224 | tf_op jit(solution)/shard_map/ppermute | solution.py:38
  23.1 3.8 %collective-permute-done.6.refs_2_ = bf16[8,512]{1,0:T(8,128)(2,1)S(1)} collective-permute-done((bf16[8,512]{1,0:T(8,128)(2,1)S(1)}, bf16[8,512]{1,0:T(8,128)(2,1)S(1)}, u32[]{:S(2)}, u32[]{:S(2)}) %collective-permute-start.6) | collective-permute-done | bytes 8224 | tf_op jit(solution)/shard_map/ppermute | solution.py:38
  26.9 0.6 %shard_map.205 = (bf16[8,512]{1,0:T(8,128)(2,1)S(1)}, f32[8,1024]{1,0:T(8,128)S(1)}, bf16[8,1024]{1,0:T(8,128)(2,1)S(1)}, bf16[8,1024]{1,0:T(8,128)(2,1)S(1)}, bf16[8,1024]{1,0:T(8,128)(2,1)S(1)}) custom-call(f32[8,512]{1,0:T(8,128)S(1)} %get-tuple-element.38.refs_0_, bf16[8,512]{1,0:T(8,128)(2,1)S(1)} %collective-permute-done.5.refs_1_, ...), custom_call_target="tpu_custom_call" | custom-call | flops 33554432 | bytes 65536 | tf_op jit(solution)/shard_map/pallas_call | solution.py:26
  27.6 2.4 %collective-permute-start.11 = (bf16[8,1024]{1,0:T(8,128)(2,1)S(1)}, bf16[8,1024]{1,0:T(8,128)(2,1)S(1)}, u32[]{:S(2)}, u32[]{:S(2)}) collective-permute-start(bf16[8,1024]{1,0:T(8,128)(2,1)S(1)} %get-tuple-element.44), channel_id=1, source_target_pairs={{0,5},{1,4},{2,7},{3,6},{4,1},{5,0},{6,3},{7,2},{8,13},{9,12},{10,... | collective-permute-start | bytes 49160 | tf_op jit(solution)/shard_map/ppermute | solution.py:38
  30.1 1.6 %collective-permute-start.12 = (bf16[8,1024]{1,0:T(8,128)(2,1)S(1)}, bf16[8,1024]{1,0:T(8,128)(2,1)S(1)}, u32[]{:S(2)}, u32[]{:S(2)}) collective-permute-start(bf16[8,1024]{1,0:T(8,128)(2,1)S(1)} %get-tuple-element.45), channel_id=1, source_target_pairs={{0,7},{1,6},{2,5},{3,4},{4,3},{5,2},{6,1},{7,0},{8,15},{9,14},{10,... | collective-permute-start | bytes 49160 | tf_op jit(solution)/shard_map/ppermute | solution.py:38
  31.7 3.3 %collective-permute-done.12.refs_3_ = bf16[8,1024]{1,0:T(8,128)(2,1)S(1)} collective-permute-done((bf16[8,1024]{1,0:T(8,128)(2,1)S(1)}, bf16[8,1024]{1,0:T(8,128)(2,1)S(1)}, u32[]{:S(2)}, u32[]{:S(2)}) %collective-permute-start.12) | collective-permute-done | bytes 16416 | tf_op jit(solution)/shard_map/ppermute | solution.py:38
  35.0 0.5 shard_map.207
  35.6 1.9 %collective-permute-start.15 = (bf16[2,1024]{1,0:T(2,128)(2,1)S(1)}, bf16[2,1024]{1,0:T(2,128)(2,1)S(1)}, u32[]{:S(2)}, u32[]{:S(2)}) collective-permute-start(bf16[2,1024]{1,0:T(2,128)(2,1)S(1)} %get-tuple-element.46.refs_0_), channel_id=1, source_target_pairs={{0,5},{1,4},{2,7},{3,6},{4,1},{5,0},{6,3},{7,2},{8,13},{9,12},{10,... | collective-permute-start | bytes 12296 | tf_op jit(solution)/shard_map/ppermute | solution.py:38
  37.5 1.9 %collective-permute-start.16 = (bf16[2,1024]{1,0:T(2,128)(2,1)S(1)}, bf16[2,1024]{1,0:T(2,128)(2,1)S(1)}, u32[]{:S(2)}, u32[]{:S(2)}) collective-permute-start(bf16[2,1024]{1,0:T(2,128)(2,1)S(1)} %get-tuple-element.46.refs_0_), channel_id=1, source_target_pairs={{0,7},{1,6},{2,5},{3,4},{4,3},{5,2},{6,1},{7,0},{8,15},{9,14},{10,... | collective-permute-start | bytes 12296 | tf_op jit(solution)/shard_map/ppermute | solution.py:38
  39.6 2.8 %collective-permute-done.16.refs_3_ = bf16[2,1024]{1,0:T(2,128)(2,1)S(1)} collective-permute-done((bf16[2,1024]{1,0:T(2,128)(2,1)S(1)}, bf16[2,1024]{1,0:T(2,128)(2,1)S(1)}, u32[]{:S(2)}, u32[]{:S(2)}) %collective-permute-start.16) | collective-permute-done | bytes 4128 | tf_op jit(solution)/shard_map/ppermute | solution.py:38
  42.6 1.9 %collective-permute-start.20 = (bf16[8,512]{1,0:T(8,128)(2,1)S(1)}, bf16[8,512]{1,0:T(8,128)(2,1)S(1)}, u32[]{:S(2)}, u32[]{:S(2)}) collective-permute-start(bf16[8,512]{1,0:T(8,128)(2,1)S(1)} %shard_map.208.x.after), channel_id=1, source_target_pairs={{6,1},{7,0},{4,3},{5,2},{2,5},{3,4},{0,7},{1,6},{14,9},{15,8},{12,... | collective-permute-start | bytes 24584 | tf_op jit(solution)/shard_map/ppermute | solution.py:56
  44.5 1.7 %collective-permute-start.18 = (bf16[8,512]{1,0:T(8,128)(2,1)S(1)}, bf16[8,512]{1,0:T(8,128)(2,1)S(1)}, u32[]{:S(2)}, u32[]{:S(2)}) collective-permute-start(bf16[8,512]{1,0:T(8,128)(2,1)S(1)} %shard_map.208.x.after), channel_id=1, source_target_pairs={{4,1},{5,0},{0,3},{1,2},{6,5},{7,4},{2,7},{3,6},{12,9},{13,8},{8,1... | collective-permute-start | bytes 24584 | tf_op jit(solution)/shard_map/ppermute | solution.py:56
  46.8 0.7 %collective-permute-done.20.x = bf16[8,512]{1,0:T(8,128)(2,1)S(1)} collective-permute-done((bf16[8,512]{1,0:T(8,128)(2,1)S(1)}, bf16[8,512]{1,0:T(8,128)(2,1)S(1)}, u32[]{:S(2)}, u32[]{:S(2)}) %collective-permute-start.20) | collective-permute-done | bytes 8224 | tf_op jit(solution)/shard_map/ppermute | solution.py:56
  48.0 0.5 shard_map.211
  48.5 0.7 %shard_map.212 = (bf16[8,704]{1,0:T(8,128)(2,1)S(1)}, f32[8,256]{1,0:T(8,128)S(1)}) custom-call(bf16[8,512]{1,0:T(8,128)(2,1)S(1)} %collective-permute-done.18.x, f32[1,2048]{1,0:T(1,128)S(1)} %bitcast.31, bf16[704,2048]{1,0:T(8,128)(2,1)S(1)} %bitcast.19, bf16[704,2048]{1,0:T(8,128)(2,1)S(1)} %bitcast.23, f32[2,8,704]{2,1,0:T(8,128)S(1)} %get-tuple-element.52.acc, ...), custom_call_target="tpu_custom_call" | custom-call | flops 23068672 | bytes 65536 | tf_op jit(solution)/shard_map/pallas_call | solution.py:26
  50.3 0.7 %collective-permute-done.24.other = f32[8,256]{1,0:T(8,128)S(1)} collective-permute-done((f32[8,256]{1,0:T(8,128)S(1)}, f32[8,256]{1,0:T(8,128)S(1)}, u32[]{:S(2)}, u32[]{:S(2)}) %collective-permute-start.24) | collective-permute-done | bytes 8224 | tf_op jit(solution)/shard_map/ppermute | solution.py:38
  51.0 1.9 %collective-permute-start.25 = (bf16[8,256]{1,0:T(8,128)(2,1)S(1)}, bf16[8,256]{1,0:T(8,128)(2,1)S(1)}, u32[]{:S(2)}, u32[]{:S(2)}) collective-permute-start(bf16[8,256]{1,0:T(8,128)(2,1)S(1)} %shard_map.216), channel_id=1, source_target_pairs={{0,7},{1,6},{2,5},{3,4},{4,3},{5,2},{6,1},{7,0},{8,15},{9,14},{10,... | collective-permute-start | bytes 12296 | tf_op jit(solution)/shard_map/ppermute | solution.py:38
  53.0 2.0 %collective-permute-start.23 = (bf16[8,256]{1,0:T(8,128)(2,1)S(1)}, bf16[8,256]{1,0:T(8,128)(2,1)S(1)}, u32[]{:S(2)}, u32[]{:S(2)}) collective-permute-start(bf16[8,256]{1,0:T(8,128)(2,1)S(1)} %get-tuple-element.57), channel_id=1, source_target_pairs={{0,5},{1,4},{2,7},{3,6},{4,1},{5,0},{6,3},{7,2},{8,13},{9,12},{10,... | collective-permute-start | bytes 12296 | tf_op jit(solution)/shard_map/ppermute | solution.py:38
  55.0 1.1 %shard_map.218 = f32[2,4,64,128]{3,2,1,0:T(8,128)} custom-call(f32[8,512]{1,0:T(8,128)S(1)} %get-tuple-element.59.total, f32[520,128]{1,0:T(8,128)S(1)} %shard_map.206.refs_4_.packed), custom_call_target="tpu_custom_call" | custom-call | flops 1000000000 | bytes 65536 | tf_op jit(solution)/shard_map/pallas_call | solution.py:26
  56.1 0.9 %collective-permute-done.23.refs_2_ = bf16[8,256]{1,0:T(8,128)(2,1)S(1)} collective-permute-done((bf16[8,256]{1,0:T(8,128)(2,1)S(1)}, bf16[8,256]{1,0:T(8,128)(2,1)S(1)}, u32[]{:S(2)}, u32[]{:S(2)}) %collective-permute-start.23) | collective-permute-done | bytes 4128 | tf_op jit(solution)/shard_map/ppermute | solution.py:38
  57.0 0.6 %shard_map.217 = bf16[8,256]{1,0:T(8,128)(2,1)} custom-call(bf16[8,512]{1,0:T(8,128)(2,1)S(1)} %shard_map.208.x.after, f32[8,256]{1,0:T(8,128)S(1)} %get-tuple-element.55.refs_0_, bf16[8,256]{1,0:T(8,128)(2,1)S(1)} %collective-permute-done.22.refs_1_, bf16[8,256]{1,0:T(8,128)(2,1)S(1)} %collective-permute-done.23.refs_2_, ...), custom_call_target="tpu_custom_call" | custom-call | bytes 65536 | tf_op jit(solution)/shard_map/pallas_call | solution.py:26
  (83 shorter events, 7.2 us)
Async XLA Ops:
  0.6 6.2 %collective-permute-start = (bf16[8,256]{1,0:T(8,128)(2,1)}, bf16[8,256]{1,0:T(8,128)(2,1)S(1)}, u32[]{:S(2)}, u32[]{:S(2)}) collective-permute-start(bf16[8,256]{1,0:T(8,128)(2,1)} %x.1), channel_id=1, source_target_pairs={{0,1},{1,0},{2,3},{3,2},{4,5},{5,4},{6,7},{7,6},{8,9},{9,8},{10,11... | collective-permute-start | bytes 12296 | tf_op jit(solution)/shard_map/ppermute | solution.py:38
  6.2 20.7 %collective-permute-start.9 = (bf16[512,1792]{1,0:T(8,128)(2,1)S(1)}, bf16[512,1792]{1,0:T(8,128)(2,1)S(1)}, u32[]{:S(2)}, u32[]{:S(2)}) collective-permute-start(bf16[512,1792]{1,0:T(8,128)(2,1)S(1)} %shard_map.204.refs_6_), channel_id=1, source_target_pairs={{0,1},{1,0},{2,3},{3,2},{4,5},{5,4},{6,7},{7,6},{8,9},{9,8},{10,11... | collective-permute-start | bytes 5505032 | tf_op jit(solution)/shard_map/ppermute | solution.py:38
  6.8 6.6 %copy-start = (bf16[2048,704]{0,1:T(8,128)(2,1)S(1)}, bf16[2048,704]{0,1:T(8,128)(2,1)}, u32[]{:S(2)}) copy-start(bf16[2048,704]{0,1:T(8,128)(2,1)} %param.23) | copy-start | bytes 8650756
  6.8 6.6 %copy-start.1 = (bf16[2048,704]{0,1:T(8,128)(2,1)S(1)}, bf16[2048,704]{0,1:T(8,128)(2,1)}, u32[]{:S(2)}) copy-start(bf16[2048,704]{0,1:T(8,128)(2,1)} %param.24) | copy-start | bytes 8650756
  6.8 6.6 %copy-start.5 = (bf16[704,2048]{1,0:T(8,128)(2,1)S(1)}, bf16[704,2048]{1,0:T(8,128)(2,1)}, u32[]{:S(2)}) copy-start(bf16[704,2048]{1,0:T(8,128)(2,1)} %w_down.6) | copy-start | bytes 8650756
  6.9 6.5 %copy-start.12 = (f32[2048]{0:T(1024)S(1)}, f32[2048]{0:T(1024)}, u32[]{:S(2)}) copy-start(f32[2048]{0:T(1024)} %param.22) | copy-start | bytes 24580
  6.9 7.0 %collective-permute-start.3 = (bf16[8,512]{1,0:T(8,128)(2,1)S(1)}, bf16[8,512]{1,0:T(8,128)(2,1)S(1)}, u32[]{:S(2)}, u32[]{:S(2)}) collective-permute-start(bf16[8,512]{1,0:T(8,128)(2,1)S(1)} %shard_map.196.x.refs_4_), channel_id=1, source_target_pairs={{6,1},{7,0},{4,3},{5,2},{2,5},{3,4},{0,7},{1,6},{14,9},{15,8},{12,... | collective-permute-start | bytes 24584 | tf_op jit(solution)/shard_map/ppermute | solution.py:56
  11.7 3.1 %collective-permute-start.2 = (bf16[8,512]{1,0:T(8,128)(2,1)S(1)}, bf16[8,512]{1,0:T(8,128)(2,1)S(1)}, u32[]{:S(2)}, u32[]{:S(2)}) collective-permute-start(bf16[8,512]{1,0:T(8,128)(2,1)S(1)} %shard_map.196.x.refs_4_), channel_id=1, source_target_pairs={{2,1},{3,0},{6,3},{7,2},{0,5},{1,4},{4,7},{5,6},{10,9},{11,8},{14,... | collective-permute-start | bytes 24584 | tf_op jit(solution)/shard_map/ppermute | solution.py:56
  11.7 4.0 %collective-permute-start.1 = (bf16[8,512]{1,0:T(8,128)(2,1)S(1)}, bf16[8,512]{1,0:T(8,128)(2,1)S(1)}, u32[]{:S(2)}, u32[]{:S(2)}) collective-permute-start(bf16[8,512]{1,0:T(8,128)(2,1)S(1)} %shard_map.196.x.refs_4_), channel_id=1, source_target_pairs={{4,1},{5,0},{0,3},{1,2},{6,5},{7,4},{2,7},{3,6},{12,9},{13,8},{8,1... | collective-permute-start | bytes 24584 | tf_op jit(solution)/shard_map/ppermute | solution.py:56
  16.7 3.3 %collective-permute-start.4 = (f32[3,8,512]{2,1,0:T(8,128)S(1)}, f32[3,8,512]{2,1,0:T(8,128)S(1)}, u32[]{:S(2)}, u32[]{:S(2)}) collective-permute-start(f32[3,8,512]{2,1,0:T(8,128)S(1)} %shard_map.201.mine), channel_id=1, source_target_pairs={{0,1},{1,0},{2,3},{3,2},{4,5},{5,4},{6,7},{7,6},{8,9},{9,8},{10,11... | collective-permute-start | bytes 147464 | tf_op jit(solution)/shard_map/ppermute | solution.py:38
  16.8 1.2 %collective-permute-start.7 = (f32[8,512]{1,0:T(8,128)S(1)}, f32[8,512]{1,0:T(8,128)S(1)}, u32[]{:S(2)}, u32[]{:S(2)}) collective-permute-start(f32[8,512]{1,0:T(8,128)S(1)} %get-tuple-element.41.mine), channel_id=1, source_target_pairs={{0,1},{1,0},{2,3},{3,2},{4,5},{5,4},{6,7},{7,6},{8,9},{9,8},{10,11... | collective-permute-start | bytes 49160 | tf_op jit(solution)/shard_map/ppermute | solution.py:38
  17.2 14.5 %collective-permute-start.13 = (f32[520,128]{1,0:T(8,128)S(1)}, f32[520,128]{1,0:T(8,128)S(1)}, u32[]{:S(2)}, u32[]{:S(2)}) collective-permute-start(f32[520,128]{1,0:T(8,128)S(1)} %shard_map.206.refs_4_.packed), channel_id=1, source_target_pairs={{0,1},{1,0},{2,3},{3,2},{4,5},{5,4},{6,7},{7,6},{8,9},{9,8},{10,11... | collective-permute-start | bytes 798728 | tf_op jit(solution)/shard_map/ppermute | solution.py:38
  17.4 22.0 %collective-permute-start.17 = (bf16[512,512]{1,0:T(8,128)(2,1)S(1)}, bf16[512,512]{1,0:T(8,128)(2,1)S(1)}, u32[]{:S(2)}, u32[]{:S(2)}) collective-permute-start(bf16[512,512]{1,0:T(8,128)(2,1)S(1)} %copy-done.17), channel_id=1, source_target_pairs={{0,1},{1,0},{2,3},{3,2},{4,5},{5,4},{6,7},{7,6},{8,9},{9,8},{10,11... | collective-permute-start | bytes 1572872 | tf_op jit(solution)/shard_map/ppermute | solution.py:38
  18.0 8.9 %copy-start.16 = (f32[512]{0:T(512)S(1)}, f32[512]{0:T(512)}, u32[]{:S(2)}) copy-start(f32[512]{0:T(512)} %param.26) | copy-start | bytes 6148
  18.0 4.9 %collective-permute-start.8 = (bf16[8,512]{1,0:T(8,128)(2,1)S(1)}, bf16[8,512]{1,0:T(8,128)(2,1)S(1)}, u32[]{:S(2)}, u32[]{:S(2)}) collective-permute-start(bf16[8,512]{1,0:T(8,128)(2,1)S(1)} %shard_map.203), channel_id=1, source_target_pairs={{0,7},{1,6},{2,5},{3,4},{4,3},{5,2},{6,1},{7,0},{8,15},{9,14},{10,... | collective-permute-start | bytes 24584 | tf_op jit(solution)/shard_map/ppermute | solution.py:38
  20.0 3.1 %collective-permute-start.5 = (bf16[8,512]{1,0:T(8,128)(2,1)S(1)}, bf16[8,512]{1,0:T(8,128)(2,1)S(1)}, u32[]{:S(2)}, u32[]{:S(2)}) collective-permute-start(bf16[8,512]{1,0:T(8,128)(2,1)S(1)} %get-tuple-element.39), channel_id=1, source_target_pairs={{0,3},{1,2},{2,1},{3,0},{4,7},{5,6},{6,5},{7,4},{8,11},{9,10},{10,... | collective-permute-start | bytes 24584 | tf_op jit(solution)/shard_map/ppermute | solution.py:38
  22.9 4.0 %collective-permute-start.6 = (bf16[8,512]{1,0:T(8,128)(2,1)S(1)}, bf16[8,512]{1,0:T(8,128)(2,1)S(1)}, u32[]{:S(2)}, u32[]{:S(2)}) collective-permute-start(bf16[8,512]{1,0:T(8,128)(2,1)S(1)} %get-tuple-element.40), channel_id=1, source_target_pairs={{0,5},{1,4},{2,7},{3,6},{4,1},{5,0},{6,3},{7,2},{8,13},{9,12},{10,... | collective-permute-start | bytes 24584 | tf_op jit(solution)/shard_map/ppermute | solution.py:38
  27.5 4.2 %collective-permute-start.10 = (bf16[8,1024]{1,0:T(8,128)(2,1)S(1)}, bf16[8,1024]{1,0:T(8,128)(2,1)S(1)}, u32[]{:S(2)}, u32[]{:S(2)}) collective-permute-start(bf16[8,1024]{1,0:T(8,128)(2,1)S(1)} %get-tuple-element.43), channel_id=1, source_target_pairs={{0,3},{1,2},{2,1},{3,0},{4,7},{5,6},{6,5},{7,4},{8,11},{9,10},{10,... | collective-permute-start | bytes 49160 | tf_op jit(solution)/shard_map/ppermute | solution.py:38
  27.6 4.1 %collective-permute-start.11 = (bf16[8,1024]{1,0:T(8,128)(2,1)S(1)}, bf16[8,1024]{1,0:T(8,128)(2,1)S(1)}, u32[]{:S(2)}, u32[]{:S(2)}) collective-permute-start(bf16[8,1024]{1,0:T(8,128)(2,1)S(1)} %get-tuple-element.44), channel_id=1, source_target_pairs={{0,5},{1,4},{2,7},{3,6},{4,1},{5,0},{6,3},{7,2},{8,13},{9,12},{10,... | collective-permute-start | bytes 49160 | tf_op jit(solution)/shard_map/ppermute | solution.py:38
  30.1 5.0 %collective-permute-start.12 = (bf16[8,1024]{1,0:T(8,128)(2,1)S(1)}, bf16[8,1024]{1,0:T(8,128)(2,1)S(1)}, u32[]{:S(2)}, u32[]{:S(2)}) collective-permute-start(bf16[8,1024]{1,0:T(8,128)(2,1)S(1)} %get-tuple-element.45), channel_id=1, source_target_pairs={{0,7},{1,6},{2,5},{3,4},{4,3},{5,2},{6,1},{7,0},{8,15},{9,14},{10,... | collective-permute-start | bytes 49160 | tf_op jit(solution)/shard_map/ppermute | solution.py:38
  35.6 3.8 %collective-permute-start.14 = (bf16[2,1024]{1,0:T(2,128)(2,1)S(1)}, bf16[2,1024]{1,0:T(2,128)(2,1)S(1)}, u32[]{:S(2)}, u32[]{:S(2)}) collective-permute-start(bf16[2,1024]{1,0:T(2,128)(2,1)S(1)} %get-tuple-element.46.refs_0_), channel_id=1, source_target_pairs={{0,3},{1,2},{2,1},{3,0},{4,7},{5,6},{6,5},{7,4},{8,11},{9,10},{10,... | collective-permute-start | bytes 12296 | tf_op jit(solution)/shard_map/ppermute | solution.py:38
  35.6 4.0 %collective-permute-start.15 = (bf16[2,1024]{1,0:T(2,128)(2,1)S(1)}, bf16[2,1024]{1,0:T(2,128)(2,1)S(1)}, u32[]{:S(2)}, u32[]{:S(2)}) collective-permute-start(bf16[2,1024]{1,0:T(2,128)(2,1)S(1)} %get-tuple-element.46.refs_0_), channel_id=1, source_target_pairs={{0,5},{1,4},{2,7},{3,6},{4,1},{5,0},{6,3},{7,2},{8,13},{9,12},{10,... | collective-permute-start | bytes 12296 | tf_op jit(solution)/shard_map/ppermute | solution.py:38
  37.5 4.8 %collective-permute-start.16 = (bf16[2,1024]{1,0:T(2,128)(2,1)S(1)}, bf16[2,1024]{1,0:T(2,128)(2,1)S(1)}, u32[]{:S(2)}, u32[]{:S(2)}) collective-permute-start(bf16[2,1024]{1,0:T(2,128)(2,1)S(1)} %get-tuple-element.46.refs_0_), channel_id=1, source_target_pairs={{0,7},{1,6},{2,5},{3,4},{4,3},{5,2},{6,1},{7,0},{8,15},{9,14},{10,... | collective-permute-start | bytes 12296 | tf_op jit(solution)/shard_map/ppermute | solution.py:38
  42.4 3.9 %copy-start.13 = (f32[2048]{0:T(1024)S(1)}, f32[2048]{0:T(1024)}, u32[]{:S(2)}) copy-start(f32[2048]{0:T(1024)} %param.34) | copy-start | bytes 24580
  42.6 4.9 %collective-permute-start.20 = (bf16[8,512]{1,0:T(8,128)(2,1)S(1)}, bf16[8,512]{1,0:T(8,128)(2,1)S(1)}, u32[]{:S(2)}, u32[]{:S(2)}) collective-permute-start(bf16[8,512]{1,0:T(8,128)(2,1)S(1)} %shard_map.208.x.after), channel_id=1, source_target_pairs={{6,1},{7,0},{4,3},{5,2},{2,5},{3,4},{0,7},{1,6},{14,9},{15,8},{12,... | collective-permute-start | bytes 24584 | tf_op jit(solution)/shard_map/ppermute | solution.py:56
  44.5 3.5 %collective-permute-start.19 = (bf16[8,512]{1,0:T(8,128)(2,1)S(1)}, bf16[8,512]{1,0:T(8,128)(2,1)S(1)}, u32[]{:S(2)}, u32[]{:S(2)}) collective-permute-start(bf16[8,512]{1,0:T(8,128)(2,1)S(1)} %shard_map.208.x.after), channel_id=1, source_target_pairs={{2,1},{3,0},{6,3},{7,2},{0,5},{1,4},{4,7},{5,6},{10,9},{11,8},{14,... | collective-permute-start | bytes 24584 | tf_op jit(solution)/shard_map/ppermute | solution.py:56
  44.5 4.0 %collective-permute-start.18 = (bf16[8,512]{1,0:T(8,128)(2,1)S(1)}, bf16[8,512]{1,0:T(8,128)(2,1)S(1)}, u32[]{:S(2)}, u32[]{:S(2)}) collective-permute-start(bf16[8,512]{1,0:T(8,128)(2,1)S(1)} %shard_map.208.x.after), channel_id=1, source_target_pairs={{4,1},{5,0},{0,3},{1,2},{6,5},{7,4},{2,7},{3,6},{12,9},{13,8},{8,1... | collective-permute-start | bytes 24584 | tf_op jit(solution)/shard_map/ppermute | solution.py:56
  49.4 3.5 %collective-permute-start.21 = (f32[3,8,256]{2,1,0:T(8,128)S(1)}, f32[3,8,256]{2,1,0:T(8,128)S(1)}, u32[]{:S(2)}, u32[]{:S(2)}) collective-permute-start(f32[3,8,256]{2,1,0:T(8,128)S(1)} %shard_map.214), channel_id=1, source_target_pairs={{0,1},{1,0},{2,3},{3,2},{4,5},{5,4},{6,7},{7,6},{8,9},{9,8},{10,11... | collective-permute-start | bytes 73736 | tf_op jit(solution)/shard_map/ppermute | solution.py:38
  49.8 1.2 %collective-permute-start.24 = (f32[8,256]{1,0:T(8,128)S(1)}, f32[8,256]{1,0:T(8,128)S(1)}, u32[]{:S(2)}, u32[]{:S(2)}) collective-permute-start(f32[8,256]{1,0:T(8,128)S(1)} %get-tuple-element.58), channel_id=1, source_target_pairs={{0,1},{1,0},{2,3},{3,2},{4,5},{5,4},{6,7},{7,6},{8,9},{9,8},{10,11... | collective-permute-start | bytes 24584 | tf_op jit(solution)/shard_map/ppermute | solution.py:38
  51.0 5.0 %collective-permute-start.25 = (bf16[8,256]{1,0:T(8,128)(2,1)S(1)}, bf16[8,256]{1,0:T(8,128)(2,1)S(1)}, u32[]{:S(2)}, u32[]{:S(2)}) collective-permute-start(bf16[8,256]{1,0:T(8,128)(2,1)S(1)} %shard_map.216), channel_id=1, source_target_pairs={{0,7},{1,6},{2,5},{3,4},{4,3},{5,2},{6,1},{7,0},{8,15},{9,14},{10,... | collective-permute-start | bytes 12296 | tf_op jit(solution)/shard_map/ppermute | solution.py:38
  52.9 3.1 %collective-permute-start.22 = (bf16[8,256]{1,0:T(8,128)(2,1)S(1)}, bf16[8,256]{1,0:T(8,128)(2,1)S(1)}, u32[]{:S(2)}, u32[]{:S(2)}) collective-permute-start(bf16[8,256]{1,0:T(8,128)(2,1)S(1)} %get-tuple-element.56), channel_id=1, source_target_pairs={{0,3},{1,2},{2,1},{3,0},{4,7},{5,6},{6,5},{7,4},{8,11},{9,10},{10,... | collective-permute-start | bytes 12296 | tf_op jit(solution)/shard_map/ppermute | solution.py:38
  53.0 4.0 %collective-permute-start.23 = (bf16[8,256]{1,0:T(8,128)(2,1)S(1)}, bf16[8,256]{1,0:T(8,128)(2,1)S(1)}, u32[]{:S(2)}, u32[]{:S(2)}) collective-permute-start(bf16[8,256]{1,0:T(8,128)(2,1)S(1)} %get-tuple-element.57), channel_id=1, source_target_pairs={{0,5},{1,4},{2,7},{3,6},{4,1},{5,0},{6,3},{7,2},{8,13},{9,12},{10,... | collective-permute-start | bytes 12296 | tf_op jit(solution)/shard_map/ppermute | solution.py:38
  (13 other events, 21.4 us)

commit v3 on v2

--- a/solution.py
+++ b/solution.py
@@ -13,6 +13,17 @@
 f32 = jnp.float32
 bf16 = jnp.bfloat16
 LANES = 128
+XOR1, XOR2, XOR3 = (1, 0, 3, 2), (2, 3, 0, 1), (3, 2, 1, 0)
+RIGHT, LEFT = (1, 2, 3, 0), (3, 0, 1, 2)
+CYCLE, BACK = (1, 3, 0, 2), (2, 0, 3, 1)
+ROUTES = {
+    "rows": (RIGHT, LEFT, XOR2),
+    "first": (XOR2, XOR3, XOR1),
+    "parts": (XOR2, XOR3, XOR1),
+    "heads": (XOR2, XOR3, XOR1),
+    "after": (XOR3, BACK, CYCLE),
+    "second": (RIGHT, XOR2, LEFT),
+}
 WAIT = 6_000_000_000
 
 
@@ -38,29 +49,38 @@
     return lax.ppermute(x, axis, [(j, j ^ shift) for j in range(size)])
 
 
-def source(slot, kv, n):
-    if n != 4 or slot in (0, 3):
-        return kv ^ slot
-    end = (kv == 0) | (kv == 3)
-    return kv ^ jnp.where(end, 3 - slot, slot)
-
-
-def gather_kv(block, n_kv):
+def routes(stage, n):
+    if n == 4:
+        return ROUTES[stage]
+    return [tuple(j ^ s for j in range(n)) for s in range(n - 1, 0, -1)]
+
+
+def looked_up(table, kv):
+    value = jnp.int32(table[0])
+    for j in range(1, len(table)):
+        value = jnp.where(kv == j, table[j], value)
+    return value
+
+
+def target(stage, slot):
+    kv, n = lax.axis_index("kv"), lax.axis_size("kv")
+    return looked_up(routes(stage, n)[n - 1 - slot], kv) if slot else kv
+
+
+def source(stage, slot):
+    kv, n = lax.axis_index("kv"), lax.axis_size("kv")
+    if not slot:
+        return kv
+    route = routes(stage, n)[n - 1 - slot]
+    return looked_up([route.index(j) for j in range(n)], kv)
+
+
+def send_kv(stage, blocks, n_kv):
     got = []
     for slot in range(1, n_kv):
-        pairs = []
-        for kv in range(n_kv):
-            ends = n_kv == 4 and slot < 3 and kv in (0, 3)
-            start = kv ^ (3 - slot if ends else slot)
-            pairs += [(2 * start + t, 2 * kv + 1 - t) for t in range(2)]
-        got.append(lax.ppermute(block, ("kv", "tp"), pairs))
-    return got
-
-
-def send_kv(blocks, n_kv):
-    got = []
-    for s in range(1, n_kv):
-        got.append(swap(blocks[s - 1], ("kv", "tp"), 2 * n_kv, 2 * s + 1))
+        route = routes(stage, n_kv)[n_kv - 1 - slot]
+        pairs = [(2 * j + t, 2 * route[j] + 1 - t) for j in range(n_kv) for t in range(2)]
+        got.append(lax.ppermute(blocks[slot - 1], ("kv", "tp"), pairs))
     return got
 
 
@@ -82,11 +102,10 @@
     return jnp.dot(a, b, preferred_element_type=f32)
 
 
-def add_pieces(pieces, order, gain, w_gate, w_up, gate, up, square):
-    kv = lax.axis_index("kv")
+def add_pieces(stage, pieces, order, gain, w_gate, w_up, gate, up, square):
     for piece, s in zip(pieces, order):
         width = piece.shape[1]
-        cols = pl.ds(pl.multiple_of(source(s, kv, w_gate.shape[1] // width) * width, width), width)
+        cols = pl.ds(pl.multiple_of(source(stage, s) * width, width), width)
         wide = piece.astype(f32)
         scaled = (wide * gain[:, cols]).astype(bf16)
         one = dot_t(scaled, w_gate[:, cols])
@@ -115,25 +134,25 @@
     both[:, own:] = jnp.where(lower, two, one).astype(bf16)
 
 
-def up_first_kernel(x, gain, w_gate, w_up, w_later, acc, sq):
-    gate, up, square = add_pieces([x[...]], [0], gain, w_gate, w_up, None, None, None)
+def up_first_kernel(stage, x, gain, w_gate, w_up, w_later, acc, sq):
+    gate, up, square = add_pieces(stage, [x[...]], [0], gain, w_gate, w_up, None, None, None)
     acc[0], acc[1] = gate, up
     sq[...] = jnp.broadcast_to(square, sq.shape)
 
 
-def up_more_kernel(s, x, gain, w_gate, w_up, acc, sq, acc_out, sq_out):
-    gate, up, square = add_pieces([x[...]], [s], gain, w_gate, w_up, acc[0], acc[1], sq[:, :1])
+def up_more_kernel(stage, s, x, gain, w_gate, w_up, acc, sq, acc_out, sq_out):
+    gate, up, square = add_pieces(stage, [x[...]], [s], gain, w_gate, w_up, acc[0], acc[1], sq[:, :1])
     acc_out[0], acc_out[1] = gate, up
     sq_out[...] = jnp.broadcast_to(square, sq_out.shape)
 
 
 def down_block(hidden, w_down, s, width):
-    cols = pl.ds(pl.multiple_of((lax.axis_index("kv") ^ s) * width, width), width)
+    cols = pl.ds(pl.multiple_of(target("first", s) * width, width), width)
     return dot(hidden, w_down[:, cols])
 
 
 def first_kernel(x, gain, w_gate, w_up, acc, sq, w_down, keep, far):
-    gate, up, square = add_pieces([x[...]], [1], gain, w_gate, w_up, acc[0], acc[1], sq[:, :1])
+    gate, up, square = add_pieces("rows", [x[...]], [1], gain, w_gate, w_up, acc[0], acc[1], sq[:, :1])
     hidden = hidden_of(gate, up, square, w_gate.shape[1])
     keep[...] = hidden
     far[...] = down_block(hidden, w_down, w_down.shape[1] // far.shape[1] - 1, far.shape[1])
@@ -159,7 +178,6 @@
     total = sums[0][...]
     for ref in sums[1:]:
         total = total + ref[...].astype(f32)
-    kv = lax.axis_index("kv")
     mid = (x[...].astype(f32) + 0.5 * total).astype(bf16)
     middle[...] = mid
     wide = mid.astype(f32)
@@ -182,7 +200,7 @@
                     scr[j, down, across] = part[j * rows:(j + 1) * rows, at:at + LANES]
                 chunk += 1
     for s, out in enumerate(outs):
-        out[...] = scr[kv ^ s].astype(out.dtype)
+        out[...] = scr[target("parts", s)].astype(out.dtype)
 
 
 def chunk_place(chunk, rows, height, start):
@@ -297,12 +315,12 @@
 
 def after_kernel(*refs):
     *ins, middle, w_mine, w_theirs, after, scr = refs
-    kv = lax.axis_index("kv")
     half = w_mine.shape[0]
     for s, ref in enumerate(ins):
         one, two = ref[:, :half].astype(f32), ref[:, half:].astype(f32)
-        scr[kv ^ s, :, :half] = one if s == 0 else two
-        scr[kv ^ s, :, half:] = two if s == 0 else one
+        at = source("heads", s)
+        scr[at, :, :half] = one if s == 0 else two
+        scr[at, :, half:] = two if s == 0 else one
     heads = jnp.concatenate([scr[j] for j in range(len(ins))], axis=0).astype(bf16)
     mine = dot(heads[:, :half], w_mine[...]).astype(bf16).astype(f32)
     theirs = dot(heads[:, half:], w_theirs[...]).astype(bf16).astype(f32)
@@ -312,12 +330,13 @@
 def half_product(hidden, w_down, s, side, width):
     tp = lax.axis_index("tp")
     half = tp if side == 0 else 1 - tp
-    cols = pl.ds(pl.multiple_of(((lax.axis_index("kv") ^ s) * 2 + half) * width, width), width)
+    to = target("second", s)
+    cols = pl.ds(pl.multiple_of((to * 2 + half) * width, width), width)
     return dot(hidden, w_down[:, cols])
 
 
 def second_kernel(x, gain, w_gate, w_up, acc, sq, w_down, hidden, theirs):
-    gate, up, square = add_pieces([x[...]], [1], gain, w_gate, w_up, acc[0], acc[1], sq[:, :1])
+    gate, up, square = add_pieces("after", [x[...]], [1], gain, w_gate, w_up, acc[0], acc[1], sq[:, :1])
     hid = hidden_of(gate, up, square, w_gate.shape[1])
     hidden[...] = hid
     width = theirs.shape[1]
@@ -367,20 +386,22 @@
     near = call(copy_kernel, shape(stream.shape, bf16), stream, flops=WAIT)
     wide = call(pair_kernel, shape((rows, pair), bf16), near, swap(stream, "tp", n_tp, 1), flops=2 * WAIT)
     wide = call(copy_kernel, shape((rows, pair), bf16), wide, flops=WAIT)
-    others = gather_kv(wide, n_kv)
+    others = send_kv("rows", [wide] * (n_kv - 1), n_kv)
     up_flops = 4 * rows * pair * hid
     wg, wu = first_gate.T, first_up.T
 
-    def up(x, others, gain, wg, wu, down):
-        acc = call(up_first_kernel, acc_shape, x, gain, wg, wu, down, flops=up_flops, limit=12)
+    def up(stage, x, others, gain, wg, wu, down):
+        acc = call(
+            functools.partial(up_first_kernel, stage), acc_shape, x, gain, wg, wu, down, flops=up_flops, limit=12
+        )
         for s in range(n_kv - 1, 1, -1):
             acc = call(
-                functools.partial(up_more_kernel, s), acc_shape, others[s - 1], gain, wg, wu, *acc,
+                functools.partial(up_more_kernel, stage, s), acc_shape, others[s - 1], gain, wg, wu, *acc,
                 flops=up_flops, limit=12,
             )
         return acc
 
-    acc = up(wide, others, g1, wg, wu, first_down)
+    acc = up("rows", wide, others, g1, wg, wu, first_down)
     hidden, far = call(
         first_kernel, [shape((rows, hid), bf16), shape((rows, pair))], others[0], g1, wg, wu, *acc,
         first_down, flops=2 * up_flops, limit=16,
@@ -402,7 +423,7 @@
         states_kernel, shape((local_rows * heads * keys + heads // 2 * local_rows + heads, LANES)),
         old_state, decay_amounts, gh,
     )
-    arrived = send_kv(blocks + [far], n_kv)
+    arrived = send_kv("first", blocks + [far], n_kv)
     packed_other, w_other = lend((packed, output_weight))
     total = 2 * (3 * nk + 2 * nv + 2 * LANES)
     dense = (8, total * local_rows // 8)
@@ -414,7 +435,7 @@
     mixed, summed = call(
         functools.partial(mix_kernel, depth, old_state.shape),
         [shape((local_rows, 2 * nv), bf16), shape((8, dense[1] // 2))],
-        parts[0], *send_kv(parts[1:], n_kv), packed, packed_other,
+        parts[0], *send_kv("parts", parts[1:], n_kv), packed, packed_other,
         flops=8 * old_state.size,
     )
     new_state = call(
@@ -422,13 +443,13 @@
         flops=1_000_000_000,
     )
     after = call(
-        after_kernel, shape((rows, pair), bf16), mixed, *send_kv([mixed] * (n_kv - 1), n_kv),
+        after_kernel, shape((rows, pair), bf16), mixed, *send_kv("heads", [mixed] * (n_kv - 1), n_kv),
         middle, output_weight, w_other, scratch=[pltpu.VMEM((n_kv, local_rows, 2 * nv), f32)],
         flops=WAIT,
     )
-    others = gather_kv(after, n_kv)
+    others = send_kv("after", [after] * (n_kv - 1), n_kv)
     wg, wu = second_gate.T, second_up.T
-    acc = up(after, others, g2, wg, wu, second_down)
+    acc = up("after", after, others, g2, wg, wu, second_down)
     hidden, theirs = call(
         second_kernel, [shape((rows, hid), bf16), shape((rows, own))],
         others[0], g2, wg, wu, *acc, second_down, flops=2 * up_flops, limit=16,
@@ -446,7 +467,7 @@
     far = call(add_far_kernel, shape((rows, own), bf16), mine, far)
     own_block, *blocks = call(add_rest_kernel, sums((rows, own))[:-1], mine, rest)
     blocks = [own_block, *blocks, far]
-    mixed_stream = call(last_kernel, shape((rows, own), bf16), after, blocks[0], *send_kv(blocks[1:], n_kv))
+    mixed_stream = call(last_kernel, shape((rows, own), bf16), after, blocks[0], *send_kv("second", blocks[1:], n_kv))
     return (mixed_stream, new_state)
 
 

time: 58 us -> 57.7 us (level)
  starting transfers between devices: 26.3 us -> 25.5 us
  waiting for transfers between devices: 16.6 us -> 17.2 us
    ppermute x6 -> x18, waiting for transfers between devices: 1.51 us -> 16.3 us  [send_kv(): got.append(lax.ppermute(blocks[slot - 1], ('kv', 'tp'), pairs))]
    ppermute x20 -> x8, waiting for transfers between devices: 15.1 us -> 0.95 us  [swap(): return lax.ppermute(x, axis, [(j, j ^ shift) for j in range(size)])]
    ppermute x20 -> x8, starting transfers between devices: 16.2 us -> 2.27 us  [swap(): return lax.ppermute(x, axis, [(j, j ^ shift) for j in range(size)])]
    ppermute x6 -> x18, starting transfers between devices: 10.2 us -> 23.2 us  [send_kv(): got.append(lax.ppermute(blocks[slot - 1], ('kv', 'tp'), pairs))]
  transfers between devices with their start and end apart: 26 -> 26, of which waited for: 13 -> 14; matrix products, arithmetic and copies ran while one was open for 0% -> 0% of each run, Pallas kernels for 12% -> 12%
where the time goes in v3:
time: 57.7 us; the launch traced here: 57.4 us
  starting transfers between devices  25.5 us (44%)
  waiting for transfers between devices  17.2 us (30%)
  Pallas kernels  8.44 us (15%)
  local copies, waits for them, and re-layouts  5.49 us (10%)
  between operations  0.76 us (1%)
    ppermute x18, starting transfers between devices, send_kv(): got.append(lax.ppermute(blocks[slot - 1], ('kv', 'tp'), pairs))  23.2 us
    ppermute x18, waiting for transfers between devices, send_kv(): got.append(lax.ppermute(blocks[slot - 1], ('kv', 'tp'), pairs))  16.3 us
    pallas_call x25, Pallas kernels, call(): pl.pallas_call(kernel, out_shape=outs, in_specs=[vmem] * len(args), out_s...  8.44 us
    unnamed x38, local copies, waits for them, and re-layouts  5.49 us
    ppermute x8, starting transfers between devices, swap(): return lax.ppermute(x, axis, [(j, j ^ shift) for j in range(size)])  2.27 us
  transfers between devices with their start and end apart: 26, of which 14 were waited for; matrix products, arithmetic and copies ran while one was open for 0% of the time, Pallas kernels for 12%

profile of v3, /device:TPU:0, one launch (start us, length us, event | category | flops | bytes accessed | tf_op | source)
XLA Modules:
  0.0 57.4 jit_solution(10825923863813212106)
XLA Ops:
  1.2 1.0 %copy-done.6 = bf16[512,512]{1,0:T(8,128)(2,1)S(1)} copy-done((bf16[512,512]{1,0:T(8,128)(2,1)S(1)}, bf16[512,512]{1,0:T(8,128)(2,1)}, u32[]{:S(2)}) %copy-start.6) | copy-done | bytes 524312
  2.2 1.0 %copy-done.7 = bf16[512,512]{1,0:T(8,128)(2,1)S(1)} copy-done((bf16[512,512]{1,0:T(8,128)(2,1)S(1)}, bf16[512,512]{1,0:T(8,128)(2,1)}, u32[]{:S(2)}) %copy-start.7) | copy-done | bytes 524312
  3.3 0.9 %copy-done.8 = bf16[512,256]{1,0:T(8,128)(2,1)S(1)} copy-done((bf16[512,256]{1,0:T(8,128)(2,1)S(1)}, bf16[512,256]{1,0:T(8,128)(2,1)}, u32[]{:S(2)}) %copy-start.8) | copy-done | bytes 262168
  4.2 0.9 %copy-done.9 = bf16[512,256]{1,0:T(8,128)(2,1)S(1)} copy-done((bf16[512,256]{1,0:T(8,128)(2,1)S(1)}, bf16[512,256]{1,0:T(8,128)(2,1)}, u32[]{:S(2)}) %copy-start.9) | copy-done | bytes 262168
  5.2 0.9 %copy-done.10 = bf16[512,256]{1,0:T(8,128)(2,1)S(1)} copy-done((bf16[512,256]{1,0:T(8,128)(2,1)S(1)}, bf16[512,256]{1,0:T(8,128)(2,1)}, u32[]{:S(2)}) %copy-start.10) | copy-done | bytes 262168
  6.9 2.7 %collective-permute-start.3 = (bf16[8,512]{1,0:T(8,128)(2,1)S(1)}, bf16[8,512]{1,0:T(8,128)(2,1)S(1)}, u32[]{:S(2)}, u32[]{:S(2)}) collective-permute-start(bf16[8,512]{1,0:T(8,128)(2,1)S(1)} %shard_map.196.x.refs_4_), channel_id=1, source_target_pairs={{0,3},{1,2},{2,5},{3,4},{4,7},{5,6},{6,1},{7,0},{8,11},{9,10},{10,... | collective-permute-start | bytes 24584 | tf_op jit(solution)/shard_map/ppermute | solution.py:83
  9.6 2.1 %collective-permute-start.2 = (bf16[8,512]{1,0:T(8,128)(2,1)S(1)}, bf16[8,512]{1,0:T(8,128)(2,1)S(1)}, u32[]{:S(2)}, u32[]{:S(2)}) collective-permute-start(bf16[8,512]{1,0:T(8,128)(2,1)S(1)} %shard_map.196.x.refs_4_), channel_id=1, source_target_pairs={{0,7},{1,6},{2,1},{3,0},{4,3},{5,2},{6,5},{7,4},{8,15},{9,14},{10,... | collective-permute-start | bytes 24584 | tf_op jit(solution)/shard_map/ppermute | solution.py:83
  11.7 0.7 %collective-permute-start.1 = (bf16[8,512]{1,0:T(8,128)(2,1)S(1)}, bf16[8,512]{1,0:T(8,128)(2,1)S(1)}, u32[]{:S(2)}, u32[]{:S(2)}) collective-permute-start(bf16[8,512]{1,0:T(8,128)(2,1)S(1)} %shard_map.196.x.refs_4_), channel_id=1, source_target_pairs={{0,5},{1,4},{2,7},{3,6},{4,1},{5,0},{6,3},{7,2},{8,13},{9,12},{10,... | collective-permute-start | bytes 24584 | tf_op jit(solution)/shard_map/ppermute | solution.py:83
  14.0 1.7 %collective-permute-done.1.x = bf16[8,512]{1,0:T(8,128)(2,1)S(1)} collective-permute-done((bf16[8,512]{1,0:T(8,128)(2,1)S(1)}, bf16[8,512]{1,0:T(8,128)(2,1)S(1)}, u32[]{:S(2)}, u32[]{:S(2)}) %collective-permute-start.1) | collective-permute-done | bytes 8224 | tf_op jit(solution)/shard_map/ppermute | solution.py:83
  18.1 0.7 %collective-permute-start.8 = (bf16[8,512]{1,0:T(8,128)(2,1)S(1)}, bf16[8,512]{1,0:T(8,128)(2,1)S(1)}, u32[]{:S(2)}, u32[]{:S(2)}) collective-permute-start(bf16[8,512]{1,0:T(8,128)(2,1)S(1)} %shard_map.203), channel_id=1, source_target_pairs={{0,5},{1,4},{2,7},{3,6},{4,1},{5,0},{6,3},{7,2},{8,13},{9,12},{10,... | collective-permute-start | bytes 24584 | tf_op jit(solution)/shard_map/ppermute | solution.py:83
  18.8 1.6 %collective-permute-start.5 = (bf16[8,512]{1,0:T(8,128)(2,1)S(1)}, bf16[8,512]{1,0:T(8,128)(2,1)S(1)}, u32[]{:S(2)}, u32[]{:S(2)}) collective-permute-start(bf16[8,512]{1,0:T(8,128)(2,1)S(1)} %get-tuple-element.39), channel_id=1, source_target_pairs={{0,3},{1,2},{2,1},{3,0},{4,7},{5,6},{6,5},{7,4},{8,11},{9,10},{10,... | collective-permute-start | bytes 24584 | tf_op jit(solution)/shard_map/ppermute | solution.py:83
  20.4 1.7 %collective-permute-done.8.refs_3_ = bf16[8,512]{1,0:T(8,128)(2,1)S(1)} collective-permute-done((bf16[8,512]{1,0:T(8,128)(2,1)S(1)}, bf16[8,512]{1,0:T(8,128)(2,1)S(1)}, u32[]{:S(2)}, u32[]{:S(2)}) %collective-permute-start.8) | collective-permute-done | bytes 8224 | tf_op jit(solution)/shard_map/ppermute | solution.py:83
  22.1 1.7 %collective-permute-start.6 = (bf16[8,512]{1,0:T(8,128)(2,1)S(1)}, bf16[8,512]{1,0:T(8,128)(2,1)S(1)}, u32[]{:S(2)}, u32[]{:S(2)}) collective-permute-start(bf16[8,512]{1,0:T(8,128)(2,1)S(1)} %get-tuple-element.40), channel_id=1, source_target_pairs={{0,7},{1,6},{2,5},{3,4},{4,3},{5,2},{6,1},{7,0},{8,15},{9,14},{10,... | collective-permute-start | bytes 24584 | tf_op jit(solution)/shard_map/ppermute | solution.py:83
  23.8 3.2 %collective-permute-done.6.refs_2_ = bf16[8,512]{1,0:T(8,128)(2,1)S(1)} collective-permute-done((bf16[8,512]{1,0:T(8,128)(2,1)S(1)}, bf16[8,512]{1,0:T(8,128)(2,1)S(1)}, u32[]{:S(2)}, u32[]{:S(2)}) %collective-permute-start.6) | collective-permute-done | bytes 8224 | tf_op jit(solution)/shard_map/ppermute | solution.py:83
  27.6 1.7 %collective-permute-start.11 = (bf16[8,1024]{1,0:T(8,128)(2,1)S(1)}, bf16[8,1024]{1,0:T(8,128)(2,1)S(1)}, u32[]{:S(2)}, u32[]{:S(2)}) collective-permute-start(bf16[8,1024]{1,0:T(8,128)(2,1)S(1)} %get-tuple-element.44), channel_id=1, source_target_pairs={{0,7},{1,6},{2,5},{3,4},{4,3},{5,2},{6,1},{7,0},{8,15},{9,14},{10,... | collective-permute-start | bytes 49160 | tf_op jit(solution)/shard_map/ppermute | solution.py:83
  29.4 1.4 %collective-permute-start.12 = (bf16[8,1024]{1,0:T(8,128)(2,1)S(1)}, bf16[8,1024]{1,0:T(8,128)(2,1)S(1)}, u32[]{:S(2)}, u32[]{:S(2)}) collective-permute-start(bf16[8,1024]{1,0:T(8,128)(2,1)S(1)} %get-tuple-element.45), channel_id=1, source_target_pairs={{0,5},{1,4},{2,7},{3,6},{4,1},{5,0},{6,3},{7,2},{8,13},{9,12},{10,... | collective-permute-start | bytes 49160 | tf_op jit(solution)/shard_map/ppermute | solution.py:83
  30.8 1.9 %collective-permute-done.11.refs_2_ = bf16[8,1024]{1,0:T(8,128)(2,1)S(1)} collective-permute-done((bf16[8,1024]{1,0:T(8,128)(2,1)S(1)}, bf16[8,1024]{1,0:T(8,128)(2,1)S(1)}, u32[]{:S(2)}, u32[]{:S(2)}) %collective-permute-start.11) | collective-permute-done | bytes 16416 | tf_op jit(solution)/shard_map/ppermute | solution.py:83
  32.7 0.7 %collective-permute-done.12.refs_3_ = bf16[8,1024]{1,0:T(8,128)(2,1)S(1)} collective-permute-done((bf16[8,1024]{1,0:T(8,128)(2,1)S(1)}, bf16[8,1024]{1,0:T(8,128)(2,1)S(1)}, u32[]{:S(2)}, u32[]{:S(2)}) %collective-permute-start.12) | collective-permute-done | bytes 16416 | tf_op jit(solution)/shard_map/ppermute | solution.py:83
  34.0 0.8 %collective-permute-start.14 = (bf16[2,1024]{1,0:T(2,128)(2,1)S(1)}, bf16[2,1024]{1,0:T(2,128)(2,1)S(1)}, u32[]{:S(2)}, u32[]{:S(2)}) collective-permute-start(bf16[2,1024]{1,0:T(2,128)(2,1)S(1)} %get-tuple-element.46.refs_0_), channel_id=1, source_target_pairs={{0,3},{1,2},{2,1},{3,0},{4,7},{5,6},{6,5},{7,4},{8,11},{9,10},{10,... | collective-permute-start | bytes 12296 | tf_op jit(solution)/shard_map/ppermute | solution.py:83
  34.8 1.9 %collective-permute-start.15 = (bf16[2,1024]{1,0:T(2,128)(2,1)S(1)}, bf16[2,1024]{1,0:T(2,128)(2,1)S(1)}, u32[]{:S(2)}, u32[]{:S(2)}) collective-permute-start(bf16[2,1024]{1,0:T(2,128)(2,1)S(1)} %get-tuple-element.46.refs_0_), channel_id=1, source_target_pairs={{0,7},{1,6},{2,5},{3,4},{4,3},{5,2},{6,1},{7,0},{8,15},{9,14},{10,... | collective-permute-start | bytes 12296 | tf_op jit(solution)/shard_map/ppermute | solution.py:83
  36.7 0.8 %collective-permute-start.16 = (bf16[2,1024]{1,0:T(2,128)(2,1)S(1)}, bf16[2,1024]{1,0:T(2,128)(2,1)S(1)}, u32[]{:S(2)}, u32[]{:S(2)}) collective-permute-start(bf16[2,1024]{1,0:T(2,128)(2,1)S(1)} %get-tuple-element.46.refs_0_), channel_id=1, source_target_pairs={{0,5},{1,4},{2,7},{3,6},{4,1},{5,0},{6,3},{7,2},{8,13},{9,12},{10,... | collective-permute-start | bytes 12296 | tf_op jit(solution)/shard_map/ppermute | solution.py:83
  37.5 2.1 %collective-permute-done.15.refs_2_ = bf16[2,1024]{1,0:T(2,128)(2,1)S(1)} collective-permute-done((bf16[2,1024]{1,0:T(2,128)(2,1)S(1)}, bf16[2,1024]{1,0:T(2,128)(2,1)S(1)}, u32[]{:S(2)}, u32[]{:S(2)}) %collective-permute-start.15) | collective-permute-done | bytes 4128 | tf_op jit(solution)/shard_map/ppermute | solution.py:83
  39.6 1.0 %collective-permute-done.16.refs_3_ = bf16[2,1024]{1,0:T(2,128)(2,1)S(1)} collective-permute-done((bf16[2,1024]{1,0:T(2,128)(2,1)S(1)}, bf16[2,1024]{1,0:T(2,128)(2,1)S(1)}, u32[]{:S(2)}, u32[]{:S(2)}) %collective-permute-start.16) | collective-permute-done | bytes 4128 | tf_op jit(solution)/shard_map/ppermute | solution.py:83
  40.8 1.7 %collective-permute-start.20 = (bf16[8,512]{1,0:T(8,128)(2,1)S(1)}, bf16[8,512]{1,0:T(8,128)(2,1)S(1)}, u32[]{:S(2)}, u32[]{:S(2)}) collective-permute-start(bf16[8,512]{1,0:T(8,128)(2,1)S(1)} %shard_map.208.x.after), channel_id=1, source_target_pairs={{0,7},{1,6},{2,5},{3,4},{4,3},{5,2},{6,1},{7,0},{8,15},{9,14},{10,... | collective-permute-start | bytes 24584 | tf_op jit(solution)/shard_map/ppermute | solution.py:83
  42.5 1.7 %collective-permute-start.18 = (bf16[8,512]{1,0:T(8,128)(2,1)S(1)}, bf16[8,512]{1,0:T(8,128)(2,1)S(1)}, u32[]{:S(2)}, u32[]{:S(2)}) collective-permute-start(bf16[8,512]{1,0:T(8,128)(2,1)S(1)} %shard_map.208.x.after), channel_id=1, source_target_pairs={{0,3},{1,2},{2,7},{3,6},{4,1},{5,0},{6,5},{7,4},{8,11},{9,10},{10,... | collective-permute-start | bytes 24584 | tf_op jit(solution)/shard_map/ppermute | solution.py:83
  44.8 1.0 %collective-permute-done.20.x = bf16[8,512]{1,0:T(8,128)(2,1)S(1)} collective-permute-done((bf16[8,512]{1,0:T(8,128)(2,1)S(1)}, bf16[8,512]{1,0:T(8,128)(2,1)S(1)}, u32[]{:S(2)}, u32[]{:S(2)}) %collective-permute-start.20) | collective-permute-done | bytes 8224 | tf_op jit(solution)/shard_map/ppermute | solution.py:83
  46.7 0.7 %shard_map.212 = (bf16[8,704]{1,0:T(8,128)(2,1)S(1)}, f32[8,256]{1,0:T(8,128)S(1)}) custom-call(bf16[8,512]{1,0:T(8,128)(2,1)S(1)} %collective-permute-done.18.x, f32[1,2048]{1,0:T(1,128)S(1)} %bitcast.31, bf16[704,2048]{1,0:T(8,128)(2,1)S(1)} %bitcast.19, bf16[704,2048]{1,0:T(8,128)(2,1)S(1)} %bitcast.23, f32[2,8,704]{2,1,0:T(8,128)S(1)} %get-tuple-element.52.acc, ...), custom_call_target="tpu_custom_call" | custom-call | flops 23068672 | bytes 65536 | tf_op jit(solution)/shard_map/pallas_call | solution.py:37
  48.5 0.7 %collective-permute-done.24.other = f32[8,256]{1,0:T(8,128)S(1)} collective-permute-done((f32[8,256]{1,0:T(8,128)S(1)}, f32[8,256]{1,0:T(8,128)S(1)}, u32[]{:S(2)}, u32[]{:S(2)}) %collective-permute-start.24) | collective-permute-done | bytes 8224 | tf_op jit(solution)/shard_map/ppermute | solution.py:49
  49.2 0.6 %collective-permute-start.25 = (bf16[8,256]{1,0:T(8,128)(2,1)S(1)}, bf16[8,256]{1,0:T(8,128)(2,1)S(1)}, u32[]{:S(2)}, u32[]{:S(2)}) collective-permute-start(bf16[8,256]{1,0:T(8,128)(2,1)S(1)} %shard_map.216), channel_id=1, source_target_pairs={{0,3},{1,2},{2,5},{3,4},{4,7},{5,6},{6,1},{7,0},{8,11},{9,10},{10,... | collective-permute-start | bytes 12296 | tf_op jit(solution)/shard_map/ppermute | solution.py:83
  49.9 3.0 %collective-permute-start.22 = (bf16[8,256]{1,0:T(8,128)(2,1)S(1)}, bf16[8,256]{1,0:T(8,128)(2,1)S(1)}, u32[]{:S(2)}, u32[]{:S(2)}) collective-permute-start(bf16[8,256]{1,0:T(8,128)(2,1)S(1)} %get-tuple-element.56), channel_id=1, source_target_pairs={{0,7},{1,6},{2,1},{3,0},{4,3},{5,2},{6,5},{7,4},{8,15},{9,14},{10,... | collective-permute-start | bytes 12296 | tf_op jit(solution)/shard_map/ppermute | solution.py:83
  52.8 1.1 %shard_map.218 = f32[2,4,64,128]{3,2,1,0:T(8,128)} custom-call(f32[8,512]{1,0:T(8,128)S(1)} %get-tuple-element.59.total, f32[520,128]{1,0:T(8,128)S(1)} %shard_map.206.refs_4_.packed), custom_call_target="tpu_custom_call" | custom-call | flops 1000000000 | bytes 65536 | tf_op jit(solution)/shard_map/pallas_call | solution.py:37
  54.2 2.6 %collective-permute-done.23.refs_2_ = bf16[8,256]{1,0:T(8,128)(2,1)S(1)} collective-permute-done((bf16[8,256]{1,0:T(8,128)(2,1)S(1)}, bf16[8,256]{1,0:T(8,128)(2,1)S(1)}, u32[]{:S(2)}, u32[]{:S(2)}) %collective-permute-start.23) | collective-permute-done | bytes 4128 | tf_op jit(solution)/shard_map/ppermute | solution.py:83
  (83 shorter events, 10.2 us)
Async XLA Ops:
  0.6 6.2 %collective-permute-start = (bf16[8,256]{1,0:T(8,128)(2,1)}, bf16[8,256]{1,0:T(8,128)(2,1)S(1)}, u32[]{:S(2)}, u32[]{:S(2)}) collective-permute-start(bf16[8,256]{1,0:T(8,128)(2,1)} %x.1), channel_id=1, source_target_pairs={{0,1},{1,0},{2,3},{3,2},{4,5},{5,4},{6,7},{7,6},{8,9},{9,8},{10,11... | collective-permute-start | bytes 12296 | tf_op jit(solution)/shard_map/ppermute | solution.py:49
  6.2 20.7 %collective-permute-start.9 = (bf16[512,1792]{1,0:T(8,128)(2,1)S(1)}, bf16[512,1792]{1,0:T(8,128)(2,1)S(1)}, u32[]{:S(2)}, u32[]{:S(2)}) collective-permute-start(bf16[512,1792]{1,0:T(8,128)(2,1)S(1)} %shard_map.204.refs_6_), channel_id=1, source_target_pairs={{0,1},{1,0},{2,3},{3,2},{4,5},{5,4},{6,7},{7,6},{8,9},{9,8},{10,11... | collective-permute-start | bytes 5505032 | tf_op jit(solution)/shard_map/ppermute | solution.py:49
  6.8 5.5 %copy-start = (bf16[2048,704]{0,1:T(8,128)(2,1)S(1)}, bf16[2048,704]{0,1:T(8,128)(2,1)}, u32[]{:S(2)}) copy-start(bf16[2048,704]{0,1:T(8,128)(2,1)} %param.23) | copy-start | bytes 8650756
  6.8 5.5 %copy-start.1 = (bf16[2048,704]{0,1:T(8,128)(2,1)S(1)}, bf16[2048,704]{0,1:T(8,128)(2,1)}, u32[]{:S(2)}) copy-start(bf16[2048,704]{0,1:T(8,128)(2,1)} %param.24) | copy-start | bytes 8650756
  6.8 5.5 %copy-start.5 = (bf16[704,2048]{1,0:T(8,128)(2,1)S(1)}, bf16[704,2048]{1,0:T(8,128)(2,1)}, u32[]{:S(2)}) copy-start(bf16[704,2048]{1,0:T(8,128)(2,1)} %w_down.6) | copy-start | bytes 8650756
  6.9 5.5 %copy-start.12 = (f32[2048]{0:T(1024)S(1)}, f32[2048]{0:T(1024)}, u32[]{:S(2)}) copy-start(f32[2048]{0:T(1024)} %param.22) | copy-start | bytes 24580
  6.9 6.1 %collective-permute-start.3 = (bf16[8,512]{1,0:T(8,128)(2,1)S(1)}, bf16[8,512]{1,0:T(8,128)(2,1)S(1)}, u32[]{:S(2)}, u32[]{:S(2)}) collective-permute-start(bf16[8,512]{1,0:T(8,128)(2,1)S(1)} %shard_map.196.x.refs_4_), channel_id=1, source_target_pairs={{0,3},{1,2},{2,5},{3,4},{4,7},{5,6},{6,1},{7,0},{8,11},{9,10},{10,... | collective-permute-start | bytes 24584 | tf_op jit(solution)/shard_map/ppermute | solution.py:83
  9.6 3.8 %collective-permute-start.2 = (bf16[8,512]{1,0:T(8,128)(2,1)S(1)}, bf16[8,512]{1,0:T(8,128)(2,1)S(1)}, u32[]{:S(2)}, u32[]{:S(2)}) collective-permute-start(bf16[8,512]{1,0:T(8,128)(2,1)S(1)} %shard_map.196.x.refs_4_), channel_id=1, source_target_pairs={{0,7},{1,6},{2,1},{3,0},{4,3},{5,2},{6,5},{7,4},{8,15},{9,14},{10,... | collective-permute-start | bytes 24584 | tf_op jit(solution)/shard_map/ppermute | solution.py:83
  11.7 4.0 %collective-permute-start.1 = (bf16[8,512]{1,0:T(8,128)(2,1)S(1)}, bf16[8,512]{1,0:T(8,128)(2,1)S(1)}, u32[]{:S(2)}, u32[]{:S(2)}) collective-permute-start(bf16[8,512]{1,0:T(8,128)(2,1)S(1)} %shard_map.196.x.refs_4_), channel_id=1, source_target_pairs={{0,5},{1,4},{2,7},{3,6},{4,1},{5,0},{6,3},{7,2},{8,13},{9,12},{10,... | collective-permute-start | bytes 24584 | tf_op jit(solution)/shard_map/ppermute | solution.py:83
  16.7 2.1 %collective-permute-start.4 = (f32[3,8,512]{2,1,0:T(8,128)S(1)}, f32[3,8,512]{2,1,0:T(8,128)S(1)}, u32[]{:S(2)}, u32[]{:S(2)}) collective-permute-start(f32[3,8,512]{2,1,0:T(8,128)S(1)} %shard_map.201.mine), channel_id=1, source_target_pairs={{0,1},{1,0},{2,3},{3,2},{4,5},{5,4},{6,7},{7,6},{8,9},{9,8},{10,11... | collective-permute-start | bytes 147464 | tf_op jit(solution)/shard_map/ppermute | solution.py:49
  16.8 1.2 %collective-permute-start.7 = (f32[8,512]{1,0:T(8,128)S(1)}, f32[8,512]{1,0:T(8,128)S(1)}, u32[]{:S(2)}, u32[]{:S(2)}) collective-permute-start(f32[8,512]{1,0:T(8,128)S(1)} %get-tuple-element.41.mine), channel_id=1, source_target_pairs={{0,1},{1,0},{2,3},{3,2},{4,5},{5,4},{6,7},{7,6},{8,9},{9,8},{10,11... | collective-permute-start | bytes 49160 | tf_op jit(solution)/shard_map/ppermute | solution.py:49
  17.3 13.5 %collective-permute-start.13 = (f32[520,128]{1,0:T(8,128)S(1)}, f32[520,128]{1,0:T(8,128)S(1)}, u32[]{:S(2)}, u32[]{:S(2)}) collective-permute-start(f32[520,128]{1,0:T(8,128)S(1)} %shard_map.206.refs_4_.packed), channel_id=1, source_target_pairs={{0,1},{1,0},{2,3},{3,2},{4,5},{5,4},{6,7},{7,6},{8,9},{9,8},{10,11... | collective-permute-start | bytes 798728 | tf_op jit(solution)/shard_map/ppermute | solution.py:49
  17.5 20.0 %collective-permute-start.17 = (bf16[512,512]{1,0:T(8,128)(2,1)S(1)}, bf16[512,512]{1,0:T(8,128)(2,1)S(1)}, u32[]{:S(2)}, u32[]{:S(2)}) collective-permute-start(bf16[512,512]{1,0:T(8,128)(2,1)S(1)} %copy-done.17), channel_id=1, source_target_pairs={{0,1},{1,0},{2,3},{3,2},{4,5},{5,4},{6,7},{7,6},{8,9},{9,8},{10,11... | collective-permute-start | bytes 1572872 | tf_op jit(solution)/shard_map/ppermute | solution.py:49
  18.1 8.9 %copy-start.16 = (f32[512]{0:T(512)S(1)}, f32[512]{0:T(512)}, u32[]{:S(2)}) copy-start(f32[512]{0:T(512)} %param.26) | copy-start | bytes 6148
  18.1 4.0 %collective-permute-start.8 = (bf16[8,512]{1,0:T(8,128)(2,1)S(1)}, bf16[8,512]{1,0:T(8,128)(2,1)S(1)}, u32[]{:S(2)}, u32[]{:S(2)}) collective-permute-start(bf16[8,512]{1,0:T(8,128)(2,1)S(1)} %shard_map.203), channel_id=1, source_target_pairs={{0,5},{1,4},{2,7},{3,6},{4,1},{5,0},{6,3},{7,2},{8,13},{9,12},{10,... | collective-permute-start | bytes 24584 | tf_op jit(solution)/shard_map/ppermute | solution.py:83
  18.8 5.0 %collective-permute-start.5 = (bf16[8,512]{1,0:T(8,128)(2,1)S(1)}, bf16[8,512]{1,0:T(8,128)(2,1)S(1)}, u32[]{:S(2)}, u32[]{:S(2)}) collective-permute-start(bf16[8,512]{1,0:T(8,128)(2,1)S(1)} %get-tuple-element.39), channel_id=1, source_target_pairs={{0,3},{1,2},{2,1},{3,0},{4,7},{5,6},{6,5},{7,4},{8,11},{9,10},{10,... | collective-permute-start | bytes 24584 | tf_op jit(solution)/shard_map/ppermute | solution.py:83
  22.1 4.9 %collective-permute-start.6 = (bf16[8,512]{1,0:T(8,128)(2,1)S(1)}, bf16[8,512]{1,0:T(8,128)(2,1)S(1)}, u32[]{:S(2)}, u32[]{:S(2)}) collective-permute-start(bf16[8,512]{1,0:T(8,128)(2,1)S(1)} %get-tuple-element.40), channel_id=1, source_target_pairs={{0,7},{1,6},{2,5},{3,4},{4,3},{5,2},{6,1},{7,0},{8,15},{9,14},{10,... | collective-permute-start | bytes 24584 | tf_op jit(solution)/shard_map/ppermute | solution.py:83
  27.6 3.2 %collective-permute-start.10 = (bf16[8,1024]{1,0:T(8,128)(2,1)S(1)}, bf16[8,1024]{1,0:T(8,128)(2,1)S(1)}, u32[]{:S(2)}, u32[]{:S(2)}) collective-permute-start(bf16[8,1024]{1,0:T(8,128)(2,1)S(1)} %get-tuple-element.43), channel_id=1, source_target_pairs={{0,3},{1,2},{2,1},{3,0},{4,7},{5,6},{6,5},{7,4},{8,11},{9,10},{10,... | collective-permute-start | bytes 49160 | tf_op jit(solution)/shard_map/ppermute | solution.py:83
  27.6 5.1 %collective-permute-start.11 = (bf16[8,1024]{1,0:T(8,128)(2,1)S(1)}, bf16[8,1024]{1,0:T(8,128)(2,1)S(1)}, u32[]{:S(2)}, u32[]{:S(2)}) collective-permute-start(bf16[8,1024]{1,0:T(8,128)(2,1)S(1)} %get-tuple-element.44), channel_id=1, source_target_pairs={{0,7},{1,6},{2,5},{3,4},{4,3},{5,2},{6,1},{7,0},{8,15},{9,14},{10,... | collective-permute-start | bytes 49160 | tf_op jit(solution)/shard_map/ppermute | solution.py:83
  29.4 4.1 %collective-permute-start.12 = (bf16[8,1024]{1,0:T(8,128)(2,1)S(1)}, bf16[8,1024]{1,0:T(8,128)(2,1)S(1)}, u32[]{:S(2)}, u32[]{:S(2)}) collective-permute-start(bf16[8,1024]{1,0:T(8,128)(2,1)S(1)} %get-tuple-element.45), channel_id=1, source_target_pairs={{0,5},{1,4},{2,7},{3,6},{4,1},{5,0},{6,3},{7,2},{8,13},{9,12},{10,... | collective-permute-start | bytes 49160 | tf_op jit(solution)/shard_map/ppermute | solution.py:83
  34.0 3.5 %collective-permute-start.14 = (bf16[2,1024]{1,0:T(2,128)(2,1)S(1)}, bf16[2,1024]{1,0:T(2,128)(2,1)S(1)}, u32[]{:S(2)}, u32[]{:S(2)}) collective-permute-start(bf16[2,1024]{1,0:T(2,128)(2,1)S(1)} %get-tuple-element.46.refs_0_), channel_id=1, source_target_pairs={{0,3},{1,2},{2,1},{3,0},{4,7},{5,6},{6,5},{7,4},{8,11},{9,10},{10,... | collective-permute-start | bytes 12296 | tf_op jit(solution)/shard_map/ppermute | solution.py:83
  34.8 4.8 %collective-permute-start.15 = (bf16[2,1024]{1,0:T(2,128)(2,1)S(1)}, bf16[2,1024]{1,0:T(2,128)(2,1)S(1)}, u32[]{:S(2)}, u32[]{:S(2)}) collective-permute-start(bf16[2,1024]{1,0:T(2,128)(2,1)S(1)} %get-tuple-element.46.refs_0_), channel_id=1, source_target_pairs={{0,7},{1,6},{2,5},{3,4},{4,3},{5,2},{6,1},{7,0},{8,15},{9,14},{10,... | collective-permute-start | bytes 12296 | tf_op jit(solution)/shard_map/ppermute | solution.py:83
  36.7 3.9 %collective-permute-start.16 = (bf16[2,1024]{1,0:T(2,128)(2,1)S(1)}, bf16[2,1024]{1,0:T(2,128)(2,1)S(1)}, u32[]{:S(2)}, u32[]{:S(2)}) collective-permute-start(bf16[2,1024]{1,0:T(2,128)(2,1)S(1)} %get-tuple-element.46.refs_0_), channel_id=1, source_target_pairs={{0,5},{1,4},{2,7},{3,6},{4,1},{5,0},{6,3},{7,2},{8,13},{9,12},{10,... | collective-permute-start | bytes 12296 | tf_op jit(solution)/shard_map/ppermute | solution.py:83
  40.6 3.7 %copy-start.13 = (f32[2048]{0:T(1024)S(1)}, f32[2048]{0:T(1024)}, u32[]{:S(2)}) copy-start(f32[2048]{0:T(1024)} %param.34) | copy-start | bytes 24580
  40.8 4.9 %collective-permute-start.20 = (bf16[8,512]{1,0:T(8,128)(2,1)S(1)}, bf16[8,512]{1,0:T(8,128)(2,1)S(1)}, u32[]{:S(2)}, u32[]{:S(2)}) collective-permute-start(bf16[8,512]{1,0:T(8,128)(2,1)S(1)} %shard_map.208.x.after), channel_id=1, source_target_pairs={{0,7},{1,6},{2,5},{3,4},{4,3},{5,2},{6,1},{7,0},{8,15},{9,14},{10,... | collective-permute-start | bytes 24584 | tf_op jit(solution)/shard_map/ppermute | solution.py:83
  42.5 3.7 %collective-permute-start.19 = (bf16[8,512]{1,0:T(8,128)(2,1)S(1)}, bf16[8,512]{1,0:T(8,128)(2,1)S(1)}, u32[]{:S(2)}, u32[]{:S(2)}) collective-permute-start(bf16[8,512]{1,0:T(8,128)(2,1)S(1)} %shard_map.208.x.after), channel_id=1, source_target_pairs={{0,5},{1,4},{2,1},{3,0},{4,7},{5,6},{6,3},{7,2},{8,13},{9,12},{10,... | collective-permute-start | bytes 24584 | tf_op jit(solution)/shard_map/ppermute | solution.py:83
  42.5 4.2 %collective-permute-start.18 = (bf16[8,512]{1,0:T(8,128)(2,1)S(1)}, bf16[8,512]{1,0:T(8,128)(2,1)S(1)}, u32[]{:S(2)}, u32[]{:S(2)}) collective-permute-start(bf16[8,512]{1,0:T(8,128)(2,1)S(1)} %shard_map.208.x.after), channel_id=1, source_target_pairs={{0,3},{1,2},{2,7},{3,6},{4,1},{5,0},{6,5},{7,4},{8,11},{9,10},{10,... | collective-permute-start | bytes 24584 | tf_op jit(solution)/shard_map/ppermute | solution.py:83
  47.7 2.2 %collective-permute-start.21 = (f32[3,8,256]{2,1,0:T(8,128)S(1)}, f32[3,8,256]{2,1,0:T(8,128)S(1)}, u32[]{:S(2)}, u32[]{:S(2)}) collective-permute-start(f32[3,8,256]{2,1,0:T(8,128)S(1)} %shard_map.214), channel_id=1, source_target_pairs={{0,1},{1,0},{2,3},{3,2},{4,5},{5,4},{6,7},{7,6},{8,9},{9,8},{10,11... | collective-permute-start | bytes 73736 | tf_op jit(solution)/shard_map/ppermute | solution.py:49
  48.0 1.2 %collective-permute-start.24 = (f32[8,256]{1,0:T(8,128)S(1)}, f32[8,256]{1,0:T(8,128)S(1)}, u32[]{:S(2)}, u32[]{:S(2)}) collective-permute-start(f32[8,256]{1,0:T(8,128)S(1)} %get-tuple-element.58), channel_id=1, source_target_pairs={{0,1},{1,0},{2,3},{3,2},{4,5},{5,4},{6,7},{7,6},{8,9},{9,8},{10,11... | collective-permute-start | bytes 24584 | tf_op jit(solution)/shard_map/ppermute | solution.py:49
  49.2 4.8 %collective-permute-start.25 = (bf16[8,256]{1,0:T(8,128)(2,1)S(1)}, bf16[8,256]{1,0:T(8,128)(2,1)S(1)}, u32[]{:S(2)}, u32[]{:S(2)}) collective-permute-start(bf16[8,256]{1,0:T(8,128)(2,1)S(1)} %shard_map.216), channel_id=1, source_target_pairs={{0,3},{1,2},{2,5},{3,4},{4,7},{5,6},{6,1},{7,0},{8,11},{9,10},{10,... | collective-permute-start | bytes 12296 | tf_op jit(solution)/shard_map/ppermute | solution.py:83
  49.9 4.3 %collective-permute-start.22 = (bf16[8,256]{1,0:T(8,128)(2,1)S(1)}, bf16[8,256]{1,0:T(8,128)(2,1)S(1)}, u32[]{:S(2)}, u32[]{:S(2)}) collective-permute-start(bf16[8,256]{1,0:T(8,128)(2,1)S(1)} %get-tuple-element.56), channel_id=1, source_target_pairs={{0,7},{1,6},{2,1},{3,0},{4,3},{5,2},{6,5},{7,4},{8,15},{9,14},{10,... | collective-permute-start | bytes 12296 | tf_op jit(solution)/shard_map/ppermute | solution.py:83
  52.8 3.9 %collective-permute-start.23 = (bf16[8,256]{1,0:T(8,128)(2,1)S(1)}, bf16[8,256]{1,0:T(8,128)(2,1)S(1)}, u32[]{:S(2)}, u32[]{:S(2)}) collective-permute-start(bf16[8,256]{1,0:T(8,128)(2,1)S(1)} %get-tuple-element.57), channel_id=1, source_target_pairs={{0,5},{1,4},{2,7},{3,6},{4,1},{5,0},{6,3},{7,2},{8,13},{9,12},{10,... | collective-permute-start | bytes 12296 | tf_op jit(solution)/shard_map/ppermute | solution.py:83
  (13 other events, 20.7 us)
